TPU v7x, 512 devices: a whole 4x4x16 slice. The times are simulated.
512 devices in a mesh: sp: 16 (over z), tp: 4 (over y), dp: 8 (over x, core).
Axes of the slice: x: 4, y: 4, z: 16, core: 2. Of those that a mesh axis runs over, the one named last changes fastest.
Arguments:
- latent: bfloat16 [8, 6144, 2048], P('dp', 'sp'), may hold values from -6 to 6
- conditioning: bfloat16 [8, 2048], P(None, 'sp'), may hold values from -6 to 6
- context_cond: bfloat16 [2048], P('sp'), may hold values from -6 to 6
- modulation: bfloat16 [3, 2048, 2048], P(None, 'sp', ('tp', 'dp')), may hold values from -4.2426407 to 4.2426407
- context: bfloat16 [8, 1024, 2048], P('dp', 'sp'), may hold values from -6 to 6
- query_weight: bfloat16 [2048, 1024], P(None, 'tp'), may hold values from -2.1213203 to 2.1213203
- key_projection: bfloat16 [2048, 256], P(None, 'tp'), may hold values from -0.13258252 to 0.13258252
- value_projection: bfloat16 [2048, 256], P(None, 'tp'), may hold values from -0.125 to 0.125
- out_weight: bfloat16 [1024, 2048], P(None, 'tp'), may hold values from -0.1875 to 0.1875
- sink_head_logit: float32 [16], P('tp'), may hold values from 5 to 7.5
- prefix_logit_bias: float32 [16], P('tp'), may hold values from -2.5 to -1
Outputs:
- updated: float32 [8, 6144, 2048], P('dp', 'sp', 'tp')
All inputs are finite; a program needn't handle non-finite values.
Results may differ from a plain program's by a relative error of at most 0.0073.
Values may be sent and summed in bfloat16 or wider, within the bound.
No kernel may reach another device: no remote copies, remote signals or barrier semaphores. Data moves between devices by JAX's collectives and lax.ppermute only.
A program may use at most 64 MiB of HBM per device.

v0:
```python
import jax
import jax.numpy as jnp
from jax import lax
from jax.sharding import PartitionSpec as P

HEAD_SIZE = 64
GRID_W = 64
WINDOW_REACH = 128


NORM_EPSILON = 1e-06
ROTARY_BASE = 10000.0
MASKED = -1e30


def sent_to_all(value, axis):
    size = lax.axis_size(axis)
    return lax.all_to_all(
        jnp.broadcast_to(value[None], (size, *value.shape)), axis, 0, 0, tiled=True
    )


def over_copies(value, axis):
    everything = sent_to_all(value, axis)
    return jnp.sum(everything, axis=0)


def laid_out(pieces, dim):
    shape = list(pieces.shape[1:])
    shape[dim] *= pieces.shape[0]
    return jnp.moveaxis(pieces, 0, dim).reshape(shape)


def gathered_copies(value, axis, dim):
    pieces = sent_to_all(value, axis)
    return laid_out(pieces, dim)


def extended(value, sides, width):
    for axis, dim in sides:
        size, length = (lax.axis_size(axis), value.shape[dim])
        up = [(i, (i + 1) % size) for i in range(size - 1)]
        down = [(j, i) for i, j in up]
        last = lax.slice_in_dim(value, length - width, length, axis=dim)
        leading = lax.slice_in_dim(value, 0, width, axis=dim)
        before = lax.ppermute(last, axis, up)
        after = lax.ppermute(leading, axis, down)
        value = jnp.concatenate([before, value, after], axis=dim)
    return value


def layer_norm(tok_rows):
    vectors = tok_rows.astype(jnp.float32)
    centre = jnp.mean(vectors, axis=-1, keepdims=True)
    spread = jnp.mean(jnp.square(vectors - centre), axis=-1, keepdims=True)
    return (vectors - centre) * lax.rsqrt(spread + NORM_EPSILON)


def turn_half(segment, token_positions):
    half_width = segment.shape[-1]
    quarter = half_width // 2
    frequency = ROTARY_BASE ** (-jnp.arange(0, half_width, 2, dtype=jnp.float32) / half_width)
    angles = token_positions.astype(jnp.float32)[:, None] * frequency[None, :]
    cosine = jnp.cos(angles)[:, None, :]
    sine_table = jnp.sin(angles)[:, None, :]
    leading = segment[..., :quarter]
    trailing = segment[..., quarter:]
    return jnp.concatenate(
        [leading * cosine - trailing * sine_table, trailing * cosine + leading * sine_table],
        axis=-1,
    )


def apply_rotary(head_rows, token_positions):
    half_width = head_rows.shape[-1] // 2
    return jnp.concatenate(
        [
            turn_half(head_rows[..., :half_width], token_positions // GRID_W),
            turn_half(head_rows[..., half_width:], token_positions % GRID_W),
        ],
        axis=-1,
    )


def per_device(
    latent,
    conditioning,
    context_cond,
    modulation,
    context,
    query_weight,
    key_projection,
    value_projection,
    out_weight,
    sink_head_logit,
    prefix_logit_bias,
):
    sample = lax.axis_index("dp")
    samples = conditioning.shape[0]
    cond_rows = jnp.concatenate([conditioning, context_cond[None, :]], axis=0)
    activated = jax.nn.silu(cond_rows.astype(jnp.float32)).astype(jnp.bfloat16)
    partial_value = jnp.einsum(
        "sd,mdc->msc", activated, modulation, preferred_element_type=jnp.float32
    )
    summed = over_copies(partial_value, "sp")
    mod_all = gathered_copies(summed, ("tp", "dp"), 2)
    mod_shift = lax.dynamic_index_in_dim(mod_all[0], sample, 0, keepdims=False)
    mod_scale = lax.dynamic_index_in_dim(mod_all[1], sample, 0, keepdims=False)
    mod_gate = lax.dynamic_index_in_dim(mod_all[2], sample, 0, keepdims=False)
    ctx_shift = mod_all[0, samples]
    ctx_scale = mod_all[1, samples]
    ctx_normed = (layer_norm(context[0]) * (1.0 + ctx_scale) + ctx_shift).astype(jnp.bfloat16)
    prefix_keys = jnp.dot(ctx_normed, key_projection, preferred_element_type=jnp.float32).astype(
        jnp.bfloat16
    )
    prefix_values = jnp.dot(
        ctx_normed, value_projection, preferred_element_type=jnp.float32
    ).astype(jnp.bfloat16)
    context_pairs = gathered_copies(jnp.concatenate([prefix_keys, prefix_values], axis=1), "sp", 0)
    tok_rows = latent.shape[1]
    own_rows = latent[0]
    normalized_input = (layer_norm(own_rows) * (1.0 + mod_scale) + mod_shift).astype(jnp.bfloat16)
    offset = lax.axis_index("sp") * tok_rows
    token_positions = offset + jnp.arange(tok_rows, dtype=jnp.int32)
    local_heads = query_weight.shape[1] // HEAD_SIZE
    local_kv = key_projection.shape[1] // HEAD_SIZE
    heads_per_group = local_heads // local_kv
    kv_width = local_kv * HEAD_SIZE
    query_rows = apply_rotary(
        jnp.dot(normalized_input, query_weight, preferred_element_type=jnp.float32).reshape(
            tok_rows, local_heads, HEAD_SIZE
        ),
        token_positions,
    ).astype(jnp.bfloat16)
    key_token_rows = apply_rotary(
        jnp.dot(normalized_input, key_projection, preferred_element_type=jnp.float32).reshape(
            tok_rows, local_kv, HEAD_SIZE
        ),
        token_positions,
    ).astype(jnp.bfloat16)
    value_token_rows = jnp.dot(
        normalized_input, value_projection, preferred_element_type=jnp.float32
    ).astype(jnp.bfloat16)
    own_pairs = jnp.concatenate(
        [key_token_rows.reshape(tok_rows, kv_width), value_token_rows], axis=1
    )
    padded = extended(own_pairs, (("sp", 0),), WINDOW_REACH)
    block_list = tok_rows // WINDOW_REACH
    stacked = padded.reshape(block_list + 2, WINDOW_REACH, 2 * kv_width)
    window_pairs = jnp.concatenate([stacked[:-2], stacked[1:-1], stacked[2:]], axis=1)
    window_keys = window_pairs[..., :kv_width].reshape(
        block_list, 3 * WINDOW_REACH, local_kv, HEAD_SIZE
    )
    window_values = window_pairs[..., kv_width:].reshape(
        block_list, 3 * WINDOW_REACH, local_kv, HEAD_SIZE
    )
    context_keys = context_pairs[:, :kv_width].reshape(-1, local_kv, HEAD_SIZE)
    context_values = context_pairs[:, kv_width:].reshape(-1, local_kv, HEAD_SIZE)
    query_block_list = query_rows.reshape(
        block_list, WINDOW_REACH, local_kv, heads_per_group, HEAD_SIZE
    )
    block_start = jnp.arange(block_list, dtype=jnp.int32)[:, None] * WINDOW_REACH
    query_pos = block_start + jnp.arange(WINDOW_REACH, dtype=jnp.int32)[None, :]
    key_pos = block_start - WINDOW_REACH + jnp.arange(3 * WINDOW_REACH, dtype=jnp.int32)[None, :]
    global_key = key_pos + offset
    inside = (global_key >= 0) & (global_key < tok_rows * lax.axis_size("sp"))
    valid = (jnp.abs(query_pos[:, :, None] - key_pos[:, None, :]) <= WINDOW_REACH) & inside[
        :, None, :
    ]
    factor = HEAD_SIZE ** (-0.5)
    win_scores = (
        jnp.einsum(
            "nqkgd,njkd->nkgqj", query_block_list, window_keys, preferred_element_type=jnp.float32
        )
        * factor
    )
    win_scores = jnp.where(valid[:, None, None, :, :], win_scores, MASKED)
    head_bias_rows = prefix_logit_bias.reshape(local_kv, heads_per_group)[None, :, :, None, None]
    ctx_scores = (
        jnp.einsum(
            "nqkgd,ckd->nkgqc", query_block_list, context_keys, preferred_element_type=jnp.float32
        )
        * factor
        + head_bias_rows
    )
    sink_head_rows = sink_head_logit.reshape(local_kv, heads_per_group)[None, :, :, None]
    highest = jnp.maximum(
        jnp.maximum(jnp.max(win_scores, axis=-1), jnp.max(ctx_scores, axis=-1)), sink_head_rows
    )
    win_exp = jnp.exp(win_scores - highest[..., None])
    ctx_exp = jnp.exp(ctx_scores - highest[..., None])
    denominator = (
        jnp.sum(win_exp, axis=-1) + jnp.sum(ctx_exp, axis=-1) + jnp.exp(sink_head_rows - highest)
    )
    win_probs = (win_exp / denominator[..., None]).astype(jnp.bfloat16)
    ctx_probs = (ctx_exp / denominator[..., None]).astype(jnp.bfloat16)
    attended = jnp.einsum(
        "nkgqj,njkd->nqkgd", win_probs, window_values, preferred_element_type=jnp.float32
    )
    attended = attended + jnp.einsum(
        "nkgqc,ckd->nqkgd", ctx_probs, context_values, preferred_element_type=jnp.float32
    )
    attended = attended.astype(jnp.bfloat16).reshape(tok_rows, local_heads * HEAD_SIZE)
    col_width = out_weight.shape[1]
    mixed = jnp.dot(
        lax.all_gather(attended, "tp", axis=1, tiled=True),
        out_weight,
        preferred_element_type=jnp.float32,
    )
    col_start = lax.axis_index("tp") * col_width
    residual = lax.dynamic_slice_in_dim(own_rows, col_start, col_width, 1).astype(jnp.float32)
    gate_cols = lax.dynamic_slice_in_dim(mod_gate, col_start, col_width, 0)
    return (residual + gate_cols * mixed)[None]


def solution(mesh):
    placed = (
        P("dp", "sp", None),
        P(None, "sp"),
        P("sp"),
        P(None, "sp", ("tp", "dp")),
        P("dp", "sp", None),
        P(None, "tp"),
        P(None, "tp"),
        P(None, "tp"),
        P(None, "tp"),
        P("tp"),
        P("tp"),
    )
    return jax.shard_map(
        per_device, mesh=mesh, in_specs=placed, out_specs=P("dp", "sp", "tp"), check_vma=False
    )
```

profile of v0, /device:TPU:32, one launch (start us, length us, event | category | flops | bytes accessed | tf_op | source)
XLA Modules:
  0.0 112.0 jit_solution(2030573647287617)
XLA Ops:
  0.0 1.1 convolution_bitcast_fusion.2
  2.1 15.2 %all-to-all-start = ((f32[16,1,1728]{2,1,0:T(1,128)}), f32[16,1,1728]{2,1,0:T(1,128)S(1)}, u32[]{:S(2)}, u32[]{:S(2)}) async-start(f32[16,1,1728]{2,1,0:T(1,128)} %reshape.534), calls=%async_computation | async-start | bytes 229376 | tf_op jit(solution)/shard_map/all_to_all | solution.py:18
  17.4 1.1 convert_reduce_fusion.1
  18.5 1.2 %fusion.40 = f32[64]{0:T(128)S(1)} fusion(bf16[1,64,2048]{2,1,0:T(8,128)(2,1)} %param.15, f32[64]{0:T(128)S(1)} %broadcast_multiply_fusion.1), kind=kLoop, calls=%fused_computation.55 | loop fusion | flops 524224 | bytes 262656 | tf_op jit(solution)/shard_map/reduce_sum | solution.py:55
  19.7 1.7 %convert_reduce_fusion = f32[384]{0:T(512)S(1)} fusion(bf16[1,384,2048]{2,1,0:T(8,128)(2,1)} %param.11), kind=kLoop, calls=%fused_computation.7 | loop fusion | flops 1572480 | bytes 1574400 | tf_op jit(solution)/shard_map/reduce_sum | solution.py:54
  23.3 2.3 %copy.49 = bf16[2048,256]{0,1:T(8,128)(2,1)} copy(bf16[2048,256]{1,0:T(8,128)(2,1)} %param.16) | data formatting | bytes 2097152 | tf_op args[5]
  26.9 3.9 %all-to-all-done = f32[16,1,1728]{2,1,0:T(1,128)S(1)} async-done(((f32[16,1,1728]{2,1,0:T(1,128)}), f32[16,1,1728]{2,1,0:T(1,128)S(1)}, u32[]{:S(2)}, u32[]{:S(2)}) %all-to-all-start) | async-done | bytes 110624 | tf_op jit(solution)/shard_map/all_to_all | solution.py:18
  32.7 1.2 %reshape.536 = f32[32,1,1728]{2,1,0:T(1,128)} reshape(f32[32,9,3,64]{3,2,1,0:T(4,128)S(1)} %broadcast_bitcast_fusion) | data formatting | bytes 442368
  33.8 7.3 %all-to-all-start.1 = ((f32[32,1,1728]{2,1,0:T(1,128)}), f32[32,1,1728]{2,1,0:T(1,128)S(1)}, u32[]{:S(2)}, u32[]{:S(2)}) async-start(f32[32,1,1728]{2,1,0:T(1,128)} %reshape.536), calls=%async_computation.1 | async-start | bytes 458752 | tf_op jit(solution)/shard_map/all_to_all | solution.py:18
  41.7 7.9 %all-to-all-done.1 = f32[32,1,1728]{2,1,0:T(1,128)S(1)} async-done(((f32[32,1,1728]{2,1,0:T(1,128)}), f32[32,1,1728]{2,1,0:T(1,128)S(1)}, u32[]{:S(2)}, u32[]{:S(2)}) %all-to-all-start.1) | async-done | bytes 221216 | tf_op jit(solution)/shard_map/all_to_all | solution.py:18
  49.6 1.9 %reduce.7 = f32[32,1728]{1,0:T(8,128)} reduce(f32[32,1,1728]{2,1,0:T(1,128)S(1)} %all-to-all-done.1, f32[]{:T(128)} %broadcast.437), dimensions={1}, to_apply=%all_to_all.10.reduce_sub_computation | reduce | bytes 442372 | tf_op jit(solution)/shard_map/all_to_all | solution.py:18
  51.5 1.2 %reshape.537 = f32[32,9,3,64]{3,2,1,0:T(4,128)S(1)} reshape(f32[32,1728]{1,0:T(8,128)} %reduce.7) | data formatting | bytes 442368
  52.9 1.1 fusion.88
  53.9 0.9 reshape.522
  55.7 1.3 %convolution_convert_fusion.1 = bf16[64,64]{1,0:T(8,128)(2,1)S(1)} fusion(bf16[2048,64]{0,1:T(8,128)(2,1)} %param.18, bf16[1,64,2048]{2,1,0:T(8,128)(2,1)} %param.15, f32[2048]{0:T(1024)S(1)} %bitcast.232, f32[2048]{0:T(1024)S(1)} %bitcast.230, f32[64]{0:T(128)} %add_rsqrt_fusion.1, f32[64]{0:T(128)} %copy-done.16), kind=kOutput, calls=%fused_computation.46 | convolution fusion | flops 17567744 | bytes 549376 | tf_op jit(solution)/shard_map/dot_general | solution.py:116
  57.1 1.3 %convolution_convert_fusion.2 = bf16[64,64]{1,0:T(8,128)(2,1)S(1)} fusion(bf16[2048,64]{0,1:T(8,128)(2,1)} %param.17, bf16[1,64,2048]{2,1,0:T(8,128)(2,1)S(1)} %copy-done.4, f32[2048]{0:T(1024)S(1)} %bitcast.233, f32[2048]{0:T(1024)S(1)} %bitcast.231, f32[64]{0:T(128)} %add_rsqrt_fusion.1, f32[64]{0:T(128)} %copy-done.16), kind=kOutput, calls=%fused_computation.47 | convolution fusion | flops 17567744 | bytes 549376 | tf_op jit(solution)/shard_map/dot_general | solution.py:113
  58.4 0.9 copy.42
  59.4 0.9 copy.41
  61.2 8.1 %all-to-all-start.2 = ((bf16[16,64,128]{2,1,0:T(8,128)(2,1)}), bf16[16,64,128]{2,1,0:T(8,128)(2,1)S(1)}, u32[]{:S(2)}, u32[]{:S(2)}) async-start(bf16[16,64,128]{2,1,0:T(8,128)(2,1)} %broadcast_in_dim.23), calls=%async_computation.2 | async-start | bytes 524288 | tf_op jit(solution)/shard_map/all_to_all | solution.py:18
  69.4 1.4 %fusion.8 = bf16[384,2048]{1,0:T(8,128)(2,1)S(1)} fusion(bf16[1,384,2048]{2,1,0:T(8,128)(2,1)S(1)} %copy-done.1, f32[2048]{0:T(1024)S(1)} %bitcast.228, f32[2048]{0:T(1024)S(1)} %bitcast.226, f32[384]{0:T(512)} %add_rsqrt_fusion, f32[384]{0:T(512)} %copy-done.9), kind=kLoop, calls=%fused_computation.15 | loop fusion | flops 4718592 | bytes 3165184 | tf_op jit(solution)/shard_map/convert_element_type | solution.py:122
  70.9 0.9 fusion.18
  73.9 3.4 %collective-permute-start = (bf16[128,128]{0,1:T(8,128)(2,1)S(1)}, bf16[128,128]{0,1:T(8,128)(2,1)}, u32[]{:S(2)}, u32[]{:S(2)}) collective-permute-start(bf16[128,128]{0,1:T(8,128)(2,1)S(1)} %get-tuple-element.18), channel_id=1, source_target_pairs={{0,32},{32,64},{64,96},{96,128},{128,160},{160,192},{192,224},{224... | collective-permute-start | bytes 98312 | tf_op jit(solution)/shard_map/ppermute | solution.py:46
  77.3 3.2 %collective-permute-start.1 = (bf16[128,128]{0,1:T(8,128)(2,1)S(1)}, bf16[128,128]{0,1:T(8,128)(2,1)}, u32[]{:S(2)}, u32[]{:S(2)}) collective-permute-start(bf16[128,128]{0,1:T(8,128)(2,1)S(1)} %get-tuple-element.19), channel_id=1, source_target_pairs={{32,0},{64,32},{96,64},{128,96},{160,128},{192,160},{224,192},{256... | collective-permute-start | bytes 98312 | tf_op jit(solution)/shard_map/ppermute | solution.py:47
  82.0 1.0 squeeze.16
  83.0 1.6 %copy.47 = bf16[3,128,128]{1,2,0:T(8,128)(2,1)} copy(bf16[3,128,128]{2,1,0:T(8,128)(2,1)} %bitcast.223) | data formatting | bytes 196608 | tf_op jit(solution)/shard_map/slice | solution.py:150
  87.3 1.0 pad_maximum_fusion
  88.3 1.9 %fusion.16 = (f32[3,4,128]{2,1,0:T(4,128)S(1)}, f32[3,384,128,4]{2,1,3,0:T(8,128)}) fusion(pred[3,128,384]{1,2,0:T(8,128)(4,1)S(1)} %fusion.36, bf16[3,128,4,64]{1,3,2,0:T(8,128)(2,1)S(1)} %bitcast_dynamic-update-slice_fusion, bf16[3,384,128]{1,2,0:T(8,128)(2,1)S(1)} %pad_maximum_fusion), kind=kOutput, calls=%fused_computation.26 | convolution fusion | flops 77265408 | bytes 2856960 | tf_op jit(solution)/shard_map/nqkgd,njkd->nkgqj/dot_general | solution.py:172
  90.2 1.0 bitcast_reduce_fusion
  91.3 1.3 %fusion.1 = f32[3,4,128]{2,1,0:T(4,128)S(1)} fusion(f32[1024,3,128,4]{2,0,3,1:T(8,128)S(1)} %get-tuple-element.29, f32[3,4,128]{2,1,0:T(4,128)S(1)} %maximum_maximum_fusion, f32[4]{0:T(128)S(1)} %copy-done.14), kind=kLoop, calls=%fused_computation.5 | loop fusion | flops 6289920 | bytes 6303760 | tf_op jit(solution)/shard_map/reduce_sum | solution.py:193
  93.6 1.7 %fusion.27 = f32[3,128,1,4,64]{1,4,3,0,2:T(8,128)S(1)} fusion(f32[3,4,128]{2,1,0:T(4,128)S(1)} %exponential_add_fusion, f32[3,4,128]{2,1,0:T(4,128)S(1)} %maximum_maximum_fusion, f32[4]{0:T(128)S(1)} %copy-done.14, f32[1024,3,128,4]{2,0,3,1:T(8,128)S(1)} %get-tuple-element.29, bf16[1024,128]{1,0:T(8,128)(2,1)S(1)} %bitcast.219), kind=kOutput, calls=%fused_computation.38 | convolution fusion | flops 209190912 | bytes 6959120 | tf_op jit(solution)/shard_map/nkgqc,ckd->nqkgd/dot_general | solution.py:200
  96.3 14.3 %all_gather.3 = bf16[384,1024]{0,1:T(8,128)(2,1)S(1)} all-gather(bf16[384,256]{0,1:T(8,128)(2,1)S(1)} %bitcast.222), channel_id=1, replica_groups=mesh['sp'=16,'tp'=4,'dp'=8] {'tp'}, dimensions={1}, use_global_device_ids=true | all-gather | bytes 983040 | tf_op jit(solution)/shard_map/all_gather | solution.py:206
  110.6 1.5 %fusion.25 = f32[1,384,512]{2,1,0:T(8,128)} fusion(bf16[384,1024]{0,1:T(8,128)(2,1)S(1)} %all_gather.3, bf16[1024,512]{1,0:T(8,128)(2,1)S(1)} %copy-done, f32[512]{0:T(512)S(1)} %bitcast.234, bf16[1,384,2048]{2,1,0:T(8,128)(2,1)S(1)} %copy-done.1, s32[]{:T(128)S(6)} %select_n.41), kind=kOutput, calls=%fused_computation.35 | convolution fusion | flops 403243008 | bytes 3016708 | tf_op jit(solution)/shard_map/dot_general | solution.py:205
  (93 shorter events, 16.7 us)
Async XLA Ops:
  0.0 110.5 %copy-start = (bf16[1024,512]{1,0:T(8,128)(2,1)S(1)}, bf16[1024,512]{1,0:T(8,128)(2,1)}, u32[]{:S(2)}) copy-start(bf16[1024,512]{1,0:T(8,128)(2,1)} %param.19) | copy-start | bytes 3145732
  0.0 22.0 %copy-start.1 = (bf16[1,384,2048]{2,1,0:T(8,128)(2,1)S(1)}, bf16[1,384,2048]{2,1,0:T(8,128)(2,1)}, u32[]{:S(2)}) copy-start(bf16[1,384,2048]{2,1,0:T(8,128)(2,1)} %param.11) | copy-start | bytes 4718596
  2.1 28.8 %all-to-all-start = ((f32[16,1,1728]{2,1,0:T(1,128)}), f32[16,1,1728]{2,1,0:T(1,128)S(1)}, u32[]{:S(2)}, u32[]{:S(2)}) async-start(f32[16,1,1728]{2,1,0:T(1,128)} %reshape.534), calls=%async_computation | async-start | bytes 229376 | tf_op jit(solution)/shard_map/all_to_all | solution.py:18
  17.3 9.1 %copy-start.11 = (f32[16]{0:T(128)}, f32[16]{0:T(128)S(1)}, u32[]{:S(2)}) copy-start(f32[16]{0:T(128)S(1)} %multiply_power_fusion) | copy-start | bytes 196
  18.5 7.9 %copy-start.16 = (f32[64]{0:T(128)}, f32[64]{0:T(128)S(1)}, u32[]{:S(2)}) copy-start(f32[64]{0:T(128)S(1)} %broadcast_multiply_fusion.1) | copy-start | bytes 772
  21.4 0.6 copy-start.9
  33.8 15.8 %all-to-all-start.1 = ((f32[32,1,1728]{2,1,0:T(1,128)}), f32[32,1,1728]{2,1,0:T(1,128)S(1)}, u32[]{:S(2)}, u32[]{:S(2)}) async-start(f32[32,1,1728]{2,1,0:T(1,128)} %reshape.536), calls=%async_computation.1 | async-start | bytes 458752 | tf_op jit(solution)/shard_map/all_to_all | solution.py:18
  52.8 4.3 %copy-start.4 = (bf16[1,64,2048]{2,1,0:T(8,128)(2,1)S(1)}, bf16[1,64,2048]{2,1,0:T(8,128)(2,1)}, u32[]{:S(2)}) copy-start(bf16[1,64,2048]{2,1,0:T(8,128)(2,1)} %param.15) | copy-start | bytes 786436
  57.1 13.7 %copy-start.10 = (f32[384]{0:T(512)S(1)}, f32[384]{0:T(512)}, u32[]{:S(2)}) copy-start(f32[384]{0:T(512)} %copy-done.9) | copy-start | bytes 4612
  57.1 13.7 %copy-start.13 = (f32[384]{0:T(512)S(1)}, f32[384]{0:T(512)}, u32[]{:S(2)}) copy-start(f32[384]{0:T(512)} %add_rsqrt_fusion) | copy-start | bytes 4612
  61.2 29.0 %all-to-all-start.2 = ((bf16[16,64,128]{2,1,0:T(8,128)(2,1)}), bf16[16,64,128]{2,1,0:T(8,128)(2,1)S(1)}, u32[]{:S(2)}, u32[]{:S(2)}) async-start(bf16[16,64,128]{2,1,0:T(8,128)(2,1)} %broadcast_in_dim.23), calls=%async_computation.2 | async-start | bytes 524288 | tf_op jit(solution)/shard_map/all_to_all | solution.py:18
  69.3 1.5 %copy-start.3 = (bf16[2048,256]{0,1:T(8,128)(2,1)S(1)}, bf16[2048,256]{0,1:T(8,128)(2,1)}, u32[]{:S(2)}) copy-start(bf16[2048,256]{0,1:T(8,128)(2,1)} %copy.49) | copy-start | bytes 3145732
  70.8 1.0 copy-start.8
  70.8 1.1 copy-start.7
  70.8 1.7 %copy-start.12 = (f32[16]{0:T(128)S(1)}, f32[16]{0:T(128)}, u32[]{:S(2)}) copy-start(f32[16]{0:T(128)} %copy-done.11) | copy-start | bytes 196
  70.8 2.4 %copy-start.6 = (bf16[2048,64]{0,1:T(8,128)(2,1)S(1)}, bf16[2048,64]{0,1:T(8,128)(2,1)}, u32[]{:S(2)}) copy-start(bf16[2048,64]{0,1:T(8,128)(2,1)} %param.18) | copy-start | bytes 786436
  71.8 9.5 %copy-start.5 = (f32[1,9,32,64]{3,0,1,2:T(1,128)S(1)}, f32[1,9,32,64]{3,0,1,2:T(1,128)}, u32[]{:S(2)}) copy-start(f32[1,9,32,64]{3,0,1,2:T(1,128)} %get-tuple-element.5) | copy-start | bytes 221188
  73.9 16.4 %copy-start.14 = (f32[4]{0:T(128)S(1)}, f32[4]{0:T(128)}, u32[]{:S(2)}) copy-start(f32[4]{0:T(128)} %param.21) | copy-start | bytes 52
  73.9 10.8 %collective-permute-start = (bf16[128,128]{0,1:T(8,128)(2,1)S(1)}, bf16[128,128]{0,1:T(8,128)(2,1)}, u32[]{:S(2)}, u32[]{:S(2)}) collective-permute-start(bf16[128,128]{0,1:T(8,128)(2,1)S(1)} %get-tuple-element.18), channel_id=1, source_target_pairs={{0,32},{32,64},{64,96},{96,128},{128,160},{160,192},{192,224},{224... | collective-permute-start | bytes 98312 | tf_op jit(solution)/shard_map/ppermute | solution.py:46
  77.3 7.4 %collective-permute-start.1 = (bf16[128,128]{0,1:T(8,128)(2,1)S(1)}, bf16[128,128]{0,1:T(8,128)(2,1)}, u32[]{:S(2)}, u32[]{:S(2)}) collective-permute-start(bf16[128,128]{0,1:T(8,128)(2,1)S(1)} %get-tuple-element.19), channel_id=1, source_target_pairs={{32,0},{64,32},{96,64},{128,96},{160,128},{192,160},{224,192},{256... | collective-permute-start | bytes 98312 | tf_op jit(solution)/shard_map/ppermute | solution.py:47
  90.2 1.0 copy-start.15
  91.3 1.7 %copy-start.2 = (f32[3,384,128,4]{2,1,3,0:T(8,128)S(1)}, f32[3,384,128,4]{2,1,3,0:T(8,128)}, u32[]{:S(2)}) copy-start(f32[3,384,128,4]{2,1,3,0:T(8,128)} %get-tuple-element.27) | copy-start | bytes 7077892
where the time goes:
time: 113 us; the launch traced here: 112 us
  starting transfers between devices  37.2 us (33%)
  local copies, waits for them, and re-layouts  18.5 us (16%)
  other arithmetic  17 us (15%)
  blocking collectives  14.3 us (13%)
  matrix products  12.7 us (11%)
  waiting for transfers between devices  11.9 us (11%)
    all_to_all x3, starting transfers between devices, sent_to_all(): lax.all_to_all(jnp.broadcast_to(value[None], (size, *value.shape)), axis,...  30.6 us
    all_gather x1, blocking collectives, per_device(): lax.all_gather(attended, 'tp', axis=1, tiled=True)  14.3 us
    all_to_all x3, waiting for transfers between devices, sent_to_all(): lax.all_to_all(jnp.broadcast_to(value[None], (size, *value.shape)), axis,...  11.9 us
    unnamed x45, local copies, waits for them, and re-layouts  6.88 us
    ppermute x1, starting transfers between devices, extended(): before = lax.ppermute(last, axis, up)  3.37 us
    ppermute x1, starting transfers between devices, extended(): after = lax.ppermute(leading, axis, down)  3.23 us
    reduce_sum x2, other arithmetic, layer_norm(): centre = jnp.mean(vectors, axis=-1, keepdims=True)  2.79 us
    all_to_all x2, other arithmetic, sent_to_all(): lax.all_to_all(jnp.broadcast_to(value[None], (size, *value.shape)), axis,...  2.78 us
  transfers between devices with their start and end apart: 5, of which 2 were waited for; matrix products, arithmetic and copies ran while one was open for 21% of the time, Pallas kernels for 0%

commit v1 on v0

v1 whole, which is shorter than its diff:
```python
import functools

import jax
import jax.numpy as jnp
import numpy as np
from jax import lax
from jax.experimental import pallas as pl
from jax.experimental.pallas import tpu as pltpu
from jax.sharding import PartitionSpec as P

HEAD = 64
GRID_W = 64
REACH = 128
EPS = 1e-06
ROTARY_BASE = 10000.0
MASKED = -1e30
LANES = 128

f32 = jnp.float32
bf16 = jnp.bfloat16
VMEM = pl.BlockSpec(memory_space=pltpu.VMEM)
SMEM = pl.BlockSpec(memory_space=pltpu.SMEM)


def dot_nt(a, b):
    return lax.dot_general(a, b, (((1,), (1,)), ((), ())), preferred_element_type=f32)


def lanes_of(shape):
    return lax.broadcasted_iota(jnp.int32, shape, len(shape) - 1)


def call(kernel, out_shape, ins, scratch=()):
    return pl.pallas_call(
        kernel,
        out_shape=out_shape,
        in_specs=ins,
        out_specs=jax.tree.map(lambda _: VMEM, out_shape),
        scratch_shapes=list(scratch),
    )


def partial_kernel(cond_ref, ctx_ref, mod_ref, out_ref, rows, packed):
    samples = cond_ref.shape[0]
    rows[...] = jnp.zeros_like(rows)
    rows[0:samples, :] = cond_ref[...].astype(f32)
    rows[samples : samples + 1, :] = ctx_ref[...].astype(f32)
    v = rows[...]
    act = (v / (1.0 + jnp.exp(-v))).astype(bf16)
    shift = jnp.dot(act, mod_ref[0], preferred_element_type=f32)
    scale = jnp.dot(act, mod_ref[1], preferred_element_type=f32)
    gate = jnp.dot(act, mod_ref[2], preferred_element_type=f32)
    packed[...] = jnp.concatenate([shift, scale], axis=1)
    packed[9:13, :] = jnp.concatenate([gate[0:4], gate[4:8]], axis=1)
    out_ref[...] = jnp.broadcast_to(packed[...][None], out_ref.shape)


def rows_kernel(in_ref, out_ref, total):
    total[...] = jnp.sum(in_ref[...], axis=0)
    copies = out_ref.shape[0] // 8
    for d in range(8):
        gate = total[9 + d % 4 : 10 + d % 4, :]
        if d >= 4:
            gate = pltpu.roll(gate, 64, 1)
        for t in range(copies):
            out_ref[t * 8 + d, 0:1, :] = total[d : d + 1, :]
            out_ref[t * 8 + d, 1:2, :] = total[8:9, :]
            out_ref[t * 8 + d, 2:3, :] = gate
            out_ref[t * 8 + d, 3:4, :] = gate


def stats_kernel(x_ref, mean_ref, rstd_ref):
    width = x_ref.shape[1]
    step = 64

    def body(i, carry):
        at = pl.ds(pl.multiple_of(i * step, step), step)
        x = x_ref[at, :].astype(f32)
        mean = jnp.sum(x, axis=1, keepdims=True) * (1.0 / width)
        d = x - mean
        var = jnp.sum(d * d, axis=1, keepdims=True) * (1.0 / width)
        mean_ref[at, :] = jnp.broadcast_to(mean, (step, LANES))
        rstd_ref[at, :] = jnp.broadcast_to(lax.rsqrt(var + EPS), (step, LANES))
        return carry

    lax.fori_loop(0, x_ref.shape[0] // step, body, 0)


def stats(x):
    shape = jax.ShapeDtypeStruct((x.shape[0], LANES), f32)
    return call(stats_kernel, (shape, shape), [VMEM])(x)


def mod_tile(rows_ref, row, m):
    a = rows_ref[2 * m, row : row + 1, :]
    b = rows_ref[2 * m + 1, row : row + 1, :]
    low = lanes_of((1, LANES)) < 64
    shift = jnp.where(low, a, pltpu.roll(b, 64, 1))
    scale = jnp.where(low, pltpu.roll(a, 64, 1), b)
    return shift, 1.0 + scale


def modulate(x_ref, mean_ref, rstd_ref, rows_ref, row, out_ref, start):
    n = x_ref.shape[0]
    for m in range(x_ref.shape[1] // LANES):
        shift, scale = mod_tile(rows_ref, row, m)
        cols = slice(m * LANES, (m + 1) * LANES)
        x = x_ref[:, cols].astype(f32)
        y = (x - mean_ref[...]) * rstd_ref[...] * scale + shift
        out_ref[start : start + n, cols] = y.astype(bf16)


def ctx_kernel(x_ref, mean_ref, rstd_ref, rows_ref, wkv_ref, out_ref, normed):
    modulate(x_ref, mean_ref, rstd_ref, rows_ref, 1, normed, 0)
    kv = jnp.dot(normed[...], wkv_ref[...], preferred_element_type=f32).astype(bf16)
    out_ref[...] = jnp.broadcast_to(kv[None], out_ref.shape)


def turned(u, cos, sin):
    low = lanes_of(u.shape) % 32 < 16
    other = jnp.where(low, pltpu.roll(u, LANES - 16, 1), pltpu.roll(u, 16, 1))
    return u * cos + other * sin


def with_ones(kv):
    return jnp.where(lanes_of(kv.shape) < HEAD, jnp.ones_like(kv), kv)


def latent_kernel(
    x_ref, xb_ref, xa_ref, mean_ref, rstd_ref, hmean_ref, hrstd_ref, rows_ref, wq_ref, wkv_ref,
    cos_ref, sin_ref, q_ref, win_ref, normed, kv_s, ones_s,
):
    n = x_ref.shape[0]
    total = n + 2 * REACH
    modulate(xb_ref, hmean_ref.at[0:REACH], hrstd_ref.at[0:REACH], rows_ref, 0, normed, 0)
    modulate(x_ref, mean_ref, rstd_ref, rows_ref, 0, normed, REACH)
    modulate(
        xa_ref, hmean_ref.at[REACH : 2 * REACH], hrstd_ref.at[REACH : 2 * REACH], rows_ref, 0,
        normed, REACH + n,
    )
    cos, sin = cos_ref[...], sin_ref[...]
    key_lane = lanes_of((total, LANES)) < HEAD
    kv = jnp.dot(normed[...], wkv_ref[...], preferred_element_type=f32)
    kv = turned(kv, jnp.where(key_lane, cos, 1.0), jnp.where(key_lane, sin, 0.0)).astype(bf16)
    kv_s[...] = kv
    ones_s[...] = with_ones(kv)
    q = jnp.dot(normed[REACH : REACH + n, :], wq_ref[...], preferred_element_type=f32)
    low = lanes_of((n, LANES)) < HEAD
    own_cos, own_sin = cos_ref[REACH : REACH + n, :], sin_ref[REACH : REACH + n, :]
    for pair in range(q.shape[1] // LANES):
        u = turned(q[:, pair * LANES : (pair + 1) * LANES], own_cos, own_sin) * (HEAD ** -0.5)
        q_ref[2 * pair] = jnp.where(low, u, 0.0).astype(bf16)
        q_ref[2 * pair + 1] = jnp.where(low, pltpu.roll(u, HEAD, 1), 0.0).astype(bf16)
    heads = q_ref.shape[0]
    rows = heads * REACH
    blocks = n // REACH
    i = lax.broadcasted_iota(jnp.int32, (rows, 3 * REACH), 0) % REACH
    j = lanes_of((rows, 3 * REACH))
    near = (j >= i) & (j <= i + 2 * REACH)
    place = lax.axis_index("sp")
    first, last = place == 0, place == lax.axis_size("sp") - 1
    for b in range(blocks):
        qb = q_ref[:, b * REACH : (b + 1) * REACH, :].reshape(rows, LANES)
        s = dot_nt(qb, kv_s[b * REACH : (b + 3) * REACH, :])
        valid = near
        if b == 0:
            valid = valid & (j >= jnp.where(first, REACH, 0))
        if b == blocks - 1:
            valid = valid & (j < jnp.where(last, 2 * REACH, 3 * REACH))
        s = jnp.where(valid, s, MASKED)
        top = jnp.max(s, axis=1, keepdims=True)
        p = jnp.exp(s - top).astype(bf16)
        acc = jnp.dot(p, ones_s[b * REACH : (b + 3) * REACH, :], preferred_element_type=f32)
        acc = jnp.where(lanes_of(acc.shape) == 0, top, acc)
        win_ref[:, b * REACH : (b + 1) * REACH, :] = acc.reshape(heads, REACH, LANES)


def attend_kernel(q_ref, win_ref, ctx_ref, sink_ref, bias_ref, out_ref, ones_s, done):
    heads, n, _ = q_ref.shape
    kv = ctx_ref[...]
    ones_s[...] = with_ones(kv)
    step = REACH
    lane = lanes_of((step, LANES))
    for b in range(n // step):
        at = slice(b * step, (b + 1) * step)
        pieces = []
        for h in range(heads):
            bias, sink = bias_ref[h], sink_ref[h]
            s = dot_nt(q_ref[h, at, :], kv)
            win = win_ref[h, at, :]
            win_top = win[:, 0:1]
            top = jnp.maximum(
                jnp.maximum(jnp.max(s, axis=1, keepdims=True) + bias, win_top), sink
            )
            p = jnp.exp(s - (top - bias)).astype(bf16)
            acc = jnp.dot(p, ones_s[...], preferred_element_type=f32)
            acc = acc + win * jnp.exp(win_top - top)
            den = acc[:, 1:2] + jnp.exp(sink - top)
            acc = acc / den
            pieces.append(acc)
        for pair in range(heads // 2):
            even = pltpu.roll(pieces[2 * pair], HEAD, 1)
            both = jnp.where(lane < HEAD, even, pieces[2 * pair + 1])
            done[at, pair * LANES : (pair + 1) * LANES] = both.astype(bf16)
    out_ref[...] = jnp.broadcast_to(done[...][None], out_ref.shape)


def out_kernel(att_ref, w_ref, x_ref, rows_ref, out_ref):
    sources, n, width = att_ref.shape
    t = lax.axis_index("tp")
    mixed = jnp.dot(att_ref[0], w_ref[0:width, :], preferred_element_type=f32)
    for k in range(1, sources):
        mixed = mixed + jnp.dot(
            att_ref[k], w_ref[k * width : (k + 1) * width, :], preferred_element_type=f32
        )
    low = lanes_of((1, LANES)) < 64
    for m in range(out_ref.shape[1] // LANES):
        cols = slice(m * LANES, (m + 1) * LANES)
        a = rows_ref[t * 8 + 2 * m, 2:3, :]
        b = rows_ref[t * 8 + 2 * m + 1, 2:3, :]
        gate = jnp.where(low, a, pltpu.roll(b, 64, 1))
        out_ref[:, cols] = x_ref[:, cols].astype(f32) + gate * mixed[:, cols]


def rotary_tables(rows, start):
    lane = np.arange(LANES)
    freq = ROTARY_BASE ** (-np.arange(0, 32, 2, dtype=np.float32) / 32)
    freq = jnp.asarray(freq[lane % 16].astype(np.float32))
    by_row = jnp.asarray(lane % 64 < 32)
    sign = jnp.asarray(np.where(lane % 32 < 16, -1.0, 1.0).astype(np.float32))
    position = start + jnp.arange(rows, dtype=jnp.int32)
    row, col = position // GRID_W, position % GRID_W
    place = jnp.where(by_row[None, :], row[:, None], col[:, None]).astype(f32)
    angle = place * freq[None, :]
    return jnp.cos(angle), jnp.sin(angle) * sign[None, :]


def per_device(
    latent, conditioning, context_cond, modulation, context, query_weight, key_projection,
    value_projection, out_weight, sink_head_logit, prefix_logit_bias,
):
    sp, tp = lax.axis_size("sp"), lax.axis_size("tp")
    spread = tp * lax.axis_size("dp")
    x, ctx = latent[0], context[0]
    n = x.shape[0]
    partial = call(
        partial_kernel,
        jax.ShapeDtypeStruct((sp, 16, LANES), f32),
        [VMEM] * 3,
        [pltpu.VMEM((16, LANES), f32), pltpu.VMEM((16, LANES), f32)],
    )(conditioning, context_cond[None, :], modulation)
    with jax.named_scope("sums"):
        partials = lax.all_to_all(partial, "sp", 0, 0, tiled=True)
    up = [(i, i + 1) for i in range(sp - 1)]
    down = [(i + 1, i) for i in range(sp - 1)]
    with jax.named_scope("halo"):
        before = lax.ppermute(x[n - REACH :], "sp", up)
        after = lax.ppermute(x[:REACH], "sp", down)
    mean, rstd = stats(x)
    cmean, crstd = stats(ctx)
    wkv = jnp.concatenate([key_projection, value_projection], axis=1)
    start = lax.axis_index("sp") * n - REACH
    cos, sin = rotary_tables(n + 2 * REACH, start)
    send = call(
        rows_kernel,
        jax.ShapeDtypeStruct((spread, 4, LANES), f32),
        [VMEM],
        [pltpu.VMEM((16, LANES), f32)],
    )(partials)
    with jax.named_scope("spread"):
        rows = lax.all_to_all(send, ("tp", "dp"), 0, 0, tiled=True)
    hmean, hrstd = stats(jnp.concatenate([before, after], axis=0))
    ctx_kv = call(
        ctx_kernel,
        jax.ShapeDtypeStruct((sp, ctx.shape[0], LANES), bf16),
        [VMEM] * 5,
        [pltpu.VMEM(ctx.shape, bf16)],
    )(ctx, cmean, crstd, rows, wkv)
    with jax.named_scope("context"):
        ctx_all = lax.all_to_all(ctx_kv, "sp", 0, 0, tiled=True).reshape(-1, LANES)
    heads = query_weight.shape[1] // HEAD
    total = n + 2 * REACH
    q, win = call(
        latent_kernel,
        (
            jax.ShapeDtypeStruct((heads, n, LANES), bf16),
            jax.ShapeDtypeStruct((heads, n, LANES), f32),
        ),
        [VMEM] * 12,
        [
            pltpu.VMEM((total, x.shape[1]), bf16),
            pltpu.VMEM((total, LANES), bf16),
            pltpu.VMEM((total, LANES), bf16),
        ],
    )(x, before, after, mean, rstd, hmean, hrstd, rows, query_weight, wkv, cos, sin)
    attended = call(
        attend_kernel,
        jax.ShapeDtypeStruct((tp, n, heads * HEAD), bf16),
        [VMEM] * 3 + [SMEM] * 2,
        [pltpu.VMEM(ctx_all.shape, bf16), pltpu.VMEM((n, heads * HEAD), bf16)],
    )(q, win, ctx_all, sink_head_logit, prefix_logit_bias)
    with jax.named_scope("heads"):
        every = lax.all_to_all(attended, "tp", 0, 0, tiled=True)
    cols = out_weight.shape[1]
    own = lax.dynamic_slice_in_dim(x, lax.axis_index("tp") * cols, cols, 1)
    out = call(out_kernel, jax.ShapeDtypeStruct((n, cols), f32), [VMEM] * 4)(
        every, out_weight, own, rows
    )
    return out[None]


def solution(mesh):
    placed = (
        P("dp", "sp", None),
        P(None, "sp"),
        P("sp"),
        P(None, "sp", ("tp", "dp")),
        P("dp", "sp", None),
        P(None, "tp"),
        P(None, "tp"),
        P(None, "tp"),
        P(None, "tp"),
        P("tp"),
        P("tp"),
    )
    return jax.shard_map(
        per_device, mesh=mesh, in_specs=placed, out_specs=P("dp", "sp", "tp"), check_vma=False
    )
```

time: 113 us -> 122 us (1.080)
  the two profiles are of different devices: /device:TPU:32 before, /device:TPU:96 now
where the time goes in v1:
time: 122 us; the launch traced here: 121 us
  waiting for transfers between devices  38.5 us (32%)
  starting transfers between devices  37.2 us (30%)
  Pallas kernels  32 us (26%)
  local copies, waits for them, and re-layouts  7.86 us (6%)
  other arithmetic  5.43 us (4%)
    all_to_all x1, starting transfers between devices, per_device(): partials = lax.all_to_all(partial, 'sp', 0, 0, tiled=True)  14.3 us
    all_to_all x1, waiting for transfers between devices, per_device(): partials = lax.all_to_all(partial, 'sp', 0, 0, tiled=True)  11.5 us
    all_to_all x1, waiting for transfers between devices, per_device(): every = lax.all_to_all(attended, 'tp', 0, 0, tiled=True)  10.2 us
    ppermute x1, waiting for transfers between devices, per_device(): before = lax.ppermute(x[n - REACH:], 'sp', up)  9.94 us
    pallas_call x3, Pallas kernels, stats(): return call(stats_kernel, (shape, shape), [VMEM])(x)  8.3 us
    pallas_call x1, Pallas kernels, per_device(): call(attend_kernel, jax.ShapeDtypeStruct((tp, n, heads * HEAD), bf16), [V...  7.71 us
    all_to_all x1, starting transfers between devices, per_device(): rows = lax.all_to_all(send, ('tp', 'dp'), 0, 0, tiled=True)  7.32 us
    pallas_call x1, Pallas kernels, per_device(): call(latent_kernel, (jax.ShapeDtypeStruct((heads, n, LANES), bf16), jax.S...  7.3 us
  transfers between devices with their start and end apart: 6, of which 5 were waited for; matrix products, arithmetic and copies ran while one was open for 7% of the time, Pallas kernels for 13%

profile of v1, /device:TPU:96, one launch (start us, length us, event | category | flops | bytes accessed | tf_op | source)
XLA Modules:
  0.0 121.1 jit_solution(8952286676385275537)
XLA Ops:
  0.0 1.6 %copy.15.mod_ref = bf16[3,128,64]{2,1,0:T(8,128)(2,1)} copy(bf16[3,128,64]{1,2,0:T(8,128)(2,1)} %param.17) | data formatting | bytes 98304 | tf_op args[3]
  1.6 1.8 %shard_map.138 = f32[16,16,128]{2,1,0:T(8,128)} custom-call(bf16[8,128]{1,0:T(8,128)(2,1)} %cond_ref.1, bf16[1,128]{1,0:T(2,128)(2,1)} %bitcast.16, bf16[3,128,64]{2,1,0:T(8,128)(2,1)} %copy.15.mod_ref), custom_call_target="tpu_custom_call" | custom-call | tf_op jit(solution)/shard_map/pallas_call | solution.py:246
  3.4 14.3 %all-to-all-start = ((f32[16,16,128]{2,1,0:T(8,128)}), f32[16,16,128]{2,1,0:T(8,128)S(1)}, u32[]{:S(2)}, u32[]{:S(2)}) async-start(f32[16,16,128]{2,1,0:T(8,128)} %shard_map.138), calls=%async_computation | async-start | bytes 262144 | tf_op jit(solution)/shard_map/sums/all_to_all | solution.py:253
  17.7 1.2 %copy.16 = bf16[2048,64]{1,0:T(8,128)(2,1)S(1)} copy(bf16[2048,64]{0,1:T(8,128)(2,1)} %param.20) | data formatting | bytes 524288 | tf_op args[6]
  18.9 0.3 copy.17
  19.2 11.5 %all-to-all-done.in_ref = f32[16,16,128]{2,1,0:T(8,128)S(1)} async-done(((f32[16,16,128]{2,1,0:T(8,128)}), f32[16,16,128]{2,1,0:T(8,128)S(1)}, u32[]{:S(2)}, u32[]{:S(2)}) %all-to-all-start) | async-done | bytes 131104 | tf_op jit(solution)/shard_map/sums/all_to_all | solution.py:253
  30.7 0.7 copy-done.6
  31.4 1.6 %shard_map.139 = f32[32,4,128]{2,1,0:T(4,128)} custom-call(f32[16,16,128]{2,1,0:T(8,128)} %copy-done.6), custom_call_target="tpu_custom_call" | custom-call | tf_op jit(solution)/shard_map/pallas_call | solution.py:264
  33.0 7.3 %all-to-all-start.1 = ((f32[32,4,128]{2,1,0:T(4,128)}), f32[32,4,128]{2,1,0:T(4,128)S(1)}, u32[]{:S(2)}, u32[]{:S(2)}) async-start(f32[32,4,128]{2,1,0:T(4,128)} %shard_map.139), calls=%async_computation.1 | async-start | bytes 131072 | tf_op jit(solution)/shard_map/spread/all_to_all | solution.py:271
  40.3 1.1 pad_maximum_fusion.1.wkv_ref
  41.4 1.8 %shard_map.141 = (f32[64,128]{1,0:T(8,128)}, f32[64,128]{1,0:T(8,128)}) custom-call(bf16[64,2048]{1,0:T(8,128)(2,1)} %bitcast.13), custom_call_target="tpu_custom_call" | custom-call | tf_op jit(solution)/shard_map/pallas_call | solution.py:91
  43.2 4.6 %all-to-all-done.1.rows_ref = f32[32,4,128]{2,1,0:T(4,128)S(1)} async-done(((f32[32,4,128]{2,1,0:T(4,128)}), f32[32,4,128]{2,1,0:T(4,128)S(1)}, u32[]{:S(2)}, u32[]{:S(2)}) %all-to-all-start.1) | async-done | bytes 65568 | tf_op jit(solution)/shard_map/spread/all_to_all | solution.py:271
  47.8 0.6 copy-done.4
  48.4 2.2 %shard_map.142 = bf16[16,64,128]{2,1,0:T(8,128)(2,1)} custom-call(bf16[64,2048]{1,0:T(8,128)(2,1)} %bitcast.14, f32[64,128]{1,0:T(8,128)} %get-tuple-element.19.mean_ref, f32[64,128]{1,0:T(8,128)} %get-tuple-element.20.rstd_ref, f32[32,4,128]{2,1,0:T(4,128)} %copy-done.4, bf16[2048,128]{1,0:T(8,128)(2,1)} %pad_maximum_fusion.1.wkv_ref), custom_call_target="tpu_custom_call" | custom-call | tf_op jit(solution)/shard_map/pallas_call | solution.py:273
  50.6 5.5 %all-to-all-start.2 = ((bf16[16,64,128]{2,1,0:T(8,128)(2,1)}), bf16[16,64,128]{2,1,0:T(8,128)(2,1)S(1)}, u32[]{:S(2)}, u32[]{:S(2)}) async-start(bf16[16,64,128]{2,1,0:T(8,128)(2,1)} %shard_map.142), calls=%async_computation.2 | async-start | bytes 524288 | tf_op jit(solution)/shard_map/context/all_to_all | solution.py:280
  56.2 0.1 slice_bitcast_fusion
  56.3 4.6 %collective-permute-start = (bf16[128,2048]{1,0:T(8,128)(2,1)S(1)}, bf16[128,2048]{1,0:T(8,128)(2,1)S(1)}, u32[]{:S(2)}, u32[]{:S(2)}) collective-permute-start(bf16[128,2048]{1,0:T(8,128)(2,1)S(1)} %get-tuple-element.22), channel_id=1, source_target_pairs={{0,32},{32,64},{64,96},{96,128},{128,160},{160,192},{192,224},{224... | collective-permute-start | bytes 1572872 | tf_op jit(solution)/shard_map/halo/ppermute | solution.py:257
  60.9 1.9 %collective-permute-start.1 = (bf16[128,2048]{1,0:T(8,128)(2,1)S(1)}, bf16[128,2048]{1,0:T(8,128)(2,1)S(1)}, u32[]{:S(2)}, u32[]{:S(2)}) collective-permute-start(bf16[128,2048]{1,0:T(8,128)(2,1)S(1)} %get-tuple-element.21), channel_id=1, source_target_pairs={{32,0},{64,32},{96,64},{128,96},{160,128},{192,160},{224,192},{256... | collective-permute-start | bytes 1572872 | tf_op jit(solution)/shard_map/halo/ppermute | solution.py:258
  62.8 3.6 %shard_map.136 = (f32[384,128]{1,0:T(8,128)}, f32[384,128]{1,0:T(8,128)}) custom-call(bf16[384,2048]{1,0:T(8,128)(2,1)} %bitcast.11), custom_call_target="tpu_custom_call" | custom-call | tf_op jit(solution)/shard_map/pallas_call | solution.py:91
  66.5 3.1 %sine_multiply_fusion = (f32[640,128]{1,0:T(8,128)}, f32[640,128]{1,0:T(8,128)}) fusion(f32[128]{0:T(128)S(1)} %copy-done.10, f32[128]{0:T(128)S(1)} %copy-done.8, s32[640]{0:T(1024)S(1)} %get-tuple-element.25, s32[640]{0:T(1024)S(1)} %get-tuple-element.26, pred[128]{0:T(512)(128)(4,1)S(1)} %copy-done.9), kind=kLoop, calls=%fused_computation.5 | loop fusion | flops 327680 | bytes 661632 | tf_op jit(solution)/shard_map/mul | solution.py:235
  69.6 9.9 %collective-permute-done.xb_ref = bf16[128,2048]{1,0:T(8,128)(2,1)S(1)} collective-permute-done((bf16[128,2048]{1,0:T(8,128)(2,1)S(1)}, bf16[128,2048]{1,0:T(8,128)(2,1)S(1)}, u32[]{:S(2)}, u32[]{:S(2)}) %collective-permute-start) | collective-permute-done | bytes 524320 | tf_op jit(solution)/shard_map/halo/ppermute | solution.py:257
  79.6 2.3 %collective-permute-done.1.xa_ref = bf16[128,2048]{1,0:T(8,128)(2,1)S(1)} collective-permute-done((bf16[128,2048]{1,0:T(8,128)(2,1)S(1)}, bf16[128,2048]{1,0:T(8,128)(2,1)S(1)}, u32[]{:S(2)}, u32[]{:S(2)}) %collective-permute-start.1) | collective-permute-done | bytes 524320 | tf_op jit(solution)/shard_map/halo/ppermute | solution.py:258
  81.9 1.2 pad_maximum_fusion.x_ref
  83.1 2.9 %shard_map.137 = (f32[256,128]{1,0:T(8,128)}, f32[256,128]{1,0:T(8,128)}) custom-call(bf16[256,2048]{1,0:T(8,128)(2,1)} %pad_maximum_fusion.x_ref), custom_call_target="tpu_custom_call" | custom-call | tf_op jit(solution)/shard_map/pallas_call | solution.py:91
  86.0 7.3 %shard_map.140 = (bf16[4,384,128]{2,1,0:T(8,128)(2,1)}, f32[4,384,128]{2,1,0:T(8,128)}) custom-call(bf16[384,2048]{1,0:T(8,128)(2,1)} %bitcast.12, bf16[128,2048]{1,0:T(8,128)(2,1)} %copy-done.2, bf16[128,2048]{1,0:T(8,128)(2,1)} %copy-done.3, f32[384,128]{1,0:T(8,128)} %get-tuple-element.13.mean_ref, f32[384,128]{1,0:T(8,128)} %get-tuple-element.14.rstd_ref, ...), custom_call_target="tpu_custom_call" | custom-call | tf_op jit(solution)/shard_map/pallas_call | solution.py:283
  93.3 0.7 copy-done.5
  94.0 7.7 %shard_map.143 = bf16[4,384,256]{2,1,0:T(8,128)(2,1)} custom-call(bf16[4,384,128]{2,1,0:T(8,128)(2,1)} %get-tuple-element.17.q_ref, f32[4,384,128]{2,1,0:T(8,128)} %get-tuple-element.18.win_ref, bf16[1024,128]{1,0:T(8,128)(2,1)} %bitcast.15, f32[4]{0:T(128)} %sink_ref.1, f32[4]{0:T(128)} %bias_ref.1), custom_call_target="tpu_custom_call" | custom-call | tf_op jit(solution)/shard_map/pallas_call | solution.py:296
  101.7 3.5 %all-to-all-start.3 = ((bf16[4,384,256]{2,1,0:T(8,128)(2,1)}), bf16[4,384,256]{2,1,0:T(8,128)(2,1)S(1)}, u32[]{:S(2)}, u32[]{:S(2)}) async-start(bf16[4,384,256]{2,1,0:T(8,128)(2,1)} %shard_map.143), calls=%async_computation.3 | async-start | bytes 1572864 | tf_op jit(solution)/shard_map/heads/all_to_all | solution.py:303
  105.2 1.8 %dynamic-slice_bitcast_fusion.x_ref = bf16[384,512]{1,0:T(8,128)(2,1)} fusion(bf16[1,384,2048]{2,1,0:T(8,128)(2,1)} %param.14, s32[]{:T(128)S(6)} %select_n.30), kind=kLoop, calls=%fused_computation.4 | loop fusion | bytes 786436 | tf_op jit(solution)/shard_map/dynamic_slice | solution.py:305
  107.0 10.2 %all-to-all-done.3.att_ref = bf16[4,384,256]{2,1,0:T(8,128)(2,1)S(1)} async-done(((bf16[4,384,256]{2,1,0:T(8,128)(2,1)}), bf16[4,384,256]{2,1,0:T(8,128)(2,1)S(1)}, u32[]{:S(2)}, u32[]{:S(2)}) %all-to-all-start.3) | async-done | bytes 786464 | tf_op jit(solution)/shard_map/heads/all_to_all | solution.py:303
  117.2 0.9 copy-done.1
  118.1 3.0 %shard_map.144 = f32[384,512]{1,0:T(8,128)} custom-call(bf16[4,384,256]{2,1,0:T(8,128)(2,1)} %copy-done.1, bf16[1024,512]{1,0:T(8,128)(2,1)} %w_ref.1, bf16[384,512]{1,0:T(8,128)(2,1)} %dynamic-slice_bitcast_fusion.x_ref, f32[32,4,128]{2,1,0:T(4,128)} %copy-done.4), custom_call_target="tpu_custom_call" | custom-call | tf_op jit(solution)/shard_map/pallas_call | solution.py:306
  (20 shorter events, 0.1 us)
Async XLA Ops:
  0.0 18.9 %copy-start.7 = (bf16[2048,64]{0,1:T(8,128)(2,1)S(1)}, bf16[2048,64]{0,1:T(8,128)(2,1)}, u32[]{:S(2)}) copy-start(bf16[2048,64]{0,1:T(8,128)(2,1)} %param.21) | copy-start | bytes 786436
  3.4 27.3 %all-to-all-start = ((f32[16,16,128]{2,1,0:T(8,128)}), f32[16,16,128]{2,1,0:T(8,128)S(1)}, u32[]{:S(2)}, u32[]{:S(2)}) async-start(f32[16,16,128]{2,1,0:T(8,128)} %shard_map.138), calls=%async_computation | async-start | bytes 262144 | tf_op jit(solution)/shard_map/sums/all_to_all | solution.py:253
  30.7 0.7 copy-start.6
  33.0 14.8 %all-to-all-start.1 = ((f32[32,4,128]{2,1,0:T(4,128)}), f32[32,4,128]{2,1,0:T(4,128)S(1)}, u32[]{:S(2)}, u32[]{:S(2)}) async-start(f32[32,4,128]{2,1,0:T(4,128)} %shard_map.139), calls=%async_computation.1 | async-start | bytes 131072 | tf_op jit(solution)/shard_map/spread/all_to_all | solution.py:271
  40.3 15.9 %copy-start = (bf16[1,384,2048]{2,1,0:T(8,128)(2,1)S(1)}, bf16[1,384,2048]{2,1,0:T(8,128)(2,1)}, u32[]{:S(2)}) copy-start(bf16[1,384,2048]{2,1,0:T(8,128)(2,1)} %param.14) | copy-start | bytes 4718596
  47.8 0.6 copy-start.4
  50.6 42.7 %all-to-all-start.2 = ((bf16[16,64,128]{2,1,0:T(8,128)(2,1)}), bf16[16,64,128]{2,1,0:T(8,128)(2,1)S(1)}, u32[]{:S(2)}, u32[]{:S(2)}) async-start(bf16[16,64,128]{2,1,0:T(8,128)(2,1)} %shard_map.142), calls=%async_computation.2 | async-start | bytes 524288 | tf_op jit(solution)/shard_map/context/all_to_all | solution.py:280
  56.2 10.3 %copy-start.8 = (f32[128]{0:T(128)S(1)}, f32[128]{0:T(128)}, u32[]{:S(2)}) copy-start(f32[128]{0:T(128)} %constant.56.clone) | copy-start | bytes 1540
  56.2 10.3 %copy-start.9 = (pred[128]{0:T(512)(128)(4,1)S(1)}, pred[128]{0:T(512)(128)(4,1)}, u32[]{:S(2)}) copy-start(pred[128]{0:T(512)(128)(4,1)} %constant.57.clone) | copy-start | bytes 388
  56.2 10.3 %copy-start.10 = (f32[128]{0:T(128)S(1)}, f32[128]{0:T(128)}, u32[]{:S(2)}) copy-start(f32[128]{0:T(128)} %constant.58.clone) | copy-start | bytes 1540
  56.3 23.3 %collective-permute-start = (bf16[128,2048]{1,0:T(8,128)(2,1)S(1)}, bf16[128,2048]{1,0:T(8,128)(2,1)S(1)}, u32[]{:S(2)}, u32[]{:S(2)}) collective-permute-start(bf16[128,2048]{1,0:T(8,128)(2,1)S(1)} %get-tuple-element.22), channel_id=1, source_target_pairs={{0,32},{32,64},{64,96},{96,128},{128,160},{160,192},{192,224},{224... | collective-permute-start | bytes 1572872 | tf_op jit(solution)/shard_map/halo/ppermute | solution.py:257
  60.9 21.0 %collective-permute-start.1 = (bf16[128,2048]{1,0:T(8,128)(2,1)S(1)}, bf16[128,2048]{1,0:T(8,128)(2,1)S(1)}, u32[]{:S(2)}, u32[]{:S(2)}) collective-permute-start(bf16[128,2048]{1,0:T(8,128)(2,1)S(1)} %get-tuple-element.21), channel_id=1, source_target_pairs={{32,0},{64,32},{96,64},{128,96},{160,128},{192,160},{224,192},{256... | collective-permute-start | bytes 1572872 | tf_op jit(solution)/shard_map/halo/ppermute | solution.py:258
  79.6 6.4 %copy-start.2 = (bf16[128,2048]{1,0:T(8,128)(2,1)}, bf16[128,2048]{1,0:T(8,128)(2,1)S(1)}, u32[]{:S(2)}) copy-start(bf16[128,2048]{1,0:T(8,128)(2,1)S(1)} %collective-permute-done.xb_ref) | copy-start | bytes 1572868
  81.9 4.1 %copy-start.3 = (bf16[128,2048]{1,0:T(8,128)(2,1)}, bf16[128,2048]{1,0:T(8,128)(2,1)S(1)}, u32[]{:S(2)}) copy-start(bf16[128,2048]{1,0:T(8,128)(2,1)S(1)} %collective-permute-done.1.xa_ref) | copy-start | bytes 1572868
  93.3 0.7 copy-start.5
  101.7 15.5 %all-to-all-start.3 = ((bf16[4,384,256]{2,1,0:T(8,128)(2,1)}), bf16[4,384,256]{2,1,0:T(8,128)(2,1)S(1)}, u32[]{:S(2)}, u32[]{:S(2)}) async-start(bf16[4,384,256]{2,1,0:T(8,128)(2,1)} %shard_map.143), calls=%async_computation.3 | async-start | bytes 1572864 | tf_op jit(solution)/shard_map/heads/all_to_all | solution.py:303
  117.2 0.9 copy-start.1

commit v2 on v1

--- a/solution.py
+++ b/solution.py
@@ -20,6 +20,7 @@
 bf16 = jnp.bfloat16
 VMEM = pl.BlockSpec(memory_space=pltpu.VMEM)
 SMEM = pl.BlockSpec(memory_space=pltpu.SMEM)
+ANY = pl.BlockSpec(memory_space=pl.ANY)
 
 
 def dot_nt(a, b):
@@ -30,13 +31,14 @@
     return lax.broadcasted_iota(jnp.int32, shape, len(shape) - 1)
 
 
-def call(kernel, out_shape, ins, scratch=()):
+def call(kernel, out_shape, ins, scratch=(), mib=8):
     return pl.pallas_call(
         kernel,
         out_shape=out_shape,
         in_specs=ins,
         out_specs=jax.tree.map(lambda _: VMEM, out_shape),
         scratch_shapes=list(scratch),
+        compiler_params=pltpu.CompilerParams(vmem_limit_bytes=mib << 20),
     )
 
 
@@ -47,15 +49,16 @@
     rows[samples : samples + 1, :] = ctx_ref[...].astype(f32)
     v = rows[...]
     act = (v / (1.0 + jnp.exp(-v))).astype(bf16)
-    shift = jnp.dot(act, mod_ref[0], preferred_element_type=f32)
-    scale = jnp.dot(act, mod_ref[1], preferred_element_type=f32)
-    gate = jnp.dot(act, mod_ref[2], preferred_element_type=f32)
+    shift = dot_nt(act, mod_ref[0])
+    scale = dot_nt(act, mod_ref[1])
+    gate = dot_nt(act, mod_ref[2])
     packed[...] = jnp.concatenate([shift, scale], axis=1)
     packed[9:13, :] = jnp.concatenate([gate[0:4], gate[4:8]], axis=1)
     out_ref[...] = jnp.broadcast_to(packed[...][None], out_ref.shape)
 
 
-def rows_kernel(in_ref, out_ref, total):
+def rows_kernel(in_ref, *refs):
+    out_ref, total = refs[-2:]
     total[...] = jnp.sum(in_ref[...], axis=0)
     copies = out_ref.shape[0] // 8
     for d in range(8):
@@ -69,7 +72,7 @@
             out_ref[t * 8 + d, 3:4, :] = gate
 
 
-def stats_kernel(x_ref, mean_ref, rstd_ref):
+def stats_of(x_ref, mean_ref, rstd_ref):
     width = x_ref.shape[1]
     step = 64
 
@@ -86,9 +89,9 @@
     lax.fori_loop(0, x_ref.shape[0] // step, body, 0)
 
 
-def stats(x):
-    shape = jax.ShapeDtypeStruct((x.shape[0], LANES), f32)
-    return call(stats_kernel, (shape, shape), [VMEM])(x)
+def stats_kernel(x_ref, c_ref, mean_ref, rstd_ref, cmean_ref, crstd_ref):
+    stats_of(x_ref, mean_ref, rstd_ref)
+    stats_of(c_ref, cmean_ref, crstd_ref)
 
 
 def mod_tile(rows_ref, row, m):
@@ -112,7 +115,7 @@
 
 def ctx_kernel(x_ref, mean_ref, rstd_ref, rows_ref, wkv_ref, out_ref, normed):
     modulate(x_ref, mean_ref, rstd_ref, rows_ref, 1, normed, 0)
-    kv = jnp.dot(normed[...], wkv_ref[...], preferred_element_type=f32).astype(bf16)
+    kv = dot_nt(normed[...], wkv_ref[...]).astype(bf16)
     out_ref[...] = jnp.broadcast_to(kv[None], out_ref.shape)
 
 
@@ -126,32 +129,32 @@
     return jnp.where(lanes_of(kv.shape) < HEAD, jnp.ones_like(kv), kv)
 
 
-def latent_kernel(
-    x_ref, xb_ref, xa_ref, mean_ref, rstd_ref, hmean_ref, hrstd_ref, rows_ref, wq_ref, wkv_ref,
-    cos_ref, sin_ref, q_ref, win_ref, normed, kv_s, ones_s,
+def project_kernel(
+    x_ref, mean_ref, rstd_ref, rows_ref, wq_ref, wkv_ref, cos_ref, sin_ref,
+    q_ref, kv_ref, head_ref, tail_ref, normed,
 ):
     n = x_ref.shape[0]
-    total = n + 2 * REACH
-    modulate(xb_ref, hmean_ref.at[0:REACH], hrstd_ref.at[0:REACH], rows_ref, 0, normed, 0)
-    modulate(x_ref, mean_ref, rstd_ref, rows_ref, 0, normed, REACH)
-    modulate(
-        xa_ref, hmean_ref.at[REACH : 2 * REACH], hrstd_ref.at[REACH : 2 * REACH], rows_ref, 0,
-        normed, REACH + n,
-    )
+    modulate(x_ref, mean_ref, rstd_ref, rows_ref, 0, normed, 0)
     cos, sin = cos_ref[...], sin_ref[...]
-    key_lane = lanes_of((total, LANES)) < HEAD
-    kv = jnp.dot(normed[...], wkv_ref[...], preferred_element_type=f32)
-    kv = turned(kv, jnp.where(key_lane, cos, 1.0), jnp.where(key_lane, sin, 0.0)).astype(bf16)
-    kv_s[...] = kv
-    ones_s[...] = with_ones(kv)
-    q = jnp.dot(normed[REACH : REACH + n, :], wq_ref[...], preferred_element_type=f32)
     low = lanes_of((n, LANES)) < HEAD
-    own_cos, own_sin = cos_ref[REACH : REACH + n, :], sin_ref[REACH : REACH + n, :]
+    kv = dot_nt(normed[...], wkv_ref[...])
+    kv = turned(kv, jnp.where(low, cos, 1.0), jnp.where(low, sin, 0.0)).astype(bf16)
+    kv_ref[...] = kv
+    head_ref[...] = kv[0:REACH]
+    tail_ref[...] = kv[n - REACH : n]
+    q = jnp.dot(normed[...], wq_ref[...], preferred_element_type=f32)
     for pair in range(q.shape[1] // LANES):
-        u = turned(q[:, pair * LANES : (pair + 1) * LANES], own_cos, own_sin) * (HEAD ** -0.5)
+        u = turned(q[:, pair * LANES : (pair + 1) * LANES], cos, sin) * (HEAD ** -0.5)
         q_ref[2 * pair] = jnp.where(low, u, 0.0).astype(bf16)
         q_ref[2 * pair + 1] = jnp.where(low, pltpu.roll(u, HEAD, 1), 0.0).astype(bf16)
-    heads = q_ref.shape[0]
+
+
+def window_kernel(q_ref, kv_ref, before_ref, after_ref, win_ref, kv_s, ones_s):
+    heads, n, _ = q_ref.shape
+    kv_s[0:REACH, :] = before_ref[...]
+    kv_s[REACH : REACH + n, :] = kv_ref[...]
+    kv_s[REACH + n :, :] = after_ref[...]
+    ones_s[...] = with_ones(kv_s[...])
     rows = heads * REACH
     blocks = n // REACH
     i = lax.broadcasted_iota(jnp.int32, (rows, 3 * REACH), 0) % REACH
@@ -180,27 +183,27 @@
     kv = ctx_ref[...]
     ones_s[...] = with_ones(kv)
     step = REACH
+    rows = heads * step
     lane = lanes_of((step, LANES))
+    head = lax.broadcasted_iota(jnp.int32, (rows, 1), 0) // step
+    bias, sink = jnp.zeros((rows, 1), f32), jnp.zeros((rows, 1), f32)
+    for h in range(heads):
+        bias = jnp.where(head == h, bias_ref[h], bias)
+        sink = jnp.where(head == h, sink_ref[h], sink)
     for b in range(n // step):
         at = slice(b * step, (b + 1) * step)
-        pieces = []
-        for h in range(heads):
-            bias, sink = bias_ref[h], sink_ref[h]
-            s = dot_nt(q_ref[h, at, :], kv)
-            win = win_ref[h, at, :]
-            win_top = win[:, 0:1]
-            top = jnp.maximum(
-                jnp.maximum(jnp.max(s, axis=1, keepdims=True) + bias, win_top), sink
-            )
-            p = jnp.exp(s - (top - bias)).astype(bf16)
-            acc = jnp.dot(p, ones_s[...], preferred_element_type=f32)
-            acc = acc + win * jnp.exp(win_top - top)
-            den = acc[:, 1:2] + jnp.exp(sink - top)
-            acc = acc / den
-            pieces.append(acc)
+        s = dot_nt(q_ref[:, at, :].reshape(rows, LANES), kv)
+        win = win_ref[:, at, :].reshape(rows, LANES)
+        win_top = win[:, 0:1]
+        top = jnp.maximum(jnp.max(s, axis=1, keepdims=True) + bias, jnp.maximum(win_top, sink))
+        p = jnp.exp(s - (top - bias)).astype(bf16)
+        acc = jnp.dot(p, ones_s[...], preferred_element_type=f32)
+        acc = acc + win * jnp.exp(win_top - top)
+        den = acc[:, 1:2] + jnp.exp(sink - top)
+        acc = (acc / den).reshape(heads, step, LANES)
         for pair in range(heads // 2):
-            even = pltpu.roll(pieces[2 * pair], HEAD, 1)
-            both = jnp.where(lane < HEAD, even, pieces[2 * pair + 1])
+            even = pltpu.roll(acc[2 * pair], HEAD, 1)
+            both = jnp.where(lane < HEAD, even, acc[2 * pair + 1])
             done[at, pair * LANES : (pair + 1) * LANES] = both.astype(bf16)
     out_ref[...] = jnp.broadcast_to(done[...][None], out_ref.shape)
 
@@ -248,62 +251,74 @@
         jax.ShapeDtypeStruct((sp, 16, LANES), f32),
         [VMEM] * 3,
         [pltpu.VMEM((16, LANES), f32), pltpu.VMEM((16, LANES), f32)],
-    )(conditioning, context_cond[None, :], modulation)
+        2,
+    )(conditioning, context_cond[None, :], modulation.transpose(0, 2, 1))
     with jax.named_scope("sums"):
         partials = lax.all_to_all(partial, "sp", 0, 0, tiled=True)
-    up = [(i, i + 1) for i in range(sp - 1)]
-    down = [(i + 1, i) for i in range(sp - 1)]
-    with jax.named_scope("halo"):
-        before = lax.ppermute(x[n - REACH :], "sp", up)
-        after = lax.ppermute(x[:REACH], "sp", down)
-    mean, rstd = stats(x)
-    cmean, crstd = stats(ctx)
-    wkv = jnp.concatenate([key_projection, value_projection], axis=1)
-    start = lax.axis_index("sp") * n - REACH
-    cos, sin = rotary_tables(n + 2 * REACH, start)
+    flat = jax.ShapeDtypeStruct((n, LANES), f32)
+    cflat = jax.ShapeDtypeStruct((ctx.shape[0], LANES), f32)
+    mean, rstd, cmean, crstd = call(stats_kernel, (flat, flat, cflat, cflat), [VMEM] * 2, (), 8)(
+        x, ctx
+    )
+    wkv = jnp.concatenate([key_projection.T, value_projection.T], axis=0)
+    cos, sin = rotary_tables(n, lax.axis_index("sp") * n)
     send = call(
         rows_kernel,
         jax.ShapeDtypeStruct((spread, 4, LANES), f32),
-        [VMEM],
+        [VMEM] + [ANY] * 4,
         [pltpu.VMEM((16, LANES), f32)],
-    )(partials)
+        2,
+    )(partials, cmean, wkv, cos, sin)
     with jax.named_scope("spread"):
         rows = lax.all_to_all(send, ("tp", "dp"), 0, 0, tiled=True)
-    hmean, hrstd = stats(jnp.concatenate([before, after], axis=0))
     ctx_kv = call(
         ctx_kernel,
         jax.ShapeDtypeStruct((sp, ctx.shape[0], LANES), bf16),
         [VMEM] * 5,
         [pltpu.VMEM(ctx.shape, bf16)],
+        4,
     )(ctx, cmean, crstd, rows, wkv)
     with jax.named_scope("context"):
         ctx_all = lax.all_to_all(ctx_kv, "sp", 0, 0, tiled=True).reshape(-1, LANES)
     heads = query_weight.shape[1] // HEAD
-    total = n + 2 * REACH
-    q, win = call(
-        latent_kernel,
+    edge = jax.ShapeDtypeStruct((REACH, LANES), bf16)
+    q, kv, first, last = call(
+        project_kernel,
         (
             jax.ShapeDtypeStruct((heads, n, LANES), bf16),
-            jax.ShapeDtypeStruct((heads, n, LANES), f32),
+            jax.ShapeDtypeStruct((n, LANES), bf16),
+            edge,
+            edge,
         ),
-        [VMEM] * 12,
-        [
-            pltpu.VMEM((total, x.shape[1]), bf16),
-            pltpu.VMEM((total, LANES), bf16),
-            pltpu.VMEM((total, LANES), bf16),
-        ],
-    )(x, before, after, mean, rstd, hmean, hrstd, rows, query_weight, wkv, cos, sin)
+        [VMEM] * 8,
+        [pltpu.VMEM(x.shape, bf16)],
+        12,
+    )(x, mean, rstd, rows, query_weight, wkv, cos, sin)
+    up = [(i, i + 1) for i in range(sp - 1)]
+    down = [(i + 1, i) for i in range(sp - 1)]
+    with jax.named_scope("halo"):
+        before = lax.ppermute(last, "sp", up)
+        after = lax.ppermute(first, "sp", down)
+    wide = pltpu.VMEM((n + 2 * REACH, LANES), bf16)
+    win = call(
+        window_kernel,
+        jax.ShapeDtypeStruct((heads, n, LANES), f32),
+        [VMEM] * 4,
+        [wide, wide],
+        12,
+    )(q, kv, before, after)
     attended = call(
         attend_kernel,
         jax.ShapeDtypeStruct((tp, n, heads * HEAD), bf16),
         [VMEM] * 3 + [SMEM] * 2,
         [pltpu.VMEM(ctx_all.shape, bf16), pltpu.VMEM((n, heads * HEAD), bf16)],
+        16,
     )(q, win, ctx_all, sink_head_logit, prefix_logit_bias)
     with jax.named_scope("heads"):
         every = lax.all_to_all(attended, "tp", 0, 0, tiled=True)
     cols = out_weight.shape[1]
     own = lax.dynamic_slice_in_dim(x, lax.axis_index("tp") * cols, cols, 1)
-    out = call(out_kernel, jax.ShapeDtypeStruct((n, cols), f32), [VMEM] * 4)(
+    out = call(out_kernel, jax.ShapeDtypeStruct((n, cols), f32), [VMEM] * 4, (), 8)(
         every, out_weight, own, rows
     )
     return out[None]

time: 122 us -> 94.2 us (0.77)
  the two profiles are of different devices: /device:TPU:96 before, /device:TPU:32 now
where the time goes in v2:
time: 94.2 us; the launch traced here: 93.5 us
  starting transfers between devices  28.9 us (31%)
  waiting for transfers between devices  28.7 us (30%)
  blocking collectives  14.6 us (15%)
  Pallas kernels  12.5 us (13%)
  local copies, waits for them, and re-layouts  7.96 us (8%)
    all_to_all x1, starting transfers between devices, per_device(): partials = lax.all_to_all(partial, 'sp', 0, 0, tiled=True)  15.2 us
    all_to_all x1, blocking collectives, per_device(): rows = lax.all_to_all(send, ('tp', 'dp'), 0, 0, tiled=True)  14.6 us
    all_to_all x1, waiting for transfers between devices, per_device(): every = lax.all_to_all(attended, 'tp', 0, 0, tiled=True)  11.8 us
    all_to_all x1, waiting for transfers between devices, per_device(): partials = lax.all_to_all(partial, 'sp', 0, 0, tiled=True)  9.18 us
    unnamed x36, local copies, waits for them, and re-layouts  7.93 us
    pallas_call x1, Pallas kernels, per_device(): call(attend_kernel, jax.ShapeDtypeStruct((tp, n, heads * HEAD), bf16), [V...  4.47 us
    all_to_all x1, starting transfers between devices, per_device(): ctx_all = lax.all_to_all(ctx_kv, 'sp', 0, 0, tiled=True).reshape(-1, LANES)  4.31 us
    all_to_all x1, waiting for transfers between devices, per_device(): ctx_all = lax.all_to_all(ctx_kv, 'sp', 0, 0, tiled=True).reshape(-1, LANES)  4.24 us
  transfers between devices with their start and end apart: 5, of which 5 were waited for; matrix products, arithmetic and copies ran while one was open for 1% of the time, Pallas kernels for 5%

profile of v2, /device:TPU:32, one launch (start us, length us, event | category | flops | bytes accessed | tf_op | source)
XLA Modules:
  0.0 93.5 jit_solution(5813723328479020316)
XLA Ops:
  0.0 0.8 copy-done.8
  0.8 0.7 copy-done.9
  1.5 0.7 copy-done.10
  2.2 0.9 shard_map.137
  3.1 15.2 %all-to-all-start = ((f32[16,16,128]{2,1,0:T(8,128)}), f32[16,16,128]{2,1,0:T(8,128)S(1)}, u32[]{:S(2)}, u32[]{:S(2)}) async-start(f32[16,16,128]{2,1,0:T(8,128)} %shard_map.137), calls=%async_computation | async-start | bytes 262144 | tf_op jit(solution)/shard_map/sums/all_to_all | solution.py:257
  18.3 0.0 copy-start
  18.3 1.4 %copy-done = bf16[1,384,2048]{2,1,0:T(8,128)(2,1)S(1)} copy-done((bf16[1,384,2048]{2,1,0:T(8,128)(2,1)S(1)}, bf16[1,384,2048]{2,1,0:T(8,128)(2,1)}, u32[]{:S(2)}) %copy-start) | copy-done | bytes 1572888
  19.7 0.9 %copy-done.3 = bf16[1,64,2048]{2,1,0:T(8,128)(2,1)S(1)} copy-done((bf16[1,64,2048]{2,1,0:T(8,128)(2,1)S(1)}, bf16[1,64,2048]{2,1,0:T(8,128)(2,1)}, u32[]{:S(2)}) %copy-start.3) | copy-done | bytes 262168
  20.7 1.7 %shard_map.136 = (f32[384,128]{1,0:T(8,128)S(1)}, f32[384,128]{1,0:T(8,128)S(1)}, f32[64,128]{1,0:T(8,128)S(1)}, f32[64,128]{1,0:T(8,128)S(1)}) custom-call(bf16[384,2048]{1,0:T(8,128)(2,1)S(1)} %bitcast.10, bf16[64,2048]{1,0:T(8,128)(2,1)S(1)} %bitcast.12), custom_call_target="tpu_custom_call" | custom-call | tf_op jit(solution)/shard_map/pallas_call | solution.py:260
  22.4 0.0 copy-start.4
  22.5 0.8 sine_multiply_fusion
  23.3 0.0 copy-start.1
  23.3 9.2 %all-to-all-done.in_ref = f32[16,16,128]{2,1,0:T(8,128)S(1)} async-done(((f32[16,16,128]{2,1,0:T(8,128)}), f32[16,16,128]{2,1,0:T(8,128)S(1)}, u32[]{:S(2)}, u32[]{:S(2)}) %all-to-all-start) | async-done | bytes 131104 | tf_op jit(solution)/shard_map/sums/all_to_all | solution.py:257
  32.5 0.1 shard_map.138
  32.6 14.6 %all_to_all.20.rows_ref = f32[32,4,128]{2,1,0:T(4,128)S(1)} all-to-all(f32[32,4,128]{2,1,0:T(4,128)S(1)} %shard_map.138), channel_id=1, replica_groups=mesh['sp'=16,'tp'=4,'dp'=8] {'tp','dp'}, dimensions={0} | all-to-all | bytes 131072 | tf_op jit(solution)/shard_map/spread/all_to_all | solution.py:273
  47.2 1.1 %shard_map.141 = bf16[16,64,128]{2,1,0:T(8,128)(2,1)} custom-call(bf16[64,2048]{1,0:T(8,128)(2,1)S(1)} %bitcast.13, f32[64,128]{1,0:T(8,128)S(1)} %get-tuple-element.15.refs_0_.mean_ref, f32[64,128]{1,0:T(8,128)S(1)} %get-tuple-element.20.rstd_ref, f32[32,4,128]{2,1,0:T(4,128)S(1)} %all_to_all.20.rows_ref, bf16[128,2048]{1,0:T(8,128)(2,1)S(1)} %pad_maximum_fusion.refs_1_.wkv_ref), custom_call_target="tpu_custom_call" | custom-call | tf_op jit(solution)/shard_map/pallas_call | solution.py:274
  48.3 4.3 %all-to-all-start.2 = ((bf16[16,64,128]{2,1,0:T(8,128)(2,1)}), bf16[16,64,128]{2,1,0:T(8,128)(2,1)S(1)}, u32[]{:S(2)}, u32[]{:S(2)}) async-start(bf16[16,64,128]{2,1,0:T(8,128)(2,1)} %shard_map.141), calls=%async_computation.2 | async-start | bytes 524288 | tf_op jit(solution)/shard_map/context/all_to_all | solution.py:282
  52.6 0.0 copy-start.5
  52.6 1.2 %copy-done.5 = bf16[2048,256]{1,0:T(8,128)(2,1)S(1)} copy-done((bf16[2048,256]{1,0:T(8,128)(2,1)S(1)}, bf16[2048,256]{1,0:T(8,128)(2,1)}, u32[]{:S(2)}) %copy-start.5) | copy-done | bytes 1048600
  53.9 0.9 copy-done.7
  54.8 1.4 %shard_map.139 = (bf16[4,384,128]{2,1,0:T(8,128)(2,1)S(1)}, bf16[384,128]{1,0:T(8,128)(2,1)S(1)}, bf16[128,128]{1,0:T(8,128)(2,1)S(1)}, bf16[128,128]{1,0:T(8,128)(2,1)S(1)}) custom-call(bf16[384,2048]{1,0:T(8,128)(2,1)S(1)} %bitcast.11, f32[384,128]{1,0:T(8,128)S(1)} %get-tuple-element.13.mean_ref, f32[384,128]{1,0:T(8,128)S(1)} %copy-done.7, ...), custom_call_target="tpu_custom_call" | custom-call | tf_op jit(solution)/shard_map/pallas_call | solution.py:285
  56.2 3.4 %collective-permute-start = (bf16[128,128]{1,0:T(8,128)(2,1)S(1)}, bf16[128,128]{1,0:T(8,128)(2,1)S(1)}, u32[]{:S(2)}, u32[]{:S(2)}) collective-permute-start(bf16[128,128]{1,0:T(8,128)(2,1)S(1)} %get-tuple-element.18), channel_id=1, source_target_pairs={{0,32},{32,64},{64,96},{96,128},{128,160},{160,192},{192,224},{224... | collective-permute-start | bytes 98312 | tf_op jit(solution)/shard_map/halo/ppermute | solution.py:300
  59.6 2.5 %collective-permute-start.1 = (bf16[128,128]{1,0:T(8,128)(2,1)S(1)}, bf16[128,128]{1,0:T(8,128)(2,1)S(1)}, u32[]{:S(2)}, u32[]{:S(2)}) collective-permute-start(bf16[128,128]{1,0:T(8,128)(2,1)S(1)} %get-tuple-element.19), channel_id=1, source_target_pairs={{32,0},{64,32},{96,64},{128,96},{160,128},{192,160},{224,192},{256... | collective-permute-start | bytes 98312 | tf_op jit(solution)/shard_map/halo/ppermute | solution.py:301
  62.0 1.4 %collective-permute-done.before_ref = bf16[128,128]{1,0:T(8,128)(2,1)S(1)} collective-permute-done((bf16[128,128]{1,0:T(8,128)(2,1)S(1)}, bf16[128,128]{1,0:T(8,128)(2,1)S(1)}, u32[]{:S(2)}, u32[]{:S(2)}) %collective-permute-start) | collective-permute-done | bytes 32800 | tf_op jit(solution)/shard_map/halo/ppermute | solution.py:300
  63.5 2.1 %collective-permute-done.1.after_ref = bf16[128,128]{1,0:T(8,128)(2,1)S(1)} collective-permute-done((bf16[128,128]{1,0:T(8,128)(2,1)S(1)}, bf16[128,128]{1,0:T(8,128)(2,1)S(1)}, u32[]{:S(2)}, u32[]{:S(2)}) %collective-permute-start.1) | collective-permute-done | bytes 32800 | tf_op jit(solution)/shard_map/halo/ppermute | solution.py:301
  65.5 1.3 %shard_map.140.win_ref = f32[4,384,128]{2,1,0:T(8,128)S(1)} custom-call(bf16[4,384,128]{2,1,0:T(8,128)(2,1)S(1)} %get-tuple-element.16.q_ref, bf16[384,128]{1,0:T(8,128)(2,1)S(1)} %get-tuple-element.17.kv_ref, bf16[128,128]{1,0:T(8,128)(2,1)S(1)} %collective-permute-done.before_ref, bf16[128,128]{1,0:T(8,128)(2,1)S(1)} %collective-permute-done.1.after_ref), custom_call_target="tpu_custom_call" | custom-call | tf_op jit(solution)/shard_map/pallas_call | solution.py:303
  66.8 4.2 %all-to-all-done.2 = bf16[16,64,128]{2,1,0:T(8,128)(2,1)S(1)} async-done(((bf16[16,64,128]{2,1,0:T(8,128)(2,1)}), bf16[16,64,128]{2,1,0:T(8,128)(2,1)S(1)}, u32[]{:S(2)}, u32[]{:S(2)}) %all-to-all-start.2) | async-done | bytes 262176 | tf_op jit(solution)/shard_map/context/all_to_all | solution.py:282
  71.1 4.5 %shard_map.142 = bf16[4,384,256]{2,1,0:T(8,128)(2,1)} custom-call(bf16[4,384,128]{2,1,0:T(8,128)(2,1)S(1)} %get-tuple-element.16.q_ref, f32[4,384,128]{2,1,0:T(8,128)S(1)} %shard_map.140.win_ref, bf16[1024,128]{1,0:T(8,128)(2,1)S(1)} %bitcast.14, f32[4]{0:T(128)S(1)} %copy-done.11, f32[4]{0:T(128)S(1)} %copy-done.12), custom_call_target="tpu_custom_call" | custom-call | tf_op jit(solution)/shard_map/pallas_call | solution.py:310
  75.5 3.5 %all-to-all-start.3 = ((bf16[4,384,256]{2,1,0:T(8,128)(2,1)}), bf16[4,384,256]{2,1,0:T(8,128)(2,1)S(1)}, u32[]{:S(2)}, u32[]{:S(2)}) async-start(bf16[4,384,256]{2,1,0:T(8,128)(2,1)} %shard_map.142), calls=%async_computation.3 | async-start | bytes 1572864 | tf_op jit(solution)/shard_map/heads/all_to_all | solution.py:318
  79.1 11.8 %all-to-all-done.3.att_ref = bf16[4,384,256]{2,1,0:T(8,128)(2,1)S(1)} async-done(((bf16[4,384,256]{2,1,0:T(8,128)(2,1)}), bf16[4,384,256]{2,1,0:T(8,128)(2,1)S(1)}, u32[]{:S(2)}, u32[]{:S(2)}) %all-to-all-start.3) | async-done | bytes 786464 | tf_op jit(solution)/shard_map/heads/all_to_all | solution.py:318
  90.9 1.2 %copy-done.2 = bf16[1024,512]{1,0:T(8,128)(2,1)S(1)} copy-done((bf16[1024,512]{1,0:T(8,128)(2,1)S(1)}, bf16[1024,512]{1,0:T(8,128)(2,1)}, u32[]{:S(2)}) %copy-start.2) | copy-done | bytes 1048600
  92.1 1.5 %shard_map.143 = f32[384,512]{1,0:T(8,128)} custom-call(bf16[4,384,256]{2,1,0:T(8,128)(2,1)S(1)} %all-to-all-done.3.att_ref, bf16[1024,512]{1,0:T(8,128)(2,1)S(1)} %copy-done.2, bf16[384,512]{1,0:T(8,128)(2,1)S(1)} %dynamic-slice_bitcast_fusion.x_ref, f32[32,4,128]{2,1,0:T(4,128)S(1)} %all_to_all.20.rows_ref), custom_call_target="tpu_custom_call" | custom-call | tf_op jit(solution)/shard_map/pallas_call | solution.py:321
  (27 shorter events, 0.1 us)
Async XLA Ops:
  0.0 22.4 %copy-start.15 = (f32[128]{0:T(128)S(1)}, f32[128]{0:T(128)}, u32[]{:S(2)}) copy-start(f32[128]{0:T(128)} %constant.53.clone) | copy-start | bytes 1540
  0.0 22.4 %copy-start.16 = (pred[128]{0:T(512)(128)(4,1)S(1)}, pred[128]{0:T(512)(128)(4,1)}, u32[]{:S(2)}) copy-start(pred[128]{0:T(512)(128)(4,1)} %constant.54.clone) | copy-start | bytes 388
  0.0 22.4 %copy-start.17 = (f32[128]{0:T(128)S(1)}, f32[128]{0:T(128)}, u32[]{:S(2)}) copy-start(f32[128]{0:T(128)} %constant.55.clone) | copy-start | bytes 1540
  0.0 0.8 copy-start.8
  0.8 0.7 copy-start.9
  1.5 0.7 copy-start.10
  2.2 21.1 %copy-start.13 = (bf16[2048,64]{0,1:T(8,128)(2,1)S(1)}, bf16[2048,64]{0,1:T(8,128)(2,1)}, u32[]{:S(2)}) copy-start(bf16[2048,64]{0,1:T(8,128)(2,1)} %param.21) | copy-start | bytes 786436
  3.1 29.4 %all-to-all-start = ((f32[16,16,128]{2,1,0:T(8,128)}), f32[16,16,128]{2,1,0:T(8,128)S(1)}, u32[]{:S(2)}, u32[]{:S(2)}) async-start(f32[16,16,128]{2,1,0:T(8,128)} %shard_map.137), calls=%async_computation | async-start | bytes 262144 | tf_op jit(solution)/shard_map/sums/all_to_all | solution.py:257
  18.3 1.4 %copy-start = (bf16[1,384,2048]{2,1,0:T(8,128)(2,1)S(1)}, bf16[1,384,2048]{2,1,0:T(8,128)(2,1)}, u32[]{:S(2)}) copy-start(bf16[1,384,2048]{2,1,0:T(8,128)(2,1)} %param.14) | copy-start | bytes 4718596
  19.7 0.9 %copy-start.3 = (bf16[1,64,2048]{2,1,0:T(8,128)(2,1)S(1)}, bf16[1,64,2048]{2,1,0:T(8,128)(2,1)}, u32[]{:S(2)}) copy-start(bf16[1,64,2048]{2,1,0:T(8,128)(2,1)} %param.18) | copy-start | bytes 786436
  20.7 2.6 %copy-start.14 = (bf16[2048,64]{0,1:T(8,128)(2,1)S(1)}, bf16[2048,64]{0,1:T(8,128)(2,1)}, u32[]{:S(2)}) copy-start(bf16[2048,64]{0,1:T(8,128)(2,1)} %param.20) | copy-start | bytes 786436
  22.4 10.1 %copy-start.6 = (f32[384,128]{1,0:T(8,128)}, f32[384,128]{1,0:T(8,128)S(1)}, u32[]{:S(2)}) copy-start(f32[384,128]{1,0:T(8,128)S(1)} %get-tuple-element.14.rstd_ref) | copy-start | bytes 589828
  22.4 24.8 %copy-start.4 = (bf16[1,64,2048]{2,1,0:T(8,128)(2,1)S(1)}, bf16[1,64,2048]{2,1,0:T(8,128)(2,1)}, u32[]{:S(2)}) copy-start(bf16[1,64,2048]{2,1,0:T(8,128)(2,1)} %param.18) | copy-start | bytes 786436
  23.3 29.3 %copy-start.1 = (bf16[1,384,2048]{2,1,0:T(8,128)(2,1)S(1)}, bf16[1,384,2048]{2,1,0:T(8,128)(2,1)}, u32[]{:S(2)}) copy-start(bf16[1,384,2048]{2,1,0:T(8,128)(2,1)} %param.14) | copy-start | bytes 4718596
  48.3 22.8 %all-to-all-start.2 = ((bf16[16,64,128]{2,1,0:T(8,128)(2,1)}), bf16[16,64,128]{2,1,0:T(8,128)(2,1)S(1)}, u32[]{:S(2)}, u32[]{:S(2)}) async-start(bf16[16,64,128]{2,1,0:T(8,128)(2,1)} %shard_map.141), calls=%async_computation.2 | async-start | bytes 524288 | tf_op jit(solution)/shard_map/context/all_to_all | solution.py:282
  52.6 1.2 %copy-start.5 = (bf16[2048,256]{1,0:T(8,128)(2,1)S(1)}, bf16[2048,256]{1,0:T(8,128)(2,1)}, u32[]{:S(2)}) copy-start(bf16[2048,256]{1,0:T(8,128)(2,1)} %wq_ref.1) | copy-start | bytes 3145732
  53.9 0.9 copy-start.7
  54.8 16.3 %copy-start.11 = (f32[4]{0:T(128)S(1)}, f32[4]{0:T(128)}, u32[]{:S(2)}) copy-start(f32[4]{0:T(128)} %sink_ref.1) | copy-start | bytes 52
  54.8 16.3 %copy-start.12 = (f32[4]{0:T(128)S(1)}, f32[4]{0:T(128)}, u32[]{:S(2)}) copy-start(f32[4]{0:T(128)} %bias_ref.1) | copy-start | bytes 52
  56.2 7.3 %collective-permute-start = (bf16[128,128]{1,0:T(8,128)(2,1)S(1)}, bf16[128,128]{1,0:T(8,128)(2,1)S(1)}, u32[]{:S(2)}, u32[]{:S(2)}) collective-permute-start(bf16[128,128]{1,0:T(8,128)(2,1)S(1)} %get-tuple-element.18), channel_id=1, source_target_pairs={{0,32},{32,64},{64,96},{96,128},{128,160},{160,192},{192,224},{224... | collective-permute-start | bytes 98312 | tf_op jit(solution)/shard_map/halo/ppermute | solution.py:300
  59.6 5.9 %collective-permute-start.1 = (bf16[128,128]{1,0:T(8,128)(2,1)S(1)}, bf16[128,128]{1,0:T(8,128)(2,1)S(1)}, u32[]{:S(2)}, u32[]{:S(2)}) collective-permute-start(bf16[128,128]{1,0:T(8,128)(2,1)S(1)} %get-tuple-element.19), channel_id=1, source_target_pairs={{32,0},{64,32},{96,64},{128,96},{160,128},{192,160},{224,192},{256... | collective-permute-start | bytes 98312 | tf_op jit(solution)/shard_map/halo/ppermute | solution.py:301
  75.5 15.3 %all-to-all-start.3 = ((bf16[4,384,256]{2,1,0:T(8,128)(2,1)}), bf16[4,384,256]{2,1,0:T(8,128)(2,1)S(1)}, u32[]{:S(2)}, u32[]{:S(2)}) async-start(bf16[4,384,256]{2,1,0:T(8,128)(2,1)} %shard_map.142), calls=%async_computation.3 | async-start | bytes 1572864 | tf_op jit(solution)/shard_map/heads/all_to_all | solution.py:318
  90.9 1.2 %copy-start.2 = (bf16[1024,512]{1,0:T(8,128)(2,1)S(1)}, bf16[1024,512]{1,0:T(8,128)(2,1)}, u32[]{:S(2)}) copy-start(bf16[1024,512]{1,0:T(8,128)(2,1)} %w_ref.1) | copy-start | bytes 3145732

commit v3 on v2

--- a/solution.py
+++ b/solution.py
@@ -23,6 +23,10 @@
 ANY = pl.BlockSpec(memory_space=pl.ANY)
 
 
+def in_hbm(x):
+    return pltpu.with_memory_space_constraint(x, pltpu.HBM)
+
+
 def dot_nt(a, b):
     return lax.dot_general(a, b, (((1,), (1,)), ((), ())), preferred_element_type=f32)
 
@@ -31,12 +35,12 @@
     return lax.broadcasted_iota(jnp.int32, shape, len(shape) - 1)
 
 
-def call(kernel, out_shape, ins, scratch=(), mib=8):
+def call(kernel, out_shape, ins, scratch=(), mib=8, out=VMEM):
     return pl.pallas_call(
         kernel,
         out_shape=out_shape,
         in_specs=ins,
-        out_specs=jax.tree.map(lambda _: VMEM, out_shape),
+        out_specs=jax.tree.map(lambda _: out, out_shape),
         scratch_shapes=list(scratch),
         compiler_params=pltpu.CompilerParams(vmem_limit_bytes=mib << 20),
     )
@@ -54,12 +58,12 @@
     gate = dot_nt(act, mod_ref[2])
     packed[...] = jnp.concatenate([shift, scale], axis=1)
     packed[9:13, :] = jnp.concatenate([gate[0:4], gate[4:8]], axis=1)
-    out_ref[...] = jnp.broadcast_to(packed[...][None], out_ref.shape)
+    out_ref[...] = jnp.broadcast_to(packed[...].astype(bf16)[None], out_ref.shape)
 
 
 def rows_kernel(in_ref, *refs):
     out_ref, total = refs[-2:]
-    total[...] = jnp.sum(in_ref[...], axis=0)
+    total[...] = jnp.sum(in_ref[...].astype(f32), axis=0)
     copies = out_ref.shape[0] // 8
     for d in range(8):
         gate = total[9 + d % 4 : 10 + d % 4, :]
@@ -178,8 +182,9 @@
         win_ref[:, b * REACH : (b + 1) * REACH, :] = acc.reshape(heads, REACH, LANES)
 
 
-def attend_kernel(q_ref, win_ref, ctx_ref, sink_ref, bias_ref, out_ref, ones_s, done):
+def attend_kernel(q_ref, win_ref, ctx_ref, sink_ref, bias_ref, _, out_ref, ones_s, done, sems):
     heads, n, _ = q_ref.shape
+    copies = []
     kv = ctx_ref[...]
     ones_s[...] = with_ones(kv)
     step = REACH
@@ -205,7 +210,12 @@
             even = pltpu.roll(acc[2 * pair], HEAD, 1)
             both = jnp.where(lane < HEAD, even, acc[2 * pair + 1])
             done[at, pair * LANES : (pair + 1) * LANES] = both.astype(bf16)
-    out_ref[...] = jnp.broadcast_to(done[...][None], out_ref.shape)
+        for k in range(out_ref.shape[0]):
+            copy = pltpu.make_async_copy(done.at[at], out_ref.at[k, at], sems.at[b, k])
+            copy.start()
+            copies.append(copy)
+    for copy in copies:
+        copy.wait()
 
 
 def out_kernel(att_ref, w_ref, x_ref, rows_ref, out_ref):
@@ -248,27 +258,29 @@
     n = x.shape[0]
     partial = call(
         partial_kernel,
-        jax.ShapeDtypeStruct((sp, 16, LANES), f32),
+        jax.ShapeDtypeStruct((sp, 16, LANES), bf16),
         [VMEM] * 3,
         [pltpu.VMEM((16, LANES), f32), pltpu.VMEM((16, LANES), f32)],
-        2,
+        56,
     )(conditioning, context_cond[None, :], modulation.transpose(0, 2, 1))
     with jax.named_scope("sums"):
         partials = lax.all_to_all(partial, "sp", 0, 0, tiled=True)
     flat = jax.ShapeDtypeStruct((n, LANES), f32)
     cflat = jax.ShapeDtypeStruct((ctx.shape[0], LANES), f32)
     mean, rstd, cmean, crstd = call(stats_kernel, (flat, flat, cflat, cflat), [VMEM] * 2, (), 8)(
-        x, ctx
+        in_hbm(x), in_hbm(ctx)
     )
     wkv = jnp.concatenate([key_projection.T, value_projection.T], axis=0)
     cos, sin = rotary_tables(n, lax.axis_index("sp") * n)
+    cols = out_weight.shape[1]
+    own = lax.dynamic_slice_in_dim(x, lax.axis_index("tp") * cols, cols, 1)
     send = call(
         rows_kernel,
         jax.ShapeDtypeStruct((spread, 4, LANES), f32),
-        [VMEM] + [ANY] * 4,
+        [VMEM] + [ANY] * 5,
         [pltpu.VMEM((16, LANES), f32)],
         2,
-    )(partials, cmean, wkv, cos, sin)
+    )(partials, cmean, wkv, cos, sin, own)
     with jax.named_scope("spread"):
         rows = lax.all_to_all(send, ("tp", "dp"), 0, 0, tiled=True)
     ctx_kv = call(
@@ -292,8 +304,8 @@
         ),
         [VMEM] * 8,
         [pltpu.VMEM(x.shape, bf16)],
-        12,
-    )(x, mean, rstd, rows, query_weight, wkv, cos, sin)
+        6,
+    )(in_hbm(x), mean, rstd, rows, in_hbm(query_weight), wkv, cos, sin)
     up = [(i, i + 1) for i in range(sp - 1)]
     down = [(i + 1, i) for i in range(sp - 1)]
     with jax.named_scope("halo"):
@@ -305,19 +317,22 @@
         jax.ShapeDtypeStruct((heads, n, LANES), f32),
         [VMEM] * 4,
         [wide, wide],
-        12,
+        5,
     )(q, kv, before, after)
     attended = call(
         attend_kernel,
-        jax.ShapeDtypeStruct((tp, n, heads * HEAD), bf16),
-        [VMEM] * 3 + [SMEM] * 2,
-        [pltpu.VMEM(ctx_all.shape, bf16), pltpu.VMEM((n, heads * HEAD), bf16)],
-        16,
-    )(q, win, ctx_all, sink_head_logit, prefix_logit_bias)
+        pltpu.HBM((tp, n, heads * HEAD), bf16),
+        [VMEM] * 3 + [SMEM] * 2 + [ANY],
+        [
+            pltpu.VMEM(ctx_all.shape, bf16),
+            pltpu.VMEM((n, heads * HEAD), bf16),
+            pltpu.SemaphoreType.DMA((n // REACH, tp)),
+        ],
+        8,
+        ANY,
+    )(q, win, ctx_all, sink_head_logit, prefix_logit_bias, out_weight)
     with jax.named_scope("heads"):
         every = lax.all_to_all(attended, "tp", 0, 0, tiled=True)
-    cols = out_weight.shape[1]
-    own = lax.dynamic_slice_in_dim(x, lax.axis_index("tp") * cols, cols, 1)
     out = call(out_kernel, jax.ShapeDtypeStruct((n, cols), f32), [VMEM] * 4, (), 8)(
         every, out_weight, own, rows
     )

time: 94.2 us -> 90.9 us (0.965)
  blocking collectives: 14.6 us -> 30 us
  waiting for transfers between devices: 28.7 us -> 13.6 us
  local copies, waits for them, and re-layouts: 7.96 us -> 1.06 us
  Pallas kernels: 12.5 us -> 16.3 us
  starting transfers between devices: 28.9 us -> 27.6 us
    all_to_all x0 -> x1, blocking collectives: none -> 15.4 us  [per_device(): every = lax.all_to_all(attended, 'tp', 0, 0, tiled=True)]
    all_to_all x1 -> x0, waiting for transfers between devices: 11.8 us -> none  [per_device(): every = lax.all_to_all(attended, 'tp', 0, 0, tiled=True)]
    unnamed x36 -> x12, local copies, waits for them, and re-layouts: 7.93 us -> 0.03 us
    all_to_all x1 -> x0, starting transfers between devices: 3.49 us -> none  [per_device(): every = lax.all_to_all(attended, 'tp', 0, 0, tiled=True)]
    all_to_all x1, waiting for transfers between devices: 9.18 us -> 5.72 us  [per_device(): partials = lax.all_to_all(partial, 'sp', 0, 0, tiled=True)]
    pallas_call x3, Pallas kernels: 7.1 us -> 9.29 us  [the longest x1 4.43 us: per_device(): call(attend_kernel, pltpu.HBM((tp, n, heads * HEAD), bf16), [VMEM] * 3 +...]
    all_to_all x1, starting transfers between devices: 4.31 us -> 6.33 us  [per_device(): ctx_all = lax.all_to_all(ctx_kv, 'sp', 0, 0, tiled=True).reshape(-1, LANES)]
    pallas_call x1, Pallas kernels: 1.4 us -> 3.1 us  [per_device(): call(project_kernel, (jax.ShapeDtypeStruct((heads, n, LANES), bf16), jax....]
  transfers between devices with their start and end apart: 5 -> 4, of which waited for: 5 -> 4; matrix products, arithmetic and copies ran while one was open for 1% -> 3% of each run, Pallas kernels for 5% -> 8%
where the time goes in v3:
time: 90.9 us; the launch traced here: 90.3 us
  blocking collectives  30 us (33%)
  starting transfers between devices  27.6 us (30%)
  Pallas kernels  16.3 us (18%)
  waiting for transfers between devices  13.6 us (15%)
  other arithmetic  1.56 us (2%)
  local copies, waits for them, and re-layouts  1.06 us (1%)
    all_to_all x1, blocking collectives, per_device(): every = lax.all_to_all(attended, 'tp', 0, 0, tiled=True)  15.4 us
    all_to_all x1, starting transfers between devices, per_device(): partials = lax.all_to_all(partial, 'sp', 0, 0, tiled=True)  15.3 us
    all_to_all x1, blocking collectives, per_device(): rows = lax.all_to_all(send, ('tp', 'dp'), 0, 0, tiled=True)  14.6 us
    all_to_all x1, starting transfers between devices, per_device(): ctx_all = lax.all_to_all(ctx_kv, 'sp', 0, 0, tiled=True).reshape(-1, LANES)  6.33 us
    all_to_all x1, waiting for transfers between devices, per_device(): partials = lax.all_to_all(partial, 'sp', 0, 0, tiled=True)  5.72 us
    pallas_call x1, Pallas kernels, per_device(): call(attend_kernel, pltpu.HBM((tp, n, heads * HEAD), bf16), [VMEM] * 3 +...  4.43 us
    all_to_all x1, waiting for transfers between devices, per_device(): ctx_all = lax.all_to_all(ctx_kv, 'sp', 0, 0, tiled=True).reshape(-1, LANES)  4.34 us
    ppermute x1, starting transfers between devices, per_device(): before = lax.ppermute(last, 'sp', up)  3.51 us
  transfers between devices with their start and end apart: 4, of which 4 were waited for; matrix products, arithmetic and copies ran while one was open for 3% of the time, Pallas kernels for 8%

profile of v3, /device:TPU:32, one launch (start us, length us, event | category | flops | bytes accessed | tf_op | source)
XLA Modules:
  0.0 90.3 jit_solution(17436386989429016886)
XLA Ops:
  0.0 1.7 %shard_map.137 = bf16[16,16,128]{2,1,0:T(8,128)(2,1)} custom-call(bf16[8,128]{1,0:T(8,128)(2,1)} %cond_ref.1, bf16[1,128]{1,0:T(2,128)(2,1)} %bitcast.18, bf16[3,64,128]{2,1,0:T(8,128)(2,1)} %bitcast.17), custom_call_target="tpu_custom_call" | custom-call | tf_op jit(solution)/shard_map/pallas_call | solution.py:259
  1.7 0.0 copy-start.4
  1.7 0.0 copy-start.5
  1.7 15.3 %all-to-all-start = ((bf16[16,16,128]{2,1,0:T(8,128)(2,1)}), bf16[16,16,128]{2,1,0:T(8,128)(2,1)S(1)}, u32[]{:S(2)}, u32[]{:S(2)}) async-start(bf16[16,16,128]{2,1,0:T(8,128)(2,1)} %shard_map.137), calls=%async_computation | async-start | bytes 131072 | tf_op jit(solution)/shard_map/sums/all_to_all | solution.py:267
  17.1 1.5 %sine_multiply_fusion = (f32[384,128]{1,0:T(8,128)S(1)}, f32[384,128]{1,0:T(8,128)S(1)}) fusion(f32[128]{0:T(128)} %constant.55.clone, f32[128]{0:T(128)} %constant.53.clone, s32[384]{0:T(512)S(1)} %get-tuple-element.23, s32[384]{0:T(512)S(1)} %get-tuple-element.24, pred[128]{0:T(512)(128)(4,1)} %constant.54.clone), kind=kLoop, calls=%fused_computation.2 | loop fusion | flops 196608 | bytes 397440 | tf_op jit(solution)/shard_map/mul | solution.py:248
  18.6 1.0 %dynamic-slice_bitcast_fusion.refs_4_.x_ref = bf16[384,512]{1,0:T(8,128)(2,1)S(1)} fusion(bf16[1,384,2048]{2,1,0:T(8,128)(2,1)} %param.14, s32[]{:T(128)S(6)} %select_n.30), kind=kLoop, calls=%fused_computation.1 | loop fusion | bytes 786436 | tf_op jit(solution)/shard_map/dynamic_slice | solution.py:276
  19.6 3.2 %shard_map.136 = (f32[384,128]{1,0:T(8,128)S(1)}, f32[384,128]{1,0:T(8,128)S(1)}, f32[64,128]{1,0:T(8,128)S(1)}, f32[64,128]{1,0:T(8,128)S(1)}) custom-call(bf16[384,2048]{1,0:T(8,128)(2,1)} %bitcast.13, bf16[64,2048]{1,0:T(8,128)(2,1)} %bitcast.11), custom_call_target="tpu_custom_call" | custom-call | tf_op jit(solution)/shard_map/pallas_call | solution.py:270
  22.8 0.0 copy-start.1
  22.8 0.0 copy-done.4
  22.8 0.0 copy-done.5
  22.9 5.7 %all-to-all-done.in_ref = bf16[16,16,128]{2,1,0:T(8,128)(2,1)S(1)} async-done(((bf16[16,16,128]{2,1,0:T(8,128)(2,1)}), bf16[16,16,128]{2,1,0:T(8,128)(2,1)S(1)}, u32[]{:S(2)}, u32[]{:S(2)}) %all-to-all-start) | async-done | bytes 65568 | tf_op jit(solution)/shard_map/sums/all_to_all | solution.py:267
  28.6 0.1 shard_map.138
  28.7 14.6 %all_to_all.20.rows_ref = f32[32,4,128]{2,1,0:T(4,128)S(1)} all-to-all(f32[32,4,128]{2,1,0:T(4,128)S(1)} %shard_map.138), channel_id=1, replica_groups=mesh['sp'=16,'tp'=4,'dp'=8] {'tp','dp'}, dimensions={0} | all-to-all | bytes 131072 | tf_op jit(solution)/shard_map/spread/all_to_all | solution.py:285
  43.3 0.0 copy-done.1
  43.3 1.1 %shard_map.141 = bf16[16,64,128]{2,1,0:T(8,128)(2,1)} custom-call(bf16[64,2048]{1,0:T(8,128)(2,1)S(1)} %bitcast.12, f32[64,128]{1,0:T(8,128)S(1)} %get-tuple-element.15.refs_0_.mean_ref, f32[64,128]{1,0:T(8,128)S(1)} %get-tuple-element.20.rstd_ref, f32[32,4,128]{2,1,0:T(4,128)S(1)} %all_to_all.20.rows_ref, bf16[128,2048]{1,0:T(8,128)(2,1)S(1)} %pad_maximum_fusion.refs_1_.wkv_ref), custom_call_target="tpu_custom_call" | custom-call | tf_op jit(solution)/shard_map/pallas_call | solution.py:286
  44.4 6.3 %all-to-all-start.2 = ((bf16[16,64,128]{2,1,0:T(8,128)(2,1)}), bf16[16,64,128]{2,1,0:T(8,128)(2,1)S(1)}, u32[]{:S(2)}, u32[]{:S(2)}) async-start(bf16[16,64,128]{2,1,0:T(8,128)(2,1)} %shard_map.141), calls=%async_computation.2 | async-start | bytes 524288 | tf_op jit(solution)/shard_map/context/all_to_all | solution.py:294
  50.7 0.0 copy-start.2
  50.7 0.0 copy-start.3
  50.7 3.1 %shard_map.139 = (bf16[4,384,128]{2,1,0:T(8,128)(2,1)S(1)}, bf16[384,128]{1,0:T(8,128)(2,1)S(1)}, bf16[128,128]{1,0:T(8,128)(2,1)S(1)}, bf16[128,128]{1,0:T(8,128)(2,1)S(1)}) custom-call(bf16[384,2048]{1,0:T(8,128)(2,1)} %bitcast.14, f32[384,128]{1,0:T(8,128)S(1)} %get-tuple-element.13.mean_ref, f32[384,128]{1,0:T(8,128)S(1)} %get-tuple-element.14.rstd_ref, ...), custom_call_target="tpu_custom_call" | custom-call | tf_op jit(solution)/shard_map/pallas_call | solution.py:297
  53.8 0.0 copy-start
  53.8 3.5 %collective-permute-start = (bf16[128,128]{1,0:T(8,128)(2,1)S(1)}, bf16[128,128]{1,0:T(8,128)(2,1)S(1)}, u32[]{:S(2)}, u32[]{:S(2)}) collective-permute-start(bf16[128,128]{1,0:T(8,128)(2,1)S(1)} %get-tuple-element.18), channel_id=1, source_target_pairs={{0,32},{32,64},{64,96},{96,128},{128,160},{160,192},{192,224},{224... | collective-permute-start | bytes 98312 | tf_op jit(solution)/shard_map/halo/ppermute | solution.py:312
  57.4 2.5 %collective-permute-start.1 = (bf16[128,128]{1,0:T(8,128)(2,1)S(1)}, bf16[128,128]{1,0:T(8,128)(2,1)S(1)}, u32[]{:S(2)}, u32[]{:S(2)}) collective-permute-start(bf16[128,128]{1,0:T(8,128)(2,1)S(1)} %get-tuple-element.19), channel_id=1, source_target_pairs={{32,0},{64,32},{96,64},{128,96},{160,128},{192,160},{224,192},{256... | collective-permute-start | bytes 98312 | tf_op jit(solution)/shard_map/halo/ppermute | solution.py:313
  59.8 1.7 %collective-permute-done.before_ref = bf16[128,128]{1,0:T(8,128)(2,1)S(1)} collective-permute-done((bf16[128,128]{1,0:T(8,128)(2,1)S(1)}, bf16[128,128]{1,0:T(8,128)(2,1)S(1)}, u32[]{:S(2)}, u32[]{:S(2)}) %collective-permute-start) | collective-permute-done | bytes 32800 | tf_op jit(solution)/shard_map/halo/ppermute | solution.py:312
  61.5 1.9 %collective-permute-done.1.after_ref = bf16[128,128]{1,0:T(8,128)(2,1)S(1)} collective-permute-done((bf16[128,128]{1,0:T(8,128)(2,1)S(1)}, bf16[128,128]{1,0:T(8,128)(2,1)S(1)}, u32[]{:S(2)}, u32[]{:S(2)}) %collective-permute-start.1) | collective-permute-done | bytes 32800 | tf_op jit(solution)/shard_map/halo/ppermute | solution.py:313
  63.4 1.3 %shard_map.140.win_ref = f32[4,384,128]{2,1,0:T(8,128)S(1)} custom-call(bf16[4,384,128]{2,1,0:T(8,128)(2,1)S(1)} %get-tuple-element.16.q_ref, bf16[384,128]{1,0:T(8,128)(2,1)S(1)} %get-tuple-element.17.kv_ref, bf16[128,128]{1,0:T(8,128)(2,1)S(1)} %collective-permute-done.before_ref, bf16[128,128]{1,0:T(8,128)(2,1)S(1)} %collective-permute-done.1.after_ref), custom_call_target="tpu_custom_call" | custom-call | tf_op jit(solution)/shard_map/pallas_call | solution.py:315
  64.7 4.3 %all-to-all-done.2 = bf16[16,64,128]{2,1,0:T(8,128)(2,1)S(1)} async-done(((bf16[16,64,128]{2,1,0:T(8,128)(2,1)}), bf16[16,64,128]{2,1,0:T(8,128)(2,1)S(1)}, u32[]{:S(2)}, u32[]{:S(2)}) %all-to-all-start.2) | async-done | bytes 262176 | tf_op jit(solution)/shard_map/context/all_to_all | solution.py:294
  69.0 0.0 copy-done.2
  69.0 0.0 copy-done.3
  69.0 0.0 copy-done
  69.1 4.4 %shard_map.142 = bf16[4,384,256]{2,1,0:T(8,128)(2,1)} custom-call(bf16[4,384,128]{2,1,0:T(8,128)(2,1)S(1)} %get-tuple-element.16.q_ref, f32[4,384,128]{2,1,0:T(8,128)S(1)} %shard_map.140.win_ref, bf16[1024,128]{1,0:T(8,128)(2,1)S(1)} %bitcast.10, f32[4]{0:T(128)S(1)} %copy-done.2, f32[4]{0:T(128)S(1)} %copy-done.3, bf16[1024,512]{1,0:T(8,128)(2,1)S(1)} %copy-done), custom_call_target="tpu_custom_call" | custom-call | tf_op jit(solution)/shard_map/pallas_call | solution.py:322
  73.5 15.4 %all_to_all.21.att_ref = bf16[4,384,256]{2,1,0:T(8,128)(2,1)S(1)} all-to-all(bf16[4,384,256]{2,1,0:T(8,128)(2,1)} %shard_map.142), channel_id=1, replica_groups=mesh['sp'=16,'tp'=4,'dp'=8] {'tp'}, dimensions={0} | all-to-all | bytes 1572864 | tf_op jit(solution)/shard_map/heads/all_to_all | solution.py:335
  88.9 1.5 %shard_map.143 = f32[384,512]{1,0:T(8,128)} custom-call(bf16[4,384,256]{2,1,0:T(8,128)(2,1)S(1)} %all_to_all.21.att_ref, bf16[1024,512]{1,0:T(8,128)(2,1)S(1)} %copy-done, bf16[384,512]{1,0:T(8,128)(2,1)S(1)} %dynamic-slice_bitcast_fusion.refs_4_.x_ref, f32[32,4,128]{2,1,0:T(4,128)S(1)} %all_to_all.20.rows_ref), custom_call_target="tpu_custom_call" | custom-call | tf_op jit(solution)/shard_map/pallas_call | solution.py:336
  (2 shorter events, 0.1 us)
Async XLA Ops:
  1.7 21.1 %copy-start.4 = (bf16[2048,64]{0,1:T(8,128)(2,1)S(1)}, bf16[2048,64]{0,1:T(8,128)(2,1)}, u32[]{:S(2)}) copy-start(bf16[2048,64]{0,1:T(8,128)(2,1)} %param.21) | copy-start | bytes 786436
  1.7 21.1 %copy-start.5 = (bf16[2048,64]{0,1:T(8,128)(2,1)S(1)}, bf16[2048,64]{0,1:T(8,128)(2,1)}, u32[]{:S(2)}) copy-start(bf16[2048,64]{0,1:T(8,128)(2,1)} %param.20) | copy-start | bytes 786436
  1.7 26.9 %all-to-all-start = ((bf16[16,16,128]{2,1,0:T(8,128)(2,1)}), bf16[16,16,128]{2,1,0:T(8,128)(2,1)S(1)}, u32[]{:S(2)}, u32[]{:S(2)}) async-start(bf16[16,16,128]{2,1,0:T(8,128)(2,1)} %shard_map.137), calls=%async_computation | async-start | bytes 131072 | tf_op jit(solution)/shard_map/sums/all_to_all | solution.py:267
  22.8 20.5 %copy-start.1 = (bf16[1,64,2048]{2,1,0:T(8,128)(2,1)S(1)}, bf16[1,64,2048]{2,1,0:T(8,128)(2,1)}, u32[]{:S(2)}) copy-start(bf16[1,64,2048]{2,1,0:T(8,128)(2,1)} %param.18) | copy-start | bytes 786436
  44.4 24.7 %all-to-all-start.2 = ((bf16[16,64,128]{2,1,0:T(8,128)(2,1)}), bf16[16,64,128]{2,1,0:T(8,128)(2,1)S(1)}, u32[]{:S(2)}, u32[]{:S(2)}) async-start(bf16[16,64,128]{2,1,0:T(8,128)(2,1)} %shard_map.141), calls=%async_computation.2 | async-start | bytes 524288 | tf_op jit(solution)/shard_map/context/all_to_all | solution.py:294
  50.7 18.3 %copy-start.2 = (f32[4]{0:T(128)S(1)}, f32[4]{0:T(128)}, u32[]{:S(2)}) copy-start(f32[4]{0:T(128)} %sink_ref.1) | copy-start | bytes 52
  50.7 18.3 %copy-start.3 = (f32[4]{0:T(128)S(1)}, f32[4]{0:T(128)}, u32[]{:S(2)}) copy-start(f32[4]{0:T(128)} %bias_ref.1) | copy-start | bytes 52
  53.8 15.2 %copy-start = (bf16[1024,512]{1,0:T(8,128)(2,1)S(1)}, bf16[1024,512]{1,0:T(8,128)(2,1)}, u32[]{:S(2)}) copy-start(bf16[1024,512]{1,0:T(8,128)(2,1)} %w_ref.1) | copy-start | bytes 3145732
  53.8 7.6 %collective-permute-start = (bf16[128,128]{1,0:T(8,128)(2,1)S(1)}, bf16[128,128]{1,0:T(8,128)(2,1)S(1)}, u32[]{:S(2)}, u32[]{:S(2)}) collective-permute-start(bf16[128,128]{1,0:T(8,128)(2,1)S(1)} %get-tuple-element.18), channel_id=1, source_target_pairs={{0,32},{32,64},{64,96},{96,128},{128,160},{160,192},{192,224},{224... | collective-permute-start | bytes 98312 | tf_op jit(solution)/shard_map/halo/ppermute | solution.py:312
  57.4 6.0 %collective-permute-start.1 = (bf16[128,128]{1,0:T(8,128)(2,1)S(1)}, bf16[128,128]{1,0:T(8,128)(2,1)S(1)}, u32[]{:S(2)}, u32[]{:S(2)}) collective-permute-start(bf16[128,128]{1,0:T(8,128)(2,1)S(1)} %get-tuple-element.19), channel_id=1, source_target_pairs={{32,0},{64,32},{96,64},{128,96},{160,128},{192,160},{224,192},{256... | collective-permute-start | bytes 98312 | tf_op jit(solution)/shard_map/halo/ppermute | solution.py:313

commit v4 on v3

--- a/solution.py
+++ b/solution.py
@@ -15,6 +15,8 @@
 ROTARY_BASE = 10000.0
 MASKED = -1e30
 LANES = 128
+PARTIAL_ROWS = 24
+GATE_ROWS = (9, 10, 11, 21)
 
 f32 = jnp.float32
 bf16 = jnp.bfloat16
@@ -56,17 +58,24 @@
     shift = dot_nt(act, mod_ref[0])
     scale = dot_nt(act, mod_ref[1])
     gate = dot_nt(act, mod_ref[2])
-    packed[...] = jnp.concatenate([shift, scale], axis=1)
-    packed[9:13, :] = jnp.concatenate([gate[0:4], gate[4:8]], axis=1)
+    both = jnp.concatenate([shift, scale], axis=1)
+    gates = jnp.concatenate([gate[0:4], gate[4:8]], axis=1)
+    packed[...] = jnp.zeros_like(packed)
+    packed[0:9, :] = both[0:9]
+    packed[12:21, :] = (both - both.astype(bf16).astype(f32))[0:9]
+    for j, row in enumerate(GATE_ROWS):
+        packed[row : row + 1, :] = gates[j : j + 1]
     out_ref[...] = jnp.broadcast_to(packed[...].astype(bf16)[None], out_ref.shape)
 
 
 def rows_kernel(in_ref, *refs):
     out_ref, total = refs[-2:]
     total[...] = jnp.sum(in_ref[...].astype(f32), axis=0)
+    total[0:9, :] = total[0:9, :] + total[12:21, :]
     copies = out_ref.shape[0] // 8
     for d in range(8):
-        gate = total[9 + d % 4 : 10 + d % 4, :]
+        row = GATE_ROWS[d % 4]
+        gate = total[row : row + 1, :]
         if d >= 4:
             gate = pltpu.roll(gate, 64, 1)
         for t in range(copies):
@@ -182,21 +191,19 @@
         win_ref[:, b * REACH : (b + 1) * REACH, :] = acc.reshape(heads, REACH, LANES)
 
 
-def attend_kernel(q_ref, win_ref, ctx_ref, sink_ref, bias_ref, _, out_ref, ones_s, done, sems):
+def attend_kernel(q_ref, win_ref, ctx_ref, sink_ref, bias_ref, _, out_ref, ones_s):
     heads, n, _ = q_ref.shape
-    copies = []
     kv = ctx_ref[...]
     ones_s[...] = with_ones(kv)
-    step = REACH
-    rows = heads * step
-    lane = lanes_of((step, LANES))
-    head = lax.broadcasted_iota(jnp.int32, (rows, 1), 0) // step
+    rows = heads * REACH
+    lane = lanes_of((REACH, LANES))
+    head = lax.broadcasted_iota(jnp.int32, (rows, 1), 0) // REACH
     bias, sink = jnp.zeros((rows, 1), f32), jnp.zeros((rows, 1), f32)
     for h in range(heads):
         bias = jnp.where(head == h, bias_ref[h], bias)
         sink = jnp.where(head == h, sink_ref[h], sink)
-    for b in range(n // step):
-        at = slice(b * step, (b + 1) * step)
+    for b in range(n // REACH):
+        at = slice(b * REACH, (b + 1) * REACH)
         s = dot_nt(q_ref[:, at, :].reshape(rows, LANES), kv)
         win = win_ref[:, at, :].reshape(rows, LANES)
         win_top = win[:, 0:1]
@@ -205,17 +212,12 @@
         acc = jnp.dot(p, ones_s[...], preferred_element_type=f32)
         acc = acc + win * jnp.exp(win_top - top)
         den = acc[:, 1:2] + jnp.exp(sink - top)
-        acc = (acc / den).reshape(heads, step, LANES)
+        acc = (acc / den).reshape(heads, REACH, LANES)
         for pair in range(heads // 2):
             even = pltpu.roll(acc[2 * pair], HEAD, 1)
-            both = jnp.where(lane < HEAD, even, acc[2 * pair + 1])
-            done[at, pair * LANES : (pair + 1) * LANES] = both.astype(bf16)
-        for k in range(out_ref.shape[0]):
-            copy = pltpu.make_async_copy(done.at[at], out_ref.at[k, at], sems.at[b, k])
-            copy.start()
-            copies.append(copy)
-    for copy in copies:
-        copy.wait()
+            both = jnp.where(lane < HEAD, even, acc[2 * pair + 1]).astype(bf16)
+            for k in range(out_ref.shape[0]):
+                out_ref[k, at, pair * LANES : (pair + 1) * LANES] = both
 
 
 def out_kernel(att_ref, w_ref, x_ref, rows_ref, out_ref):
@@ -258,9 +260,9 @@
     n = x.shape[0]
     partial = call(
         partial_kernel,
-        jax.ShapeDtypeStruct((sp, 16, LANES), bf16),
+        jax.ShapeDtypeStruct((sp, PARTIAL_ROWS, LANES), bf16),
         [VMEM] * 3,
-        [pltpu.VMEM((16, LANES), f32), pltpu.VMEM((16, LANES), f32)],
+        [pltpu.VMEM((16, LANES), f32), pltpu.VMEM((PARTIAL_ROWS, LANES), f32)],
         56,
     )(conditioning, context_cond[None, :], modulation.transpose(0, 2, 1))
     with jax.named_scope("sums"):
@@ -278,7 +280,7 @@
         rows_kernel,
         jax.ShapeDtypeStruct((spread, 4, LANES), f32),
         [VMEM] + [ANY] * 5,
-        [pltpu.VMEM((16, LANES), f32)],
+        [pltpu.VMEM((PARTIAL_ROWS, LANES), f32)],
         2,
     )(partials, cmean, wkv, cos, sin, own)
     with jax.named_scope("spread"):
@@ -321,15 +323,10 @@
     )(q, kv, before, after)
     attended = call(
         attend_kernel,
-        pltpu.HBM((tp, n, heads * HEAD), bf16),
+        jax.ShapeDtypeStruct((tp, n, heads * HEAD), bf16),
         [VMEM] * 3 + [SMEM] * 2 + [ANY],
-        [
-            pltpu.VMEM(ctx_all.shape, bf16),
-            pltpu.VMEM((n, heads * HEAD), bf16),
-            pltpu.SemaphoreType.DMA((n // REACH, tp)),
-        ],
+        [pltpu.VMEM(ctx_all.shape, bf16)],
         8,
-        ANY,
     )(q, win, ctx_all, sink_head_logit, prefix_logit_bias, out_weight)
     with jax.named_scope("heads"):
         every = lax.all_to_all(attended, "tp", 0, 0, tiled=True)

time: 90.9 us -> 88.9 us (0.978)
  starting transfers between devices: 27.6 us -> 26.2 us
  waiting for transfers between devices: 13.6 us -> 15 us
  blocking collectives: 30 us -> 28.9 us
    all_to_all x1, starting transfers between devices: 6.33 us -> 4.99 us  [per_device(): ctx_all = lax.all_to_all(ctx_kv, 'sp', 0, 0, tiled=True).reshape(-1, LANES)]
    all_to_all x1, waiting for transfers between devices: 5.72 us -> 7.05 us  [per_device(): partials = lax.all_to_all(partial, 'sp', 0, 0, tiled=True)]
    all_to_all x1, blocking collectives: 15.4 us -> 14.3 us  [per_device(): every = lax.all_to_all(attended, 'tp', 0, 0, tiled=True)]
  transfers between devices with their start and end apart: 4 -> 4, of which waited for: 4 -> 4; matrix products, arithmetic and copies ran while one was open for 3% -> 3% of each run, Pallas kernels for 8% -> 9%
where the time goes in v4:
time: 88.9 us; the launch traced here: 88.4 us
  blocking collectives  28.9 us (33%)
  starting transfers between devices  26.2 us (29%)
  Pallas kernels  15.5 us (17%)
  waiting for transfers between devices  15 us (17%)
  other arithmetic  1.61 us (2%)
  local copies, waits for them, and re-layouts  1.1 us (1%)
    all_to_all x1, starting transfers between devices, per_device(): partials = lax.all_to_all(partial, 'sp', 0, 0, tiled=True)  15.2 us
    all_to_all x1, blocking collectives, per_device(): rows = lax.all_to_all(send, ('tp', 'dp'), 0, 0, tiled=True)  14.6 us
    all_to_all x1, blocking collectives, per_device(): every = lax.all_to_all(attended, 'tp', 0, 0, tiled=True)  14.3 us
    all_to_all x1, waiting for transfers between devices, per_device(): partials = lax.all_to_all(partial, 'sp', 0, 0, tiled=True)  7.05 us
    all_to_all x1, starting transfers between devices, per_device(): ctx_all = lax.all_to_all(ctx_kv, 'sp', 0, 0, tiled=True).reshape(-1, LANES)  4.99 us
    all_to_all x1, waiting for transfers between devices, per_device(): ctx_all = lax.all_to_all(ctx_kv, 'sp', 0, 0, tiled=True).reshape(-1, LANES)  4.34 us
    pallas_call x1, Pallas kernels, per_device(): call(attend_kernel, jax.ShapeDtypeStruct((tp, n, heads * HEAD), bf16), [V...  3.56 us
    ppermute x1, starting transfers between devices, per_device(): before = lax.ppermute(last, 'sp', up)  3.49 us
  transfers between devices with their start and end apart: 4, of which 4 were waited for; matrix products, arithmetic and copies ran while one was open for 3% of the time, Pallas kernels for 9%

profile of v4, /device:TPU:32, one launch (start us, length us, event | category | flops | bytes accessed | tf_op | source)
XLA Modules:
  0.0 88.4 jit_solution(17182572120378935873)
XLA Ops:
  0.0 1.7 %shard_map.137 = bf16[16,24,128]{2,1,0:T(8,128)(2,1)} custom-call(bf16[8,128]{1,0:T(8,128)(2,1)} %cond_ref.1, bf16[1,128]{1,0:T(2,128)(2,1)} %bitcast.18, bf16[3,64,128]{2,1,0:T(8,128)(2,1)} %bitcast.17), custom_call_target="tpu_custom_call" | custom-call | tf_op jit(solution)/shard_map/pallas_call | solution.py:261
  1.7 15.2 %all-to-all-start = ((bf16[16,24,128]{2,1,0:T(8,128)(2,1)}), bf16[16,24,128]{2,1,0:T(8,128)(2,1)S(1)}, u32[]{:S(2)}, u32[]{:S(2)}) async-start(bf16[16,24,128]{2,1,0:T(8,128)(2,1)} %shard_map.137), calls=%async_computation | async-start | bytes 196608 | tf_op jit(solution)/shard_map/sums/all_to_all | solution.py:269
  16.9 0.0 copy-start.4
  16.9 0.0 copy-start.5
  17.0 1.6 %sine_multiply_fusion = (f32[384,128]{1,0:T(8,128)S(1)}, f32[384,128]{1,0:T(8,128)S(1)}) fusion(f32[128]{0:T(128)} %constant.55.clone, f32[128]{0:T(128)} %constant.53.clone, s32[384]{0:T(512)S(1)} %get-tuple-element.23, s32[384]{0:T(512)S(1)} %get-tuple-element.24, pred[128]{0:T(512)(128)(4,1)} %constant.54.clone), kind=kLoop, calls=%fused_computation.2 | loop fusion | flops 196608 | bytes 397440 | tf_op jit(solution)/shard_map/mul | solution.py:250
  18.5 3.2 %shard_map.136 = (f32[384,128]{1,0:T(8,128)S(1)}, f32[384,128]{1,0:T(8,128)S(1)}, f32[64,128]{1,0:T(8,128)S(1)}, f32[64,128]{1,0:T(8,128)S(1)}) custom-call(bf16[384,2048]{1,0:T(8,128)(2,1)} %bitcast.13, bf16[64,2048]{1,0:T(8,128)(2,1)} %bitcast.11), custom_call_target="tpu_custom_call" | custom-call | tf_op jit(solution)/shard_map/pallas_call | solution.py:272
  21.7 0.0 copy-start.1
  21.7 1.1 %dynamic-slice_bitcast_fusion.refs_4_.x_ref = bf16[384,512]{1,0:T(8,128)(2,1)S(1)} fusion(bf16[1,384,2048]{2,1,0:T(8,128)(2,1)} %param.14, s32[]{:T(128)S(6)} %select_n.30), kind=kLoop, calls=%fused_computation.1 | loop fusion | bytes 786436 | tf_op jit(solution)/shard_map/dynamic_slice | solution.py:278
  22.8 0.0 copy-done.4
  22.8 0.0 copy-done.5
  22.9 7.0 %all-to-all-done.in_ref = bf16[16,24,128]{2,1,0:T(8,128)(2,1)S(1)} async-done(((bf16[16,24,128]{2,1,0:T(8,128)(2,1)}), bf16[16,24,128]{2,1,0:T(8,128)(2,1)S(1)}, u32[]{:S(2)}, u32[]{:S(2)}) %all-to-all-start) | async-done | bytes 98336 | tf_op jit(solution)/shard_map/sums/all_to_all | solution.py:269
  29.9 0.1 shard_map.138
  30.0 14.6 %all_to_all.20.rows_ref = f32[32,4,128]{2,1,0:T(4,128)S(1)} all-to-all(f32[32,4,128]{2,1,0:T(4,128)S(1)} %shard_map.138), channel_id=1, replica_groups=mesh['sp'=16,'tp'=4,'dp'=8] {'tp','dp'}, dimensions={0} | all-to-all | bytes 131072 | tf_op jit(solution)/shard_map/spread/all_to_all | solution.py:287
  44.6 0.0 copy-done.1
  44.6 1.1 %shard_map.141 = bf16[16,64,128]{2,1,0:T(8,128)(2,1)} custom-call(bf16[64,2048]{1,0:T(8,128)(2,1)S(1)} %bitcast.12, f32[64,128]{1,0:T(8,128)S(1)} %get-tuple-element.15.refs_0_.mean_ref, f32[64,128]{1,0:T(8,128)S(1)} %get-tuple-element.20.rstd_ref, f32[32,4,128]{2,1,0:T(4,128)S(1)} %all_to_all.20.rows_ref, bf16[128,2048]{1,0:T(8,128)(2,1)S(1)} %pad_maximum_fusion.refs_1_.wkv_ref), custom_call_target="tpu_custom_call" | custom-call | tf_op jit(solution)/shard_map/pallas_call | solution.py:288
  45.7 5.0 %all-to-all-start.2 = ((bf16[16,64,128]{2,1,0:T(8,128)(2,1)}), bf16[16,64,128]{2,1,0:T(8,128)(2,1)S(1)}, u32[]{:S(2)}, u32[]{:S(2)}) async-start(bf16[16,64,128]{2,1,0:T(8,128)(2,1)} %shard_map.141), calls=%async_computation.2 | async-start | bytes 524288 | tf_op jit(solution)/shard_map/context/all_to_all | solution.py:296
  50.7 0.0 copy-start.2
  50.7 0.0 copy-start.3
  50.7 3.1 %shard_map.139 = (bf16[4,384,128]{2,1,0:T(8,128)(2,1)S(1)}, bf16[384,128]{1,0:T(8,128)(2,1)S(1)}, bf16[128,128]{1,0:T(8,128)(2,1)S(1)}, bf16[128,128]{1,0:T(8,128)(2,1)S(1)}) custom-call(bf16[384,2048]{1,0:T(8,128)(2,1)} %bitcast.14, f32[384,128]{1,0:T(8,128)S(1)} %get-tuple-element.13.mean_ref, f32[384,128]{1,0:T(8,128)S(1)} %get-tuple-element.14.rstd_ref, ...), custom_call_target="tpu_custom_call" | custom-call | tf_op jit(solution)/shard_map/pallas_call | solution.py:299
  53.8 0.0 copy-start
  53.8 3.5 %collective-permute-start = (bf16[128,128]{1,0:T(8,128)(2,1)S(1)}, bf16[128,128]{1,0:T(8,128)(2,1)S(1)}, u32[]{:S(2)}, u32[]{:S(2)}) collective-permute-start(bf16[128,128]{1,0:T(8,128)(2,1)S(1)} %get-tuple-element.18), channel_id=1, source_target_pairs={{0,32},{32,64},{64,96},{96,128},{128,160},{160,192},{192,224},{224... | collective-permute-start | bytes 98312 | tf_op jit(solution)/shard_map/halo/ppermute | solution.py:314
  57.3 2.5 %collective-permute-start.1 = (bf16[128,128]{1,0:T(8,128)(2,1)S(1)}, bf16[128,128]{1,0:T(8,128)(2,1)S(1)}, u32[]{:S(2)}, u32[]{:S(2)}) collective-permute-start(bf16[128,128]{1,0:T(8,128)(2,1)S(1)} %get-tuple-element.19), channel_id=1, source_target_pairs={{32,0},{64,32},{96,64},{128,96},{160,128},{192,160},{224,192},{256... | collective-permute-start | bytes 98312 | tf_op jit(solution)/shard_map/halo/ppermute | solution.py:315
  59.8 1.7 %collective-permute-done.before_ref = bf16[128,128]{1,0:T(8,128)(2,1)S(1)} collective-permute-done((bf16[128,128]{1,0:T(8,128)(2,1)S(1)}, bf16[128,128]{1,0:T(8,128)(2,1)S(1)}, u32[]{:S(2)}, u32[]{:S(2)}) %collective-permute-start) | collective-permute-done | bytes 32800 | tf_op jit(solution)/shard_map/halo/ppermute | solution.py:314
  61.5 1.9 %collective-permute-done.1.after_ref = bf16[128,128]{1,0:T(8,128)(2,1)S(1)} collective-permute-done((bf16[128,128]{1,0:T(8,128)(2,1)S(1)}, bf16[128,128]{1,0:T(8,128)(2,1)S(1)}, u32[]{:S(2)}, u32[]{:S(2)}) %collective-permute-start.1) | collective-permute-done | bytes 32800 | tf_op jit(solution)/shard_map/halo/ppermute | solution.py:315
  63.4 1.3 %shard_map.140.win_ref = f32[4,384,128]{2,1,0:T(8,128)S(1)} custom-call(bf16[4,384,128]{2,1,0:T(8,128)(2,1)S(1)} %get-tuple-element.16.q_ref, bf16[384,128]{1,0:T(8,128)(2,1)S(1)} %get-tuple-element.17.kv_ref, bf16[128,128]{1,0:T(8,128)(2,1)S(1)} %collective-permute-done.before_ref, bf16[128,128]{1,0:T(8,128)(2,1)S(1)} %collective-permute-done.1.after_ref), custom_call_target="tpu_custom_call" | custom-call | tf_op jit(solution)/shard_map/pallas_call | solution.py:317
  64.7 4.3 %all-to-all-done.2 = bf16[16,64,128]{2,1,0:T(8,128)(2,1)S(1)} async-done(((bf16[16,64,128]{2,1,0:T(8,128)(2,1)}), bf16[16,64,128]{2,1,0:T(8,128)(2,1)S(1)}, u32[]{:S(2)}, u32[]{:S(2)}) %all-to-all-start.2) | async-done | bytes 262176 | tf_op jit(solution)/shard_map/context/all_to_all | solution.py:296
  69.0 0.0 copy-done.2
  69.0 0.0 copy-done.3
  69.1 0.0 copy-done
  69.1 3.6 %shard_map.142 = bf16[4,384,256]{2,1,0:T(8,128)(2,1)S(1)} custom-call(bf16[4,384,128]{2,1,0:T(8,128)(2,1)S(1)} %get-tuple-element.16.q_ref, f32[4,384,128]{2,1,0:T(8,128)S(1)} %shard_map.140.win_ref, bf16[1024,128]{1,0:T(8,128)(2,1)S(1)} %bitcast.10, f32[4]{0:T(128)S(1)} %copy-done.2, f32[4]{0:T(128)S(1)} %copy-done.3, bf16[1024,512]{1,0:T(8,128)(2,1)S(1)} %copy-done), custom_call_target="tpu_custom_call" | custom-call | tf_op jit(solution)/shard_map/pallas_call | solution.py:324
  72.6 14.3 %all_to_all.21.att_ref = bf16[4,384,256]{2,1,0:T(8,128)(2,1)S(1)} all-to-all(bf16[4,384,256]{2,1,0:T(8,128)(2,1)S(1)} %shard_map.142), channel_id=1, replica_groups=mesh['sp'=16,'tp'=4,'dp'=8] {'tp'}, dimensions={0} | all-to-all | bytes 1572864 | tf_op jit(solution)/shard_map/heads/all_to_all | solution.py:332
  87.0 1.5 %shard_map.143 = f32[384,512]{1,0:T(8,128)} custom-call(bf16[4,384,256]{2,1,0:T(8,128)(2,1)S(1)} %all_to_all.21.att_ref, bf16[1024,512]{1,0:T(8,128)(2,1)S(1)} %copy-done, bf16[384,512]{1,0:T(8,128)(2,1)S(1)} %dynamic-slice_bitcast_fusion.refs_4_.x_ref, f32[32,4,128]{2,1,0:T(4,128)S(1)} %all_to_all.20.rows_ref), custom_call_target="tpu_custom_call" | custom-call | tf_op jit(solution)/shard_map/pallas_call | solution.py:333
  (2 shorter events, 0.1 us)
Async XLA Ops:
  1.7 28.2 %all-to-all-start = ((bf16[16,24,128]{2,1,0:T(8,128)(2,1)}), bf16[16,24,128]{2,1,0:T(8,128)(2,1)S(1)}, u32[]{:S(2)}, u32[]{:S(2)}) async-start(bf16[16,24,128]{2,1,0:T(8,128)(2,1)} %shard_map.137), calls=%async_computation | async-start | bytes 196608 | tf_op jit(solution)/shard_map/sums/all_to_all | solution.py:269
  16.9 5.9 %copy-start.4 = (bf16[2048,64]{0,1:T(8,128)(2,1)S(1)}, bf16[2048,64]{0,1:T(8,128)(2,1)}, u32[]{:S(2)}) copy-start(bf16[2048,64]{0,1:T(8,128)(2,1)} %param.21) | copy-start | bytes 786436
  16.9 5.9 %copy-start.5 = (bf16[2048,64]{0,1:T(8,128)(2,1)S(1)}, bf16[2048,64]{0,1:T(8,128)(2,1)}, u32[]{:S(2)}) copy-start(bf16[2048,64]{0,1:T(8,128)(2,1)} %param.20) | copy-start | bytes 786436
  21.7 22.9 %copy-start.1 = (bf16[1,64,2048]{2,1,0:T(8,128)(2,1)S(1)}, bf16[1,64,2048]{2,1,0:T(8,128)(2,1)}, u32[]{:S(2)}) copy-start(bf16[1,64,2048]{2,1,0:T(8,128)(2,1)} %param.18) | copy-start | bytes 786436
  45.7 23.3 %all-to-all-start.2 = ((bf16[16,64,128]{2,1,0:T(8,128)(2,1)}), bf16[16,64,128]{2,1,0:T(8,128)(2,1)S(1)}, u32[]{:S(2)}, u32[]{:S(2)}) async-start(bf16[16,64,128]{2,1,0:T(8,128)(2,1)} %shard_map.141), calls=%async_computation.2 | async-start | bytes 524288 | tf_op jit(solution)/shard_map/context/all_to_all | solution.py:296
  50.7 18.3 %copy-start.2 = (f32[4]{0:T(128)S(1)}, f32[4]{0:T(128)}, u32[]{:S(2)}) copy-start(f32[4]{0:T(128)} %sink_ref.1) | copy-start | bytes 52
  50.7 18.3 %copy-start.3 = (f32[4]{0:T(128)S(1)}, f32[4]{0:T(128)}, u32[]{:S(2)}) copy-start(f32[4]{0:T(128)} %bias_ref.1) | copy-start | bytes 52
  53.8 15.2 %copy-start = (bf16[1024,512]{1,0:T(8,128)(2,1)S(1)}, bf16[1024,512]{1,0:T(8,128)(2,1)}, u32[]{:S(2)}) copy-start(bf16[1024,512]{1,0:T(8,128)(2,1)} %w_ref.1) | copy-start | bytes 3145732
  53.8 7.6 %collective-permute-start = (bf16[128,128]{1,0:T(8,128)(2,1)S(1)}, bf16[128,128]{1,0:T(8,128)(2,1)S(1)}, u32[]{:S(2)}, u32[]{:S(2)}) collective-permute-start(bf16[128,128]{1,0:T(8,128)(2,1)S(1)} %get-tuple-element.18), channel_id=1, source_target_pairs={{0,32},{32,64},{64,96},{96,128},{128,160},{160,192},{192,224},{224... | collective-permute-start | bytes 98312 | tf_op jit(solution)/shard_map/halo/ppermute | solution.py:314
  57.3 6.1 %collective-permute-start.1 = (bf16[128,128]{1,0:T(8,128)(2,1)S(1)}, bf16[128,128]{1,0:T(8,128)(2,1)S(1)}, u32[]{:S(2)}, u32[]{:S(2)}) collective-permute-start(bf16[128,128]{1,0:T(8,128)(2,1)S(1)} %get-tuple-element.19), channel_id=1, source_target_pairs={{32,0},{64,32},{96,64},{128,96},{160,128},{192,160},{224,192},{256... | collective-permute-start | bytes 98312 | tf_op jit(solution)/shard_map/halo/ppermute | solution.py:315

commit v5 on v4

--- a/solution.py
+++ b/solution.py
@@ -126,10 +126,18 @@
         out_ref[start : start + n, cols] = y.astype(bf16)
 
 
-def ctx_kernel(x_ref, mean_ref, rstd_ref, rows_ref, wkv_ref, out_ref, normed):
-    modulate(x_ref, mean_ref, rstd_ref, rows_ref, 1, normed, 0)
-    kv = dot_nt(normed[...], wkv_ref[...]).astype(bf16)
-    out_ref[...] = jnp.broadcast_to(kv[None], out_ref.shape)
+def ctx_kernel(x_ref, mean_ref, rstd_ref, rows_ref, wkv_ref, out_ref):
+    acc = jnp.zeros((x_ref.shape[0], LANES), f32)
+    for m in range(0, x_ref.shape[1] // LANES, 2):
+        parts = []
+        for k in (m, m + 1):
+            shift, scale = mod_tile(rows_ref, 1, k)
+            x = x_ref[:, k * LANES : (k + 1) * LANES].astype(f32)
+            y = (x - mean_ref[...]) * rstd_ref[...] * scale + shift
+            parts.append(y.astype(bf16))
+        wide = slice(m * LANES, (m + 2) * LANES)
+        acc = acc + dot_nt(jnp.concatenate(parts, axis=1), wkv_ref[:, wide])
+    out_ref[...] = jnp.broadcast_to(acc.astype(bf16)[None], out_ref.shape)
 
 
 def turned(u, cos, sin):
@@ -143,12 +151,18 @@
 
 
 def project_kernel(
-    x_ref, mean_ref, rstd_ref, rows_ref, wq_ref, wkv_ref, cos_ref, sin_ref,
-    q_ref, kv_ref, head_ref, tail_ref, normed,
+    x_ref, mean_ref, rstd_ref, rows_ref, wq_ref, wkv_ref, row_ref, col_ref,
+    q_ref, kv_ref, head_ref, tail_ref, normed, cos_s, sin_s,
 ):
     n = x_ref.shape[0]
     modulate(x_ref, mean_ref, rstd_ref, rows_ref, 0, normed, 0)
-    cos, sin = cos_ref[...], sin_ref[...]
+    by_row = lanes_of((GRID_W, LANES)) % HEAD < HEAD // 2
+    first = lax.axis_index("sp") * (n // GRID_W)
+    for g in range(n // GRID_W):
+        at = slice(g * GRID_W, (g + 1) * GRID_W)
+        cos_s[at, :] = jnp.where(by_row, row_ref[0, pl.ds(first + g, 1), :], col_ref[0])
+        sin_s[at, :] = jnp.where(by_row, row_ref[1, pl.ds(first + g, 1), :], col_ref[1])
+    cos, sin = cos_s[...], sin_s[...]
     low = lanes_of((n, LANES)) < HEAD
     kv = dot_nt(normed[...], wkv_ref[...])
     kv = turned(kv, jnp.where(low, cos, 1.0), jnp.where(low, sin, 0.0)).astype(bf16)
@@ -220,34 +234,34 @@
                 out_ref[k, at, pair * LANES : (pair + 1) * LANES] = both
 
 
-def out_kernel(att_ref, w_ref, x_ref, rows_ref, out_ref):
-    sources, n, width = att_ref.shape
+def out_kernel(att_ref, w_ref, x_ref, rows_ref, out_ref, ready, sems):
+    sources, n, _ = att_ref.shape
     t = lax.axis_index("tp")
-    mixed = jnp.dot(att_ref[0], w_ref[0:width, :], preferred_element_type=f32)
-    for k in range(1, sources):
-        mixed = mixed + jnp.dot(
-            att_ref[k], w_ref[k * width : (k + 1) * width, :], preferred_element_type=f32
-        )
     low = lanes_of((1, LANES)) < 64
-    for m in range(out_ref.shape[1] // LANES):
-        cols = slice(m * LANES, (m + 1) * LANES)
-        a = rows_ref[t * 8 + 2 * m, 2:3, :]
-        b = rows_ref[t * 8 + 2 * m + 1, 2:3, :]
-        gate = jnp.where(low, a, pltpu.roll(b, 64, 1))
-        out_ref[:, cols] = x_ref[:, cols].astype(f32) + gate * mixed[:, cols]
-
-
-def rotary_tables(rows, start):
+    copies = []
+    for i in range(n // REACH):
+        at = slice(i * REACH, (i + 1) * REACH)
+        att = jnp.concatenate([att_ref[k, at, :] for k in range(sources)], axis=1)
+        mixed = jnp.dot(att, w_ref[...], preferred_element_type=f32)
+        for m in range(out_ref.shape[1] // LANES):
+            cols = slice(m * LANES, (m + 1) * LANES)
+            a = rows_ref[t * 8 + 2 * m, 2:3, :]
+            b = rows_ref[t * 8 + 2 * m + 1, 2:3, :]
+            gate = jnp.where(low, a, pltpu.roll(b, 64, 1))
+            ready[at, cols] = x_ref[at, cols].astype(f32) + gate * mixed[:, cols]
+        copy = pltpu.make_async_copy(ready.at[at], out_ref.at[at], sems.at[i])
+        copy.start()
+        copies.append(copy)
+    for copy in copies:
+        copy.wait()
+
+
+def rotary_table(places):
     lane = np.arange(LANES)
-    freq = ROTARY_BASE ** (-np.arange(0, 32, 2, dtype=np.float32) / 32)
-    freq = jnp.asarray(freq[lane % 16].astype(np.float32))
-    by_row = jnp.asarray(lane % 64 < 32)
-    sign = jnp.asarray(np.where(lane % 32 < 16, -1.0, 1.0).astype(np.float32))
-    position = start + jnp.arange(rows, dtype=jnp.int32)
-    row, col = position // GRID_W, position % GRID_W
-    place = jnp.where(by_row[None, :], row[:, None], col[:, None]).astype(f32)
-    angle = place * freq[None, :]
-    return jnp.cos(angle), jnp.sin(angle) * sign[None, :]
+    freq = (ROTARY_BASE ** (-np.arange(0, 32, 2, dtype=np.float32) / 32)).astype(np.float32)
+    angle = np.arange(places, dtype=np.float32)[:, None] * freq[lane % 16][None, :]
+    sign = np.where(lane % 32 < 16, -1.0, 1.0)
+    return np.stack([np.cos(angle), np.sin(angle) * sign[None, :]]).astype(np.float32)
 
 
 def per_device(
@@ -273,23 +287,24 @@
         in_hbm(x), in_hbm(ctx)
     )
     wkv = jnp.concatenate([key_projection.T, value_projection.T], axis=0)
-    cos, sin = rotary_tables(n, lax.axis_index("sp") * n)
+    by_row = jnp.asarray(rotary_table(sp * n // GRID_W))
+    by_col = jnp.asarray(rotary_table(GRID_W))
     cols = out_weight.shape[1]
     own = lax.dynamic_slice_in_dim(x, lax.axis_index("tp") * cols, cols, 1)
     send = call(
         rows_kernel,
         jax.ShapeDtypeStruct((spread, 4, LANES), f32),
-        [VMEM] + [ANY] * 5,
+        [VMEM] + [ANY] * 3,
         [pltpu.VMEM((PARTIAL_ROWS, LANES), f32)],
         2,
-    )(partials, cmean, wkv, cos, sin, own)
+    )(partials, cmean, wkv, own)
     with jax.named_scope("spread"):
         rows = lax.all_to_all(send, ("tp", "dp"), 0, 0, tiled=True)
     ctx_kv = call(
         ctx_kernel,
         jax.ShapeDtypeStruct((sp, ctx.shape[0], LANES), bf16),
         [VMEM] * 5,
-        [pltpu.VMEM(ctx.shape, bf16)],
+        [],
         4,
     )(ctx, cmean, crstd, rows, wkv)
     with jax.named_scope("context"):
@@ -305,9 +320,13 @@
             edge,
         ),
         [VMEM] * 8,
-        [pltpu.VMEM(x.shape, bf16)],
-        6,
-    )(in_hbm(x), mean, rstd, rows, in_hbm(query_weight), wkv, cos, sin)
+        [
+            pltpu.VMEM(x.shape, bf16),
+            pltpu.VMEM((n, LANES), f32),
+            pltpu.VMEM((n, LANES), f32),
+        ],
+        7,
+    )(in_hbm(x), mean, rstd, rows, in_hbm(query_weight), wkv, by_row, by_col)
     up = [(i, i + 1) for i in range(sp - 1)]
     down = [(i + 1, i) for i in range(sp - 1)]
     with jax.named_scope("halo"):
@@ -330,9 +349,14 @@
     )(q, win, ctx_all, sink_head_logit, prefix_logit_bias, out_weight)
     with jax.named_scope("heads"):
         every = lax.all_to_all(attended, "tp", 0, 0, tiled=True)
-    out = call(out_kernel, jax.ShapeDtypeStruct((n, cols), f32), [VMEM] * 4, (), 8)(
-        every, out_weight, own, rows
-    )
+    out = call(
+        out_kernel,
+        pltpu.HBM((n, cols), f32),
+        [VMEM] * 4,
+        [pltpu.VMEM((n, cols), f32), pltpu.SemaphoreType.DMA((n // REACH,))],
+        8,
+        ANY,
+    )(every, out_weight, own, rows)
     return out[None]
 
 

time: 88.9 us -> 88.2 us (level)
  waiting for transfers between devices: 15 us -> 16.9 us
  other arithmetic: 1.61 us -> 0.04 us
  starting transfers between devices: 26.2 us -> 25.3 us
    all_to_all x1, waiting for transfers between devices: 7.05 us -> 8.64 us  [per_device(): partials = lax.all_to_all(partial, 'sp', 0, 0, tiled=True)]
    mul x1 -> x0, other arithmetic: 1.55 us -> none  [rotary_tables(): return (jnp.cos(angle), jnp.sin(angle) * sign[None, :])]
  transfers between devices with their start and end apart: 4 -> 4, of which waited for: 4 -> 4; matrix products, arithmetic and copies ran while one was open for 3% -> 1% of each run, Pallas kernels for 9% -> 9%
where the time goes in v5:
time: 88.2 us; the launch traced here: 87.8 us
  blocking collectives  28.9 us (33%)
  starting transfers between devices  25.3 us (29%)
  waiting for transfers between devices  16.9 us (19%)
  Pallas kernels  15.4 us (17%)
  local copies, waits for them, and re-layouts  1.11 us (1%)
    all_to_all x1, starting transfers between devices, per_device(): partials = lax.all_to_all(partial, 'sp', 0, 0, tiled=True)  15.2 us
    all_to_all x1, blocking collectives, per_device(): rows = lax.all_to_all(send, ('tp', 'dp'), 0, 0, tiled=True)  14.6 us
    all_to_all x1, blocking collectives, per_device(): every = lax.all_to_all(attended, 'tp', 0, 0, tiled=True)  14.3 us
    all_to_all x1, waiting for transfers between devices, per_device(): partials = lax.all_to_all(partial, 'sp', 0, 0, tiled=True)  8.64 us
    all_to_all x1, waiting for transfers between devices, per_device(): ctx_all = lax.all_to_all(ctx_kv, 'sp', 0, 0, tiled=True).reshape(-1, LANES)  4.36 us
    all_to_all x1, starting transfers between devices, per_device(): ctx_all = lax.all_to_all(ctx_kv, 'sp', 0, 0, tiled=True).reshape(-1, LANES)  4.14 us
    pallas_call x1, Pallas kernels, per_device(): call(attend_kernel, jax.ShapeDtypeStruct((tp, n, heads * HEAD), bf16), [V...  3.56 us
    ppermute x1, starting transfers between devices, per_device(): before = lax.ppermute(last, 'sp', up)  3.51 us
  transfers between devices with their start and end apart: 4, of which 4 were waited for; matrix products, arithmetic and copies ran while one was open for 1% of the time, Pallas kernels for 9%

profile of v5, /device:TPU:32, one launch (start us, length us, event | category | flops | bytes accessed | tf_op | source)
XLA Modules:
  0.0 87.8 jit_solution(14569176701370878752)
XLA Ops:
  0.0 1.8 %shard_map.128 = bf16[16,24,128]{2,1,0:T(8,128)(2,1)} custom-call(bf16[8,128]{1,0:T(8,128)(2,1)} %cond_ref.1, bf16[1,128]{1,0:T(2,128)(2,1)} %bitcast.18, bf16[3,64,128]{2,1,0:T(8,128)(2,1)} %bitcast.17), custom_call_target="tpu_custom_call" | custom-call | tf_op jit(solution)/shard_map/pallas_call | solution.py:275
  1.8 15.2 %all-to-all-start = ((bf16[16,24,128]{2,1,0:T(8,128)(2,1)}), bf16[16,24,128]{2,1,0:T(8,128)(2,1)S(1)}, u32[]{:S(2)}, u32[]{:S(2)}) async-start(bf16[16,24,128]{2,1,0:T(8,128)(2,1)} %shard_map.128), calls=%async_computation | async-start | bytes 196608 | tf_op jit(solution)/shard_map/sums/all_to_all | solution.py:283
  17.0 3.2 %shard_map.127 = (f32[384,128]{1,0:T(8,128)S(1)}, f32[384,128]{1,0:T(8,128)S(1)}, f32[64,128]{1,0:T(8,128)S(1)}, f32[64,128]{1,0:T(8,128)S(1)}) custom-call(bf16[384,2048]{1,0:T(8,128)(2,1)} %bitcast.13, bf16[64,2048]{1,0:T(8,128)(2,1)} %bitcast.11), custom_call_target="tpu_custom_call" | custom-call | tf_op jit(solution)/shard_map/pallas_call | solution.py:286
  20.2 0.0 copy-start.1
  20.2 1.1 %dynamic-slice_bitcast_fusion.refs_2_.x_ref = bf16[384,512]{1,0:T(8,128)(2,1)S(1)} fusion(bf16[1,384,2048]{2,1,0:T(8,128)(2,1)} %param.13, s32[]{:T(128)S(6)} %select_n.3), kind=kLoop, calls=%fused_computation.1 | loop fusion | bytes 786436 | tf_op jit(solution)/shard_map/dynamic_slice | solution.py:293
  21.2 0.0 copy-done.6
  21.3 0.0 copy-done.7
  21.3 0.0 copy-start.2
  21.3 0.0 copy-start.3
  21.3 8.6 %all-to-all-done.in_ref = bf16[16,24,128]{2,1,0:T(8,128)(2,1)S(1)} async-done(((bf16[16,24,128]{2,1,0:T(8,128)(2,1)}), bf16[16,24,128]{2,1,0:T(8,128)(2,1)S(1)}, u32[]{:S(2)}, u32[]{:S(2)}) %all-to-all-start) | async-done | bytes 98336 | tf_op jit(solution)/shard_map/sums/all_to_all | solution.py:283
  30.0 0.1 shard_map.129
  30.1 14.6 %all_to_all.20.rows_ref = f32[32,4,128]{2,1,0:T(4,128)S(1)} all-to-all(f32[32,4,128]{2,1,0:T(4,128)S(1)} %shard_map.129), channel_id=1, replica_groups=mesh['sp'=16,'tp'=4,'dp'=8] {'tp','dp'}, dimensions={0} | all-to-all | bytes 131072 | tf_op jit(solution)/shard_map/spread/all_to_all | solution.py:302
  44.7 0.0 copy-done.1
  44.7 1.1 %shard_map.132 = bf16[16,64,128]{2,1,0:T(8,128)(2,1)} custom-call(bf16[64,2048]{1,0:T(8,128)(2,1)S(1)} %bitcast.12, f32[64,128]{1,0:T(8,128)S(1)} %get-tuple-element.15.refs_0_.mean_ref, f32[64,128]{1,0:T(8,128)S(1)} %get-tuple-element.20.rstd_ref, f32[32,4,128]{2,1,0:T(4,128)S(1)} %all_to_all.20.rows_ref, bf16[128,2048]{1,0:T(8,128)(2,1)S(1)} %pad_maximum_fusion.refs_1_.wkv_ref), custom_call_target="tpu_custom_call" | custom-call | tf_op jit(solution)/shard_map/pallas_call | solution.py:303
  45.7 4.1 %all-to-all-start.2 = ((bf16[16,64,128]{2,1,0:T(8,128)(2,1)}), bf16[16,64,128]{2,1,0:T(8,128)(2,1)S(1)}, u32[]{:S(2)}, u32[]{:S(2)}) async-start(bf16[16,64,128]{2,1,0:T(8,128)(2,1)} %shard_map.132), calls=%async_computation.2 | async-start | bytes 524288 | tf_op jit(solution)/shard_map/context/all_to_all | solution.py:311
  49.9 0.0 copy-done.2
  49.9 0.0 copy-done.3
  49.9 0.0 copy-start.4
  49.9 0.0 copy-start.5
  49.9 3.1 %shard_map.130 = (bf16[4,384,128]{2,1,0:T(8,128)(2,1)S(1)}, bf16[384,128]{1,0:T(8,128)(2,1)S(1)}, bf16[128,128]{1,0:T(8,128)(2,1)S(1)}, bf16[128,128]{1,0:T(8,128)(2,1)S(1)}) custom-call(bf16[384,2048]{1,0:T(8,128)(2,1)} %bitcast.14, f32[384,128]{1,0:T(8,128)S(1)} %get-tuple-element.13.mean_ref, f32[384,128]{1,0:T(8,128)S(1)} %get-tuple-element.14.rstd_ref, ...), custom_call_target="tpu_custom_call" | custom-call | tf_op jit(solution)/shard_map/pallas_call | solution.py:314
  53.0 3.5 %collective-permute-start = (bf16[128,128]{1,0:T(8,128)(2,1)S(1)}, bf16[128,128]{1,0:T(8,128)(2,1)S(1)}, u32[]{:S(2)}, u32[]{:S(2)}) collective-permute-start(bf16[128,128]{1,0:T(8,128)(2,1)S(1)} %get-tuple-element.18), channel_id=1, source_target_pairs={{0,32},{32,64},{64,96},{96,128},{128,160},{160,192},{192,224},{224... | collective-permute-start | bytes 98312 | tf_op jit(solution)/shard_map/halo/ppermute | solution.py:333
  56.5 2.5 %collective-permute-start.1 = (bf16[128,128]{1,0:T(8,128)(2,1)S(1)}, bf16[128,128]{1,0:T(8,128)(2,1)S(1)}, u32[]{:S(2)}, u32[]{:S(2)}) collective-permute-start(bf16[128,128]{1,0:T(8,128)(2,1)S(1)} %get-tuple-element.19), channel_id=1, source_target_pairs={{32,0},{64,32},{96,64},{128,96},{160,128},{192,160},{224,192},{256... | collective-permute-start | bytes 98312 | tf_op jit(solution)/shard_map/halo/ppermute | solution.py:334
  59.0 2.0 %collective-permute-done.before_ref = bf16[128,128]{1,0:T(8,128)(2,1)S(1)} collective-permute-done((bf16[128,128]{1,0:T(8,128)(2,1)S(1)}, bf16[128,128]{1,0:T(8,128)(2,1)S(1)}, u32[]{:S(2)}, u32[]{:S(2)}) %collective-permute-start) | collective-permute-done | bytes 32800 | tf_op jit(solution)/shard_map/halo/ppermute | solution.py:333
  61.0 1.9 %collective-permute-done.1.after_ref = bf16[128,128]{1,0:T(8,128)(2,1)S(1)} collective-permute-done((bf16[128,128]{1,0:T(8,128)(2,1)S(1)}, bf16[128,128]{1,0:T(8,128)(2,1)S(1)}, u32[]{:S(2)}, u32[]{:S(2)}) %collective-permute-start.1) | collective-permute-done | bytes 32800 | tf_op jit(solution)/shard_map/halo/ppermute | solution.py:334
  62.9 1.3 %shard_map.131.win_ref = f32[4,384,128]{2,1,0:T(8,128)S(1)} custom-call(bf16[4,384,128]{2,1,0:T(8,128)(2,1)S(1)} %get-tuple-element.16.q_ref, bf16[384,128]{1,0:T(8,128)(2,1)S(1)} %get-tuple-element.17.kv_ref, bf16[128,128]{1,0:T(8,128)(2,1)S(1)} %collective-permute-done.before_ref, bf16[128,128]{1,0:T(8,128)(2,1)S(1)} %collective-permute-done.1.after_ref), custom_call_target="tpu_custom_call" | custom-call | tf_op jit(solution)/shard_map/pallas_call | solution.py:336
  64.2 4.4 %all-to-all-done.2 = bf16[16,64,128]{2,1,0:T(8,128)(2,1)S(1)} async-done(((bf16[16,64,128]{2,1,0:T(8,128)(2,1)}), bf16[16,64,128]{2,1,0:T(8,128)(2,1)S(1)}, u32[]{:S(2)}, u32[]{:S(2)}) %all-to-all-start.2) | async-done | bytes 262176 | tf_op jit(solution)/shard_map/context/all_to_all | solution.py:311
  68.6 0.0 copy-done.4
  68.6 0.0 copy-done.5
  68.6 0.0 copy-done
  68.6 3.6 %shard_map.133 = bf16[4,384,256]{2,1,0:T(8,128)(2,1)S(1)} custom-call(bf16[4,384,128]{2,1,0:T(8,128)(2,1)S(1)} %get-tuple-element.16.q_ref, f32[4,384,128]{2,1,0:T(8,128)S(1)} %shard_map.131.win_ref, bf16[1024,128]{1,0:T(8,128)(2,1)S(1)} %bitcast.10, f32[4]{0:T(128)S(1)} %copy-done.4, f32[4]{0:T(128)S(1)} %copy-done.5, bf16[1024,512]{1,0:T(8,128)(2,1)S(1)} %copy-done), custom_call_target="tpu_custom_call" | custom-call | tf_op jit(solution)/shard_map/pallas_call | solution.py:343
  72.1 14.3 %all_to_all.21.att_ref = bf16[4,384,256]{2,1,0:T(8,128)(2,1)S(1)} all-to-all(bf16[4,384,256]{2,1,0:T(8,128)(2,1)S(1)} %shard_map.133), channel_id=1, replica_groups=mesh['sp'=16,'tp'=4,'dp'=8] {'tp'}, dimensions={0} | all-to-all | bytes 1572864 | tf_op jit(solution)/shard_map/heads/all_to_all | solution.py:351
  86.5 1.3 %shard_map.134 = f32[384,512]{1,0:T(8,128)} custom-call(bf16[4,384,256]{2,1,0:T(8,128)(2,1)S(1)} %all_to_all.21.att_ref, bf16[1024,512]{1,0:T(8,128)(2,1)S(1)} %copy-done, bf16[384,512]{1,0:T(8,128)(2,1)S(1)} %dynamic-slice_bitcast_fusion.refs_2_.x_ref, f32[32,4,128]{2,1,0:T(4,128)S(1)} %all_to_all.20.rows_ref), custom_call_target="tpu_custom_call" | custom-call | tf_op jit(solution)/shard_map/pallas_call | solution.py:352
  (4 shorter events, 0.0 us)
Async XLA Ops:
  0.0 21.2 %copy-start.6 = (bf16[2048,64]{0,1:T(8,128)(2,1)S(1)}, bf16[2048,64]{0,1:T(8,128)(2,1)}, u32[]{:S(2)}) copy-start(bf16[2048,64]{0,1:T(8,128)(2,1)} %param.20) | copy-start | bytes 786436
  0.0 21.3 %copy-start.7 = (bf16[2048,64]{0,1:T(8,128)(2,1)S(1)}, bf16[2048,64]{0,1:T(8,128)(2,1)}, u32[]{:S(2)}) copy-start(bf16[2048,64]{0,1:T(8,128)(2,1)} %param.19) | copy-start | bytes 786436
  1.8 28.2 %all-to-all-start = ((bf16[16,24,128]{2,1,0:T(8,128)(2,1)}), bf16[16,24,128]{2,1,0:T(8,128)(2,1)S(1)}, u32[]{:S(2)}, u32[]{:S(2)}) async-start(bf16[16,24,128]{2,1,0:T(8,128)(2,1)} %shard_map.128), calls=%async_computation | async-start | bytes 196608 | tf_op jit(solution)/shard_map/sums/all_to_all | solution.py:283
  20.2 24.5 %copy-start.1 = (bf16[1,64,2048]{2,1,0:T(8,128)(2,1)S(1)}, bf16[1,64,2048]{2,1,0:T(8,128)(2,1)}, u32[]{:S(2)}) copy-start(bf16[1,64,2048]{2,1,0:T(8,128)(2,1)} %param.17) | copy-start | bytes 786436
  21.3 28.6 %copy-start.2 = (f32[2,96,128]{2,1,0:T(8,128)S(1)}, f32[2,96,128]{2,1,0:T(8,128)}, u32[]{:S(2)}) copy-start(f32[2,96,128]{2,1,0:T(8,128)} %constant.16.clone.row_ref) | copy-start | bytes 294916
  21.3 28.6 %copy-start.3 = (f32[2,64,128]{2,1,0:T(8,128)S(1)}, f32[2,64,128]{2,1,0:T(8,128)}, u32[]{:S(2)}) copy-start(f32[2,64,128]{2,1,0:T(8,128)} %constant.17.clone.col_ref) | copy-start | bytes 196612
  45.7 22.8 %all-to-all-start.2 = ((bf16[16,64,128]{2,1,0:T(8,128)(2,1)}), bf16[16,64,128]{2,1,0:T(8,128)(2,1)S(1)}, u32[]{:S(2)}, u32[]{:S(2)}) async-start(bf16[16,64,128]{2,1,0:T(8,128)(2,1)} %shard_map.132), calls=%async_computation.2 | async-start | bytes 524288 | tf_op jit(solution)/shard_map/context/all_to_all | solution.py:311
  49.9 18.7 %copy-start.4 = (f32[4]{0:T(128)S(1)}, f32[4]{0:T(128)}, u32[]{:S(2)}) copy-start(f32[4]{0:T(128)} %sink_ref.1) | copy-start | bytes 52
  49.9 18.7 %copy-start.5 = (f32[4]{0:T(128)S(1)}, f32[4]{0:T(128)}, u32[]{:S(2)}) copy-start(f32[4]{0:T(128)} %bias_ref.1) | copy-start | bytes 52
  53.0 15.6 %copy-start = (bf16[1024,512]{1,0:T(8,128)(2,1)S(1)}, bf16[1024,512]{1,0:T(8,128)(2,1)}, u32[]{:S(2)}) copy-start(bf16[1024,512]{1,0:T(8,128)(2,1)} %w_ref.1) | copy-start | bytes 3145732
  53.0 7.9 %collective-permute-start = (bf16[128,128]{1,0:T(8,128)(2,1)S(1)}, bf16[128,128]{1,0:T(8,128)(2,1)S(1)}, u32[]{:S(2)}, u32[]{:S(2)}) collective-permute-start(bf16[128,128]{1,0:T(8,128)(2,1)S(1)} %get-tuple-element.18), channel_id=1, source_target_pairs={{0,32},{32,64},{64,96},{96,128},{128,160},{160,192},{192,224},{224... | collective-permute-start | bytes 98312 | tf_op jit(solution)/shard_map/halo/ppermute | solution.py:333
  56.5 6.3 %collective-permute-start.1 = (bf16[128,128]{1,0:T(8,128)(2,1)S(1)}, bf16[128,128]{1,0:T(8,128)(2,1)S(1)}, u32[]{:S(2)}, u32[]{:S(2)}) collective-permute-start(bf16[128,128]{1,0:T(8,128)(2,1)S(1)} %get-tuple-element.19), channel_id=1, source_target_pairs={{32,0},{64,32},{96,64},{128,96},{160,128},{192,160},{224,192},{256... | collective-permute-start | bytes 98312 | tf_op jit(solution)/shard_map/halo/ppermute | solution.py:334

commit v6 on v5

--- a/solution.py
+++ b/solution.py
@@ -205,31 +205,62 @@
         win_ref[:, b * REACH : (b + 1) * REACH, :] = acc.reshape(heads, REACH, LANES)
 
 
+def top_of(s):
+    m = s[:, 0:LANES]
+    for k in range(1, s.shape[1] // LANES):
+        m = jnp.maximum(m, s[:, k * LANES : (k + 1) * LANES])
+    return jnp.max(m, axis=1, keepdims=True)
+
+
 def attend_kernel(q_ref, win_ref, ctx_ref, sink_ref, bias_ref, _, out_ref, ones_s):
     heads, n, _ = q_ref.shape
     kv = ctx_ref[...]
     ones_s[...] = with_ones(kv)
-    rows = heads * REACH
     lane = lanes_of((REACH, LANES))
-    head = lax.broadcasted_iota(jnp.int32, (rows, 1), 0) // REACH
-    bias, sink = jnp.zeros((rows, 1), f32), jnp.zeros((rows, 1), f32)
-    for h in range(heads):
-        bias = jnp.where(head == h, bias_ref[h], bias)
-        sink = jnp.where(head == h, sink_ref[h], sink)
-    for b in range(n // REACH):
+
+    sub = 2
+    rows = sub * REACH
+    def part(x, fill):
+        head = lax.broadcasted_iota(jnp.int32, (rows, 1), 0) // REACH
+        out = jnp.zeros((rows, 1), f32)
+        for h in range(sub):
+            out = jnp.where(head == h, x[fill + h], out)
+        return out
+    units = [(b, g) for b in range(n // REACH) for g in range(heads // sub)]
+    biases = [part(bias_ref, g * sub) for g in range(heads // sub)]
+    sinks = [part(sink_ref, g * sub) for g in range(heads // sub)]
+    def score(u):
+        b, g = u
         at = slice(b * REACH, (b + 1) * REACH)
-        s = dot_nt(q_ref[:, at, :].reshape(rows, LANES), kv)
-        win = win_ref[:, at, :].reshape(rows, LANES)
+        q = q_ref[g * sub : (g + 1) * sub, at, :].reshape(rows, LANES)
+        return dot_nt(q, ctx_ref[...])
+    ahead = 2
+    queue = [score(u) for u in units[:ahead]]
+    done = []
+    for i, (b, g) in enumerate(units):
+        if ahead == 0:
+            s = score((b, g))
+        else:
+            s = queue.pop(0)
+            if i + ahead < len(units):
+                queue.append(score(units[i + ahead]))
+        at = slice(b * REACH, (b + 1) * REACH)
+        win = win_ref[g * sub : (g + 1) * sub, at, :].reshape(rows, LANES)
         win_top = win[:, 0:1]
-        top = jnp.maximum(jnp.max(s, axis=1, keepdims=True) + bias, jnp.maximum(win_top, sink))
+        bias, sink = biases[g], sinks[g]
+        top = jnp.maximum(top_of(s) + bias, jnp.maximum(win_top, sink))
         p = jnp.exp(s - (top - bias)).astype(bf16)
-        acc = jnp.dot(p, ones_s[...], preferred_element_type=f32)
-        acc = acc + win * jnp.exp(win_top - top)
-        den = acc[:, 1:2] + jnp.exp(sink - top)
-        acc = (acc / den).reshape(heads, REACH, LANES)
+        acc = jnp.dot(p, ones_s[...], preferred_element_type=f32) + win * jnp.exp(win_top - top)
+        acc = (acc * (1.0 / (acc[:, 1:2] + jnp.exp(sink - top)))).reshape(sub, REACH, LANES)
+        if g == 0:
+            done = []
+        done.extend(acc[h] for h in range(sub))
+        if g < heads // sub - 1:
+            continue
+
         for pair in range(heads // 2):
-            even = pltpu.roll(acc[2 * pair], HEAD, 1)
-            both = jnp.where(lane < HEAD, even, acc[2 * pair + 1]).astype(bf16)
+            even = pltpu.roll(done[2 * pair], HEAD, 1)
+            both = jnp.where(lane < HEAD, even, done[2 * pair + 1]).astype(bf16)
             for k in range(out_ref.shape[0]):
                 out_ref[k, at, pair * LANES : (pair + 1) * LANES] = both
 

time: 88.2 us -> 87.9 us (level)
  no operation moved by 1% of the time
where the time goes in v6:
time: 87.9 us; the launch traced here: 87.4 us
  blocking collectives  28.9 us (33%)
  starting transfers between devices  25.3 us (29%)
  waiting for transfers between devices  16.9 us (19%)
  Pallas kernels  15 us (17%)
  local copies, waits for them, and re-layouts  1.11 us (1%)
    all_to_all x1, starting transfers between devices, per_device(): partials = lax.all_to_all(partial, 'sp', 0, 0, tiled=True)  15.2 us
    all_to_all x1, blocking collectives, per_device(): rows = lax.all_to_all(send, ('tp', 'dp'), 0, 0, tiled=True)  14.6 us
    all_to_all x1, blocking collectives, per_device(): every = lax.all_to_all(attended, 'tp', 0, 0, tiled=True)  14.3 us
    all_to_all x1, waiting for transfers between devices, per_device(): partials = lax.all_to_all(partial, 'sp', 0, 0, tiled=True)  8.64 us
    all_to_all x1, waiting for transfers between devices, per_device(): ctx_all = lax.all_to_all(ctx_kv, 'sp', 0, 0, tiled=True).reshape(-1, LANES)  4.36 us
    all_to_all x1, starting transfers between devices, per_device(): ctx_all = lax.all_to_all(ctx_kv, 'sp', 0, 0, tiled=True).reshape(-1, LANES)  4.14 us
    ppermute x1, starting transfers between devices, per_device(): before = lax.ppermute(last, 'sp', up)  3.51 us
    pallas_call x1, Pallas kernels, per_device(): call(attend_kernel, jax.ShapeDtypeStruct((tp, n, heads * HEAD), bf16), [V...  3.22 us
  transfers between devices with their start and end apart: 4, of which 4 were waited for; matrix products, arithmetic and copies ran while one was open for 1% of the time, Pallas kernels for 9%

profile of v6, /device:TPU:32, one launch (start us, length us, event | category | flops | bytes accessed | tf_op | source)
XLA Modules:
  0.0 87.4 jit_solution(11020525289889704348)
XLA Ops:
  0.0 1.8 %shard_map.128 = bf16[16,24,128]{2,1,0:T(8,128)(2,1)} custom-call(bf16[8,128]{1,0:T(8,128)(2,1)} %cond_ref.1, bf16[1,128]{1,0:T(2,128)(2,1)} %bitcast.18, bf16[3,64,128]{2,1,0:T(8,128)(2,1)} %bitcast.17), custom_call_target="tpu_custom_call" | custom-call | tf_op jit(solution)/shard_map/pallas_call | solution.py:306
  1.8 15.2 %all-to-all-start = ((bf16[16,24,128]{2,1,0:T(8,128)(2,1)}), bf16[16,24,128]{2,1,0:T(8,128)(2,1)S(1)}, u32[]{:S(2)}, u32[]{:S(2)}) async-start(bf16[16,24,128]{2,1,0:T(8,128)(2,1)} %shard_map.128), calls=%async_computation | async-start | bytes 196608 | tf_op jit(solution)/shard_map/sums/all_to_all | solution.py:314
  17.0 3.2 %shard_map.127 = (f32[384,128]{1,0:T(8,128)S(1)}, f32[384,128]{1,0:T(8,128)S(1)}, f32[64,128]{1,0:T(8,128)S(1)}, f32[64,128]{1,0:T(8,128)S(1)}) custom-call(bf16[384,2048]{1,0:T(8,128)(2,1)} %bitcast.13, bf16[64,2048]{1,0:T(8,128)(2,1)} %bitcast.11), custom_call_target="tpu_custom_call" | custom-call | tf_op jit(solution)/shard_map/pallas_call | solution.py:317
  20.2 0.0 copy-start.1
  20.2 1.1 %dynamic-slice_bitcast_fusion.refs_2_.x_ref = bf16[384,512]{1,0:T(8,128)(2,1)S(1)} fusion(bf16[1,384,2048]{2,1,0:T(8,128)(2,1)} %param.13, s32[]{:T(128)S(6)} %select_n.3), kind=kLoop, calls=%fused_computation.1 | loop fusion | bytes 786436 | tf_op jit(solution)/shard_map/dynamic_slice | solution.py:324
  21.2 0.0 copy-done.6
  21.3 0.0 copy-done.7
  21.3 0.0 copy-start.2
  21.3 0.0 copy-start.3
  21.3 8.6 %all-to-all-done.in_ref = bf16[16,24,128]{2,1,0:T(8,128)(2,1)S(1)} async-done(((bf16[16,24,128]{2,1,0:T(8,128)(2,1)}), bf16[16,24,128]{2,1,0:T(8,128)(2,1)S(1)}, u32[]{:S(2)}, u32[]{:S(2)}) %all-to-all-start) | async-done | bytes 98336 | tf_op jit(solution)/shard_map/sums/all_to_all | solution.py:314
  30.0 0.1 shard_map.129
  30.1 14.6 %all_to_all.20.rows_ref = f32[32,4,128]{2,1,0:T(4,128)S(1)} all-to-all(f32[32,4,128]{2,1,0:T(4,128)S(1)} %shard_map.129), channel_id=1, replica_groups=mesh['sp'=16,'tp'=4,'dp'=8] {'tp','dp'}, dimensions={0} | all-to-all | bytes 131072 | tf_op jit(solution)/shard_map/spread/all_to_all | solution.py:333
  44.7 0.0 copy-done.1
  44.7 1.1 %shard_map.132 = bf16[16,64,128]{2,1,0:T(8,128)(2,1)} custom-call(bf16[64,2048]{1,0:T(8,128)(2,1)S(1)} %bitcast.12, f32[64,128]{1,0:T(8,128)S(1)} %get-tuple-element.15.refs_0_.mean_ref, f32[64,128]{1,0:T(8,128)S(1)} %get-tuple-element.20.rstd_ref, f32[32,4,128]{2,1,0:T(4,128)S(1)} %all_to_all.20.rows_ref, bf16[128,2048]{1,0:T(8,128)(2,1)S(1)} %pad_maximum_fusion.refs_1_.wkv_ref), custom_call_target="tpu_custom_call" | custom-call | tf_op jit(solution)/shard_map/pallas_call | solution.py:334
  45.7 4.1 %all-to-all-start.2 = ((bf16[16,64,128]{2,1,0:T(8,128)(2,1)}), bf16[16,64,128]{2,1,0:T(8,128)(2,1)S(1)}, u32[]{:S(2)}, u32[]{:S(2)}) async-start(bf16[16,64,128]{2,1,0:T(8,128)(2,1)} %shard_map.132), calls=%async_computation.2 | async-start | bytes 524288 | tf_op jit(solution)/shard_map/context/all_to_all | solution.py:342
  49.9 0.0 copy-done.2
  49.9 0.0 copy-done.3
  49.9 0.0 copy-start.4
  49.9 0.0 copy-start.5
  49.9 3.1 %shard_map.130 = (bf16[4,384,128]{2,1,0:T(8,128)(2,1)S(1)}, bf16[384,128]{1,0:T(8,128)(2,1)S(1)}, bf16[128,128]{1,0:T(8,128)(2,1)S(1)}, bf16[128,128]{1,0:T(8,128)(2,1)S(1)}) custom-call(bf16[384,2048]{1,0:T(8,128)(2,1)} %bitcast.14, f32[384,128]{1,0:T(8,128)S(1)} %get-tuple-element.13.mean_ref, f32[384,128]{1,0:T(8,128)S(1)} %get-tuple-element.14.rstd_ref, ...), custom_call_target="tpu_custom_call" | custom-call | tf_op jit(solution)/shard_map/pallas_call | solution.py:345
  53.0 3.5 %collective-permute-start = (bf16[128,128]{1,0:T(8,128)(2,1)S(1)}, bf16[128,128]{1,0:T(8,128)(2,1)S(1)}, u32[]{:S(2)}, u32[]{:S(2)}) collective-permute-start(bf16[128,128]{1,0:T(8,128)(2,1)S(1)} %get-tuple-element.18), channel_id=1, source_target_pairs={{0,32},{32,64},{64,96},{96,128},{128,160},{160,192},{192,224},{224... | collective-permute-start | bytes 98312 | tf_op jit(solution)/shard_map/halo/ppermute | solution.py:364
  56.5 2.5 %collective-permute-start.1 = (bf16[128,128]{1,0:T(8,128)(2,1)S(1)}, bf16[128,128]{1,0:T(8,128)(2,1)S(1)}, u32[]{:S(2)}, u32[]{:S(2)}) collective-permute-start(bf16[128,128]{1,0:T(8,128)(2,1)S(1)} %get-tuple-element.19), channel_id=1, source_target_pairs={{32,0},{64,32},{96,64},{128,96},{160,128},{192,160},{224,192},{256... | collective-permute-start | bytes 98312 | tf_op jit(solution)/shard_map/halo/ppermute | solution.py:365
  59.0 2.0 %collective-permute-done.before_ref = bf16[128,128]{1,0:T(8,128)(2,1)S(1)} collective-permute-done((bf16[128,128]{1,0:T(8,128)(2,1)S(1)}, bf16[128,128]{1,0:T(8,128)(2,1)S(1)}, u32[]{:S(2)}, u32[]{:S(2)}) %collective-permute-start) | collective-permute-done | bytes 32800 | tf_op jit(solution)/shard_map/halo/ppermute | solution.py:364
  61.0 1.9 %collective-permute-done.1.after_ref = bf16[128,128]{1,0:T(8,128)(2,1)S(1)} collective-permute-done((bf16[128,128]{1,0:T(8,128)(2,1)S(1)}, bf16[128,128]{1,0:T(8,128)(2,1)S(1)}, u32[]{:S(2)}, u32[]{:S(2)}) %collective-permute-start.1) | collective-permute-done | bytes 32800 | tf_op jit(solution)/shard_map/halo/ppermute | solution.py:365
  62.9 1.3 %shard_map.131.win_ref = f32[4,384,128]{2,1,0:T(8,128)S(1)} custom-call(bf16[4,384,128]{2,1,0:T(8,128)(2,1)S(1)} %get-tuple-element.16.q_ref, bf16[384,128]{1,0:T(8,128)(2,1)S(1)} %get-tuple-element.17.kv_ref, bf16[128,128]{1,0:T(8,128)(2,1)S(1)} %collective-permute-done.before_ref, bf16[128,128]{1,0:T(8,128)(2,1)S(1)} %collective-permute-done.1.after_ref), custom_call_target="tpu_custom_call" | custom-call | tf_op jit(solution)/shard_map/pallas_call | solution.py:367
  64.2 4.4 %all-to-all-done.2 = bf16[16,64,128]{2,1,0:T(8,128)(2,1)S(1)} async-done(((bf16[16,64,128]{2,1,0:T(8,128)(2,1)}), bf16[16,64,128]{2,1,0:T(8,128)(2,1)S(1)}, u32[]{:S(2)}, u32[]{:S(2)}) %all-to-all-start.2) | async-done | bytes 262176 | tf_op jit(solution)/shard_map/context/all_to_all | solution.py:342
  68.6 0.0 copy-done.4
  68.6 0.0 copy-done.5
  68.6 0.0 copy-done
  68.6 3.2 %shard_map.133 = bf16[4,384,256]{2,1,0:T(8,128)(2,1)S(1)} custom-call(bf16[4,384,128]{2,1,0:T(8,128)(2,1)S(1)} %get-tuple-element.16.q_ref, f32[4,384,128]{2,1,0:T(8,128)S(1)} %shard_map.131.win_ref, bf16[1024,128]{1,0:T(8,128)(2,1)S(1)} %bitcast.10, f32[4]{0:T(128)S(1)} %copy-done.4, f32[4]{0:T(128)S(1)} %copy-done.5, bf16[1024,512]{1,0:T(8,128)(2,1)S(1)} %copy-done), custom_call_target="tpu_custom_call" | custom-call | tf_op jit(solution)/shard_map/pallas_call | solution.py:374
  71.8 14.3 %all_to_all.21.att_ref = bf16[4,384,256]{2,1,0:T(8,128)(2,1)S(1)} all-to-all(bf16[4,384,256]{2,1,0:T(8,128)(2,1)S(1)} %shard_map.133), channel_id=1, replica_groups=mesh['sp'=16,'tp'=4,'dp'=8] {'tp'}, dimensions={0} | all-to-all | bytes 1572864 | tf_op jit(solution)/shard_map/heads/all_to_all | solution.py:382
  86.1 1.3 %shard_map.134 = f32[384,512]{1,0:T(8,128)} custom-call(bf16[4,384,256]{2,1,0:T(8,128)(2,1)S(1)} %all_to_all.21.att_ref, bf16[1024,512]{1,0:T(8,128)(2,1)S(1)} %copy-done, bf16[384,512]{1,0:T(8,128)(2,1)S(1)} %dynamic-slice_bitcast_fusion.refs_2_.x_ref, f32[32,4,128]{2,1,0:T(4,128)S(1)} %all_to_all.20.rows_ref), custom_call_target="tpu_custom_call" | custom-call | tf_op jit(solution)/shard_map/pallas_call | solution.py:383
  (4 shorter events, 0.0 us)
Async XLA Ops:
  0.0 21.2 %copy-start.6 = (bf16[2048,64]{0,1:T(8,128)(2,1)S(1)}, bf16[2048,64]{0,1:T(8,128)(2,1)}, u32[]{:S(2)}) copy-start(bf16[2048,64]{0,1:T(8,128)(2,1)} %param.20) | copy-start | bytes 786436
  0.0 21.3 %copy-start.7 = (bf16[2048,64]{0,1:T(8,128)(2,1)S(1)}, bf16[2048,64]{0,1:T(8,128)(2,1)}, u32[]{:S(2)}) copy-start(bf16[2048,64]{0,1:T(8,128)(2,1)} %param.19) | copy-start | bytes 786436
  1.8 28.2 %all-to-all-start = ((bf16[16,24,128]{2,1,0:T(8,128)(2,1)}), bf16[16,24,128]{2,1,0:T(8,128)(2,1)S(1)}, u32[]{:S(2)}, u32[]{:S(2)}) async-start(bf16[16,24,128]{2,1,0:T(8,128)(2,1)} %shard_map.128), calls=%async_computation | async-start | bytes 196608 | tf_op jit(solution)/shard_map/sums/all_to_all | solution.py:314
  20.2 24.5 %copy-start.1 = (bf16[1,64,2048]{2,1,0:T(8,128)(2,1)S(1)}, bf16[1,64,2048]{2,1,0:T(8,128)(2,1)}, u32[]{:S(2)}) copy-start(bf16[1,64,2048]{2,1,0:T(8,128)(2,1)} %param.17) | copy-start | bytes 786436
  21.3 28.6 %copy-start.2 = (f32[2,96,128]{2,1,0:T(8,128)S(1)}, f32[2,96,128]{2,1,0:T(8,128)}, u32[]{:S(2)}) copy-start(f32[2,96,128]{2,1,0:T(8,128)} %constant.16.clone.row_ref) | copy-start | bytes 294916
  21.3 28.6 %copy-start.3 = (f32[2,64,128]{2,1,0:T(8,128)S(1)}, f32[2,64,128]{2,1,0:T(8,128)}, u32[]{:S(2)}) copy-start(f32[2,64,128]{2,1,0:T(8,128)} %constant.17.clone.col_ref) | copy-start | bytes 196612
  45.7 22.8 %all-to-all-start.2 = ((bf16[16,64,128]{2,1,0:T(8,128)(2,1)}), bf16[16,64,128]{2,1,0:T(8,128)(2,1)S(1)}, u32[]{:S(2)}, u32[]{:S(2)}) async-start(bf16[16,64,128]{2,1,0:T(8,128)(2,1)} %shard_map.132), calls=%async_computation.2 | async-start | bytes 524288 | tf_op jit(solution)/shard_map/context/all_to_all | solution.py:342
  49.9 18.7 %copy-start.4 = (f32[4]{0:T(128)S(1)}, f32[4]{0:T(128)}, u32[]{:S(2)}) copy-start(f32[4]{0:T(128)} %sink_ref.1) | copy-start | bytes 52
  49.9 18.7 %copy-start.5 = (f32[4]{0:T(128)S(1)}, f32[4]{0:T(128)}, u32[]{:S(2)}) copy-start(f32[4]{0:T(128)} %bias_ref.1) | copy-start | bytes 52
  53.0 15.6 %copy-start = (bf16[1024,512]{1,0:T(8,128)(2,1)S(1)}, bf16[1024,512]{1,0:T(8,128)(2,1)}, u32[]{:S(2)}) copy-start(bf16[1024,512]{1,0:T(8,128)(2,1)} %w_ref.1) | copy-start | bytes 3145732
  53.0 7.9 %collective-permute-start = (bf16[128,128]{1,0:T(8,128)(2,1)S(1)}, bf16[128,128]{1,0:T(8,128)(2,1)S(1)}, u32[]{:S(2)}, u32[]{:S(2)}) collective-permute-start(bf16[128,128]{1,0:T(8,128)(2,1)S(1)} %get-tuple-element.18), channel_id=1, source_target_pairs={{0,32},{32,64},{64,96},{96,128},{128,160},{160,192},{192,224},{224... | collective-permute-start | bytes 98312 | tf_op jit(solution)/shard_map/halo/ppermute | solution.py:364
  56.5 6.3 %collective-permute-start.1 = (bf16[128,128]{1,0:T(8,128)(2,1)S(1)}, bf16[128,128]{1,0:T(8,128)(2,1)S(1)}, u32[]{:S(2)}, u32[]{:S(2)}) collective-permute-start(bf16[128,128]{1,0:T(8,128)(2,1)S(1)} %get-tuple-element.19), channel_id=1, source_target_pairs={{32,0},{64,32},{96,64},{128,96},{160,128},{192,160},{224,192},{256... | collective-permute-start | bytes 98312 | tf_op jit(solution)/shard_map/halo/ppermute | solution.py:365
